TPU v7x, 256 devices: a whole 4x4x8 slice. The times are simulated.
256 devices in a mesh: ep: 32 (over z, x), tp: 8 (over y, core).
Axes of the slice: x: 4, y: 4, z: 8, core: 2. Of those that a mesh axis runs over, the one named last changes fastest.
Arguments:
- tokens: bfloat16 [2048, 2048], P('ep'), may hold values from -6 to 6
- norm_gain: float32 [2048], replicated, may hold values from 0.1 to 1.9
- norm_shift: float32 [2048], replicated, may hold values from -3 to 3
- expert_ids: int32 [2048, 4], P('ep'), may hold values from 0 to 63, as said below
- gate_weights: float32 [2048, 4], P('ep'), may hold values from 0.1 to 1
- expert_gate: bfloat16 [64, 2048, 512], P('ep', None, 'tp'), may hold values from -0.125 to 0.125
- expert_up: bfloat16 [64, 2048, 512], P('ep', None, 'tp'), may hold values from -0.125 to 0.125
- expert_down: bfloat16 [64, 512, 2048], P('ep', 'tp'), may hold values from -0.25 to 0.25
Outputs:
- mixed_out: bfloat16 [2048, 2048], P('ep', 'tp')
Inputs may be any that keep to these rules, and one draw needn't show every extreme that they name: `expert_ids`: each row names 4 distinct experts that all lie in one group of 16 consecutive expert numbers. In the rows of one index of ep (aligned blocks of 64 rows) no expert is named by more than 8 rows, and in every block some expert is named by exactly 8 rows.
All inputs are finite; a program needn't handle non-finite values.
Results may differ from a plain program's by a relative error of at most 0.002.
Values may be sent and summed in bfloat16 or wider, within the bound.
No kernel may reach another device: no remote copies, remote signals or barrier semaphores. Data moves between devices by JAX's collectives and lax.ppermute only.
A program may use at most 64 MiB of HBM per device.

v0:
```python
import functools

import jax
import jax.numpy as jnp
from jax import lax
from jax.experimental import pallas as pl
from jax.experimental.pallas import tpu as pltpu
from jax.sharding import PartitionSpec as P


GROUPS = 4
CORES = 2
EPSILON = 1e-05
LANES = 128
HEADROOM = 13.0
TINY = 1e-30

VMEM = pl.BlockSpec(memory_space=pltpu.VMEM)
PARAMS = pltpu.CompilerParams(vmem_limit_bytes=12 * 1024 * 1024)


def on_chip(*arrays):
    return [pltpu.with_memory_space_constraint(a, pltpu.VMEM) for a in arrays]


def off_chip(*arrays):
    return [pltpu.with_memory_space_constraint(a, pltpu.HBM) for a in arrays]


def position():
    index = lax.axis_index("tp")
    return lax.shift_right_logical(index, 1), lax.bitwise_and(index, 1)


def dot_nn(a, b):
    return lax.dot_general(a, b, (((1,), (0,)), ((), ())), preferred_element_type=jnp.float32)


def dot_nt(a, b):
    return lax.dot_general(a, b, (((1,), (1,)), ((), ())), preferred_element_type=jnp.float32)


def dot_tn(a, b):
    return lax.dot_general(a, b, (((0,), (0,)), ((), ())), preferred_element_type=jnp.float32)


def iota(shape, dimension):
    return lax.broadcasted_iota(jnp.int32, shape, dimension)


def copy_all(pairs, sems):
    copies = [pltpu.make_async_copy(src, dst, sems.at[i]) for i, (src, dst) in enumerate(pairs)]
    for copy in copies:
        copy.start()
    return copies


def theirs_kernel(gate, up, out, sems):
    _, core = position()
    for copy in copy_all([(ref.at[1 - core], out.at[i]) for i, ref in enumerate((gate, up))], sems):
        copy.wait()


def pick_kernel(both, kept, giving):
    _, core = position()
    for i in range(2):
        kept[i] = both[i, core]
        giving[i] = both[i, 1 - core]


def pack_kernel(
    gate, up, tokens, gain, shift, ids, weights, stacked, packed, select_hi, select_lo, sems, *, slots
):
    copies = copy_all([(gate, stacked.at[0]), (up, stacked.at[1])], sems)
    y, core = position()
    row_half = lax.bitwise_and(y, 1)
    top_count, rows = ids.shape
    total = packed.shape[0]
    experts = total // slots
    width = packed.shape[1]
    values = tokens[...].astype(jnp.float32)
    centre = jnp.mean(values, axis=-1, keepdims=True)
    spread = jnp.mean(jnp.square(values - centre), axis=-1, keepdims=True)
    scaled = (values - centre) * lax.rsqrt(spread + EPSILON) * gain[...] + shift[...]
    normed = scaled.astype(jnp.bfloat16)
    expert = CORES * iota((experts, rows), 0) + core
    named = jnp.zeros((experts, rows), jnp.float32)
    weight = jnp.zeros((experts, rows), jnp.float32)
    for k in range(top_count):
        hit = ids[k : k + 1, :] == expert
        named = jnp.where(hit, 1.0, named)
        weight = jnp.where(hit, weights[k : k + 1, :], weight)
    earlier = jnp.where(iota((rows, rows), 0) < iota((rows, rows), 1), 1.0, 0.0)
    rank = dot_nn(named.astype(jnp.bfloat16), earlier.astype(jnp.bfloat16))
    slot = jnp.where(named > 0.0, rank, -1.0)
    cube = (experts, slots, rows)
    slot = jnp.broadcast_to(slot[:, None, :], cube)
    place = iota(cube, 1)
    sent = row_half * (slots // 2) + lax.rem(place, slots // 2)
    one_hot = jnp.where(slot == sent.astype(jnp.float32), 1.0, 0.0)
    one_hot = one_hot.reshape(total, rows).astype(jnp.bfloat16)
    first = dot_nn(one_hot, normed[:, :width])
    second = dot_nn(one_hot, normed[:, width:])
    front = lax.rem(iota((total, width), 0), slots) < slots // 2
    packed[...] = jnp.where(front, first, second).astype(jnp.bfloat16)
    factor = jnp.where(
        slot == place.astype(jnp.float32), jnp.broadcast_to(weight[:, None, :], cube), 0.0
    ).reshape(total, rows)
    high = factor.astype(jnp.bfloat16)
    select_hi[...] = high
    select_lo[...] = (factor - high.astype(jnp.float32)).astype(jnp.bfloat16)
    for copy in copies:
        copy.wait()


def pieces_kernel(down, kept, sent, sems):
    y, _ = position()
    share = kept.shape[-1]
    near, same, across = others(y)
    pairs = []
    for chips, out in (((y, same), kept), ((near, across), sent)):
        for i, chip in enumerate(chips):
            columns = pl.ds(pl.multiple_of(chip * share, share), share)
            pairs.append((down.at[:, :, columns], out.at[:, i]))
    for copy in copy_all(pairs, sems):
        copy.wait()


def others(y):
    return lax.bitwise_xor(y, 1), 3 - y, lax.bitwise_xor(y, 2)


def hidden_kernel(own_gate, own_up, arrived, swapped, kept_in, passed, hidden, local, sems, *, slots):
    _, core = position()
    copies = copy_all([(ref.at[core], local.at[i]) for i, ref in enumerate((own_gate, own_up))], sems)
    rows, width = arrived.shape
    kept = rows // 2
    count = slots // 2
    i, j = iota((kept, rows), 0), iota((kept, rows), 1)
    source = (i // count) * slots + i % count
    values = arrived[...]
    xs = []
    for q in range(2):
        pick = jnp.where(j == source + q * count, 1.0, 0.0).astype(jnp.bfloat16)
        xs.append(dot_nn(pick, values).astype(jnp.bfloat16))
    for copy in copies:
        copy.wait()
    total = None
    for q, x in enumerate(xs):
        at = slice(q * width, (q + 1) * width)
        w = jnp.concatenate(
            [ref[m, :, at] for m in range(2) for ref in (local, swapped, kept_in, passed)]
        )
        product = dot_nt(x, w)
        total = product if total is None else total + product
    units = total.shape[1] // 2
    value = total[:, :units]
    result = value / (1.0 + jnp.exp(-value)) * total[:, units:]
    hidden[...] = result.astype(jnp.bfloat16)


def give_kernel(kept, near, giving):
    _, core = position()
    giving[0] = kept[1 - core]
    giving[1] = near[1 - core]


def join_kernel(kept, near, other, mine, sent):
    _, core = position()
    units = kept.shape[2]
    for i, out in enumerate((mine, sent)):
        for j, value in enumerate((kept[core, i], other[0, i], near[core, i], other[1, i])):
            out[j * units : (j + 1) * units, :] = value


def down_kernel(h_own, h_first, h_second, h_third, mine, same, out, *, slots):
    y, core = position()
    row_half = lax.bitwise_and(y, 1)
    rows = out.shape[0]
    kept = h_own.shape[0]
    count = slots // 2
    units = h_own.shape[1] // 2
    r, j = iota((rows, 2 * kept), 0), iota((rows, 2 * kept), 1)
    i = lax.rem(j, kept)
    half = jnp.where(j < kept, row_half, 1 - row_half)
    place = (i // count) * slots + half * count + i % count
    spread = jnp.where(r == place, 1.0, 0.0).astype(jnp.bfloat16)
    turn = lax.bitwise_xor(core, row_half) == 1
    lower = iota((kept, units), 1) < units // 2

    def passed(a, b):
        a, b = a[:, units:], b[:, units:]
        forward, backward = jnp.where(lower, a, b), jnp.where(lower, b, a)
        return jnp.where(turn, forward, backward), jnp.where(turn, backward, forward)

    for_own, for_third = passed(h_first[...], h_second[...])
    for_first, for_second = passed(h_third[...], h_own[...])
    tops = (h_own[:, :units], for_first, for_second, h_third[:, :units])
    bottoms = (for_own, h_first[:, :units], h_second[:, :units], for_third)
    pieces = jnp.concatenate([jnp.concatenate(tops, axis=1), jnp.concatenate(bottoms, axis=1)])
    h = dot_nn(spread, pieces).astype(jnp.bfloat16)
    total = dot_nn(h[:, : 2 * units], mine[...]) + dot_nn(h[:, 2 * units :], same[...])
    largest = jnp.max(jnp.abs(total), axis=1, keepdims=True)
    exponent = jnp.ceil(jnp.log2(jnp.maximum(largest, TINY)))
    width = total.shape[1]
    out[:, :width] = total * jnp.exp2(HEADROOM - exponent)
    out[:, width:] = jnp.broadcast_to(exponent, (rows, out.shape[1] - width))


def combine_kernel(select_hi, select_lo, returned, kept, sent):
    _, core = position()
    width = CORES * kept.shape[1]
    values = returned[:, :width] * jnp.exp2(returned[:, width : width + 1] - HEADROOM)
    high = values.astype(jnp.bfloat16)
    low = (values - high.astype(jnp.float32)).astype(jnp.bfloat16)
    total = dot_tn(select_hi[...], high) + dot_tn(select_lo[...], high)
    total = total + dot_tn(select_hi[...], low)
    half = kept.shape[1]
    first, second = total[:, :half], total[:, half:]
    kept[...] = jnp.where(core == 0, first, second)
    sent[...] = jnp.where(core == 0, second, first)


def per_device(
    tokens, norm_gain, norm_shift, expert_ids, gate_weights, expert_gate, expert_up, expert_down
):
    tok_rows, features = tokens.shape
    top_count = expert_ids.shape[1]
    ep_size = lax.axis_size("ep")
    tp_size = lax.axis_size("tp")
    chips = tp_size // CORES
    total_experts = expert_gate.shape[0] * ep_size
    group_size = total_experts // GROUPS
    slots = tok_rows // 2 * top_count // group_size
    rows = ep_size * slots
    share = features // chips
    units = expert_gate.shape[2]
    swap = [(i, i ^ 1) for i in range(tp_size)]
    near = [(i, i ^ 2) for i in range(tp_size)]
    same = [(i, 6 - i // 2 * 2 + i % 2) for i in range(tp_size)]
    across = [(i, i ^ 4) for i in range(tp_size)]
    turns = [(i, (i + (2 if i % 2 else -2)) % tp_size) for i in range(tp_size)]
    anywhere = pl.BlockSpec(memory_space=pl.ANY)

    def ppermute(array, pairs):
        return lax.ppermute(array, "tp", pairs)

    gate_t, up_t = off_chip(expert_gate.transpose(0, 2, 1), expert_up.transpose(0, 2, 1))
    stacked, packed, select_hi, select_lo = pl.pallas_call(
        functools.partial(pack_kernel, slots=slots),
        out_shape=(
            pltpu.VMEM((2, 2, units, features), jnp.bfloat16),
            pltpu.VMEM((rows, features // 2), jnp.bfloat16),
            pltpu.VMEM((rows, tok_rows), jnp.bfloat16),
            pltpu.VMEM((rows, tok_rows), jnp.bfloat16),
        ),
        in_specs=[anywhere] * 2 + [VMEM] * 5,
        out_specs=(VMEM,) * 4,
        scratch_shapes=[pltpu.SemaphoreType.DMA((2,))],
        compiler_params=PARAMS,
        name="pack",
    )(
        gate_t,
        up_t,
        *off_chip(
            tokens,
            norm_gain.reshape(1, features),
            norm_shift.reshape(1, features),
            expert_ids.T,
            gate_weights.T,
        )
    )
    both = ppermute(stacked, turns)
    arrived = lax.all_to_all(
        packed.reshape(ep_size, slots, features // 2), "ep", split_axis=0, concat_axis=0, tiled=True
    ).reshape(rows, features // 2)

    giving = pl.pallas_call(
        theirs_kernel,
        out_shape=pltpu.VMEM((2, units, features), jnp.bfloat16),
        in_specs=[anywhere] * 2,
        out_specs=VMEM,
        scratch_shapes=[pltpu.SemaphoreType.DMA((2,))],
        compiler_params=PARAMS,
        name="theirs",
    )(gate_t, up_t)
    swapped = ppermute(giving, swap)

    pair = pltpu.VMEM((2, units, features), jnp.bfloat16)
    kept, picked = pl.pallas_call(
        pick_kernel,
        out_shape=(pair, pair),
        in_specs=[VMEM],
        out_specs=(VMEM, VMEM),
        compiler_params=PARAMS,
        name="pick",
    )(*on_chip(both))
    passed = ppermute(picked, swap)

    halves = pltpu.VMEM((2, 2, units, share), jnp.bfloat16)
    whole = pltpu.VMEM((4 * units, share), jnp.bfloat16)
    d_kept, d_sent = pl.pallas_call(
        pieces_kernel,
        out_shape=(halves, halves),
        in_specs=[anywhere],
        out_specs=(VMEM, VMEM),
        scratch_shapes=[pltpu.SemaphoreType.DMA((4,))],
        compiler_params=PARAMS,
        name="pieces",
    )(*off_chip(expert_down))
    d_near = ppermute(d_sent, near)
    d_giving = pl.pallas_call(
        give_kernel,
        out_shape=halves,
        in_specs=[VMEM] * 2,
        out_specs=VMEM,
        compiler_params=PARAMS,
        name="give",
    )(*on_chip(d_kept, d_near))
    d_other = ppermute(d_giving, swap)
    d_mine, d_passing = pl.pallas_call(
        join_kernel,
        out_shape=(whole, whole),
        in_specs=[VMEM] * 3,
        out_specs=(VMEM, VMEM),
        compiler_params=PARAMS,
        name="join",
    )(*on_chip(d_kept, d_near, d_other))
    d_same = ppermute(d_passing, same)

    hidden = pl.pallas_call(
        functools.partial(hidden_kernel, slots=slots),
        out_shape=pltpu.VMEM((rows // 2, 2 * CORES * units), jnp.bfloat16),
        in_specs=[anywhere] * 2 + [VMEM] * 4,
        out_specs=VMEM,
        scratch_shapes=[
            pltpu.VMEM((2, units, features), jnp.bfloat16),
            pltpu.SemaphoreType.DMA((2,)),
        ],
        compiler_params=PARAMS,
        name="hidden",
    )(gate_t, up_t, *on_chip(arrived, swapped, kept, passed))
    hiddens = [hidden] + [ppermute(hidden, pairs) for pairs in (near, same, across)]
    result = pl.pallas_call(
        functools.partial(down_kernel, slots=slots),
        out_shape=pltpu.VMEM((rows, share + LANES), jnp.float32),
        in_specs=[VMEM] * (chips + 2),
        out_specs=VMEM,
        compiler_params=PARAMS,
        name="down",
    )(*on_chip(*hiddens, d_mine, d_same))
    wire = result.astype(jnp.float16).reshape(ep_size, slots, share + LANES)
    returned = lax.all_to_all(wire, "ep", split_axis=0, concat_axis=0, tiled=True)
    returned = returned.astype(jnp.float32).reshape(rows, share + LANES)
    half = pltpu.VMEM((tok_rows, share // CORES), jnp.float32)
    kept, sent = pl.pallas_call(
        combine_kernel,
        out_shape=(half, half),
        in_specs=[VMEM] * 3,
        out_specs=(VMEM, VMEM),
        compiler_params=PARAMS,
        name="combine",
    )(*on_chip(select_hi, select_lo, returned))
    mixed_out = kept + lax.ppermute(sent, "tp", swap)
    return mixed_out.astype(jnp.bfloat16)


def solution(mesh):
    return jax.shard_map(
        per_device,
        mesh=mesh,
        in_specs=(
            P("ep", None),
            P(),
            P(),
            P("ep", None),
            P("ep", None),
            P("ep", None, "tp"),
            P("ep", None, "tp"),
            P("ep", "tp", None),
        ),
        out_specs=P("ep", "tp"),
        check_vma=False,
    )
```

profile of v0, /device:TPU:1, one launch (start us, length us, event | category | flops | bytes accessed | tf_op | source)
XLA Modules:
  0.0 67.9 jit_solution(8590110136646194714)
XLA Ops:
  0.0 3.6 %pack.1 = (bf16[2,2,64,2048]{3,2,1,0:T(8,128)(2,1)}, bf16[256,1024]{1,0:T(8,128)(2,1)}, bf16[256,64]{1,0:T(8,128)(2,1)S(1)}, bf16[256,64]{1,0:T(8,128)(2,1)S(1)}) custom-call(bf16[2,64,2048]{2,1,0:T(8,128)(2,1)} %bitcast.14, bf16[2,64,2048]{2,1,0:T(8,128)(2,1)} %bitcast.17, bf16[64,2048]{1,0:T(8,128)(2,1)} %tokens.1, f32[1,2048]{1,0:T(1,128)} %bitcast.20, ...), custom_call_target="tpu_custom_call" | custom-call | tf_op jit(solution)/shard_map/pack/pallas_call | solution.py:249
  3.6 2.2 %collective-permute-start.1 = (bf16[2,2,64,2048]{3,2,1,0:T(8,128)(2,1)}, bf16[2,2,64,2048]{3,2,1,0:T(8,128)(2,1)S(1)}, u32[]{:S(2)}, u32[]{:S(2)}) collective-permute-start(bf16[2,2,64,2048]{3,2,1,0:T(8,128)(2,1)} %get-tuple-element.20), channel_id=1, source_target_pairs={{0,6},{1,3},{2,0},{3,5},{4,2},{5,7},{6,4},{7,1},{8,14},{9,11},{10,... | collective-permute-start | bytes 3145736 | tf_op jit(solution)/shard_map/ppermute | solution.py:246
  5.8 11.0 %all-to-all-start = ((bf16[32,8,1024]{2,1,0:T(8,128)(2,1)}), bf16[32,8,1024]{2,1,0:T(8,128)(2,1)S(1)}, u32[]{:S(2)}, u32[]{:S(2)}) async-start(bf16[32,8,1024]{2,1,0:T(8,128)(2,1)} %bitcast.6), calls=%async_computation | async-start | bytes 1048576 | tf_op jit(solution)/shard_map/all_to_all | solution.py:274
  16.9 1.1 %pieces.1 = (bf16[2,2,64,512]{3,2,1,0:T(8,128)(2,1)S(1)}, bf16[2,2,64,512]{3,2,1,0:T(8,128)(2,1)S(1)}) custom-call(bf16[2,64,2048]{2,1,0:T(8,128)(2,1)} %down.2), custom_call_target="tpu_custom_call" | custom-call | tf_op jit(solution)/shard_map/pieces/pallas_call | solution.py:302
  18.0 1.4 %collective-permute-start.6 = (bf16[2,2,64,512]{3,2,1,0:T(8,128)(2,1)S(1)}, bf16[2,2,64,512]{3,2,1,0:T(8,128)(2,1)S(1)}, u32[]{:S(2)}, u32[]{:S(2)}) collective-permute-start(bf16[2,2,64,512]{3,2,1,0:T(8,128)(2,1)S(1)} %get-tuple-element.24), channel_id=1, source_target_pairs={{0,2},{1,3},{2,0},{3,1},{4,6},{5,7},{6,4},{7,5},{8,10},{9,11},{10,... | collective-permute-start | bytes 786440 | tf_op jit(solution)/shard_map/ppermute | solution.py:246
  19.4 1.0 %theirs.1 = bf16[2,64,2048]{2,1,0:T(8,128)(2,1)S(1)} custom-call(bf16[2,64,2048]{2,1,0:T(8,128)(2,1)} %bitcast.15, bf16[2,64,2048]{2,1,0:T(8,128)(2,1)} %bitcast.18), custom_call_target="tpu_custom_call" | custom-call | tf_op jit(solution)/shard_map/theirs/pallas_call | solution.py:278
  20.5 1.5 %collective-permute-start = (bf16[2,64,2048]{2,1,0:T(8,128)(2,1)S(1)}, bf16[2,64,2048]{2,1,0:T(8,128)(2,1)S(1)}, u32[]{:S(2)}, u32[]{:S(2)}) collective-permute-start(bf16[2,64,2048]{2,1,0:T(8,128)(2,1)S(1)} %theirs.1), channel_id=1, source_target_pairs={{0,1},{1,0},{2,3},{3,2},{4,5},{5,4},{6,7},{7,6},{8,9},{9,8},{10,11... | collective-permute-start | bytes 1572872 | tf_op jit(solution)/shard_map/ppermute | solution.py:246
  21.9 0.0 collective-permute-done.1.both
  21.9 0.1 pick.1
  22.0 0.8 %collective-permute-start.2 = (bf16[2,64,2048]{2,1,0:T(8,128)(2,1)S(1)}, bf16[2,64,2048]{2,1,0:T(8,128)(2,1)S(1)}, u32[]{:S(2)}, u32[]{:S(2)}) collective-permute-start(bf16[2,64,2048]{2,1,0:T(8,128)(2,1)S(1)} %get-tuple-element.22), channel_id=1, source_target_pairs={{0,1},{1,0},{2,3},{3,2},{4,5},{5,4},{6,7},{7,6},{8,9},{9,8},{10,11... | collective-permute-start | bytes 1572872 | tf_op jit(solution)/shard_map/ppermute | solution.py:246
  22.8 1.9 %collective-permute-done.6.near = bf16[2,2,64,512]{3,2,1,0:T(8,128)(2,1)S(1)} collective-permute-done((bf16[2,2,64,512]{3,2,1,0:T(8,128)(2,1)S(1)}, bf16[2,2,64,512]{3,2,1,0:T(8,128)(2,1)S(1)}, u32[]{:S(2)}, u32[]{:S(2)}) %collective-permute-start.6) | collective-permute-done | bytes 262176 | tf_op jit(solution)/shard_map/ppermute | solution.py:246
  24.7 2.9 %collective-permute-start.7 = (bf16[2,2,64,512]{3,2,1,0:T(8,128)(2,1)S(1)}, bf16[2,2,64,512]{3,2,1,0:T(8,128)(2,1)S(1)}, u32[]{:S(2)}, u32[]{:S(2)}) collective-permute-start(bf16[2,2,64,512]{3,2,1,0:T(8,128)(2,1)S(1)} %give.1), channel_id=1, source_target_pairs={{0,1},{1,0},{2,3},{3,2},{4,5},{5,4},{6,7},{7,6},{8,9},{9,8},{10,11... | collective-permute-start | bytes 786440 | tf_op jit(solution)/shard_map/ppermute | solution.py:246
  27.6 1.2 %collective-permute-done.7.other = bf16[2,2,64,512]{3,2,1,0:T(8,128)(2,1)S(1)} collective-permute-done((bf16[2,2,64,512]{3,2,1,0:T(8,128)(2,1)S(1)}, bf16[2,2,64,512]{3,2,1,0:T(8,128)(2,1)S(1)}, u32[]{:S(2)}, u32[]{:S(2)}) %collective-permute-start.7) | collective-permute-done | bytes 262176 | tf_op jit(solution)/shard_map/ppermute | solution.py:246
  28.8 0.7 %join.1 = (bf16[256,512]{1,0:T(8,128)(2,1)S(1)}, bf16[256,512]{1,0:T(8,128)(2,1)}) custom-call(bf16[2,2,64,512]{3,2,1,0:T(8,128)(2,1)S(1)} %get-tuple-element.23.kept, bf16[2,2,64,512]{3,2,1,0:T(8,128)(2,1)S(1)} %collective-permute-done.6.near, bf16[2,2,64,512]{3,2,1,0:T(8,128)(2,1)S(1)} %collective-permute-done.7.other), custom_call_target="tpu_custom_call" | custom-call | tf_op jit(solution)/shard_map/join/pallas_call | solution.py:321
  29.5 0.8 %collective-permute-start.8 = (bf16[256,512]{1,0:T(8,128)(2,1)}, bf16[256,512]{1,0:T(8,128)(2,1)S(1)}, u32[]{:S(2)}, u32[]{:S(2)}) collective-permute-start(bf16[256,512]{1,0:T(8,128)(2,1)} %get-tuple-element.26), channel_id=1, source_target_pairs={{0,6},{1,7},{2,4},{3,5},{4,2},{5,3},{6,0},{7,1},{8,14},{9,15},{10,... | collective-permute-start | bytes 786440 | tf_op jit(solution)/shard_map/ppermute | solution.py:246
  30.3 0.0 collective-permute-done.swapped
  30.3 0.9 %all-to-all-done = bf16[32,8,1024]{2,1,0:T(8,128)(2,1)S(1)} async-done(((bf16[32,8,1024]{2,1,0:T(8,128)(2,1)}), bf16[32,8,1024]{2,1,0:T(8,128)(2,1)S(1)}, u32[]{:S(2)}, u32[]{:S(2)}) %all-to-all-start) | async-done | bytes 524320 | tf_op jit(solution)/shard_map/all_to_all | solution.py:274
  31.1 0.0 collective-permute-done.2.passed
  31.2 2.0 %hidden.1.h_own = bf16[128,256]{1,0:T(8,128)(2,1)S(1)} custom-call(bf16[2,64,2048]{2,1,0:T(8,128)(2,1)} %bitcast.16, bf16[2,64,2048]{2,1,0:T(8,128)(2,1)} %bitcast.19, bf16[256,1024]{1,0:T(8,128)(2,1)S(1)} %bitcast.13, bf16[2,64,2048]{2,1,0:T(8,128)(2,1)S(1)} %collective-permute-done.swapped, bf16[2,64,2048]{2,1,0:T(8,128)(2,1)S(1)} %get-tuple-element.21.kept_in, ...), custom_call_target="tpu_custom_call" | custom-call | tf_op jit(solution)/shard_map/hidden/pallas_call | solution.py:331
  33.1 4.1 %collective-permute-start.3 = (bf16[128,256]{1,0:T(8,128)(2,1)S(1)}, bf16[128,256]{1,0:T(8,128)(2,1)S(1)}, u32[]{:S(2)}, u32[]{:S(2)}) collective-permute-start(bf16[128,256]{1,0:T(8,128)(2,1)S(1)} %hidden.1.h_own), channel_id=1, source_target_pairs={{0,2},{1,3},{2,0},{3,1},{4,6},{5,7},{6,4},{7,5},{8,10},{9,11},{10,... | collective-permute-start | bytes 196616 | tf_op jit(solution)/shard_map/ppermute | solution.py:246
  37.2 1.4 %collective-permute-start.4 = (bf16[128,256]{1,0:T(8,128)(2,1)S(1)}, bf16[128,256]{1,0:T(8,128)(2,1)S(1)}, u32[]{:S(2)}, u32[]{:S(2)}) collective-permute-start(bf16[128,256]{1,0:T(8,128)(2,1)S(1)} %hidden.1.h_own), channel_id=1, source_target_pairs={{0,6},{1,7},{2,4},{3,5},{4,2},{5,3},{6,0},{7,1},{8,14},{9,15},{10,... | collective-permute-start | bytes 196616 | tf_op jit(solution)/shard_map/ppermute | solution.py:246
  38.6 0.5 collective-permute-start.5
  39.1 0.0 collective-permute-done.8.same
  39.1 0.1 collective-permute-done.3.h_first
  39.1 2.4 %collective-permute-done.4.h_second = bf16[128,256]{1,0:T(8,128)(2,1)S(1)} collective-permute-done((bf16[128,256]{1,0:T(8,128)(2,1)S(1)}, bf16[128,256]{1,0:T(8,128)(2,1)S(1)}, u32[]{:S(2)}, u32[]{:S(2)}) %collective-permute-start.4) | collective-permute-done | bytes 65568 | tf_op jit(solution)/shard_map/ppermute | solution.py:246
  41.5 1.7 %collective-permute-done.5.h_third = bf16[128,256]{1,0:T(8,128)(2,1)S(1)} collective-permute-done((bf16[128,256]{1,0:T(8,128)(2,1)S(1)}, bf16[128,256]{1,0:T(8,128)(2,1)S(1)}, u32[]{:S(2)}, u32[]{:S(2)}) %collective-permute-start.5) | collective-permute-done | bytes 65568 | tf_op jit(solution)/shard_map/ppermute | solution.py:246
  43.2 0.5 down.3
  43.8 18.1 %all_to_all.10 = f16[32,8,640]{2,1,0:T(8,128)(2,1)S(1)} all-to-all(f16[32,8,640]{2,1,0:T(8,128)(2,1)S(1)} %convert_bitcast_fusion), channel_id=1, replica_groups=mesh['ep'=32,'tp'=8] {'ep'}, dimensions={0} | all-to-all | bytes 655360 | tf_op jit(solution)/shard_map/all_to_all | solution.py:353
  62.0 0.3 combine.1
  62.3 4.1 %collective-permute-start.9 = (f32[64,256]{1,0:T(8,128)S(1)}, f32[64,256]{1,0:T(8,128)S(1)}, u32[]{:S(2)}, u32[]{:S(2)}) collective-permute-start(f32[64,256]{1,0:T(8,128)S(1)} %get-tuple-element.28), channel_id=1, source_target_pairs={{0,1},{1,0},{2,3},{3,2},{4,5},{5,4},{6,7},{7,6},{8,9},{9,8},{10,11... | collective-permute-start | bytes 196616 | tf_op jit(solution)/shard_map/ppermute | solution.py:364
  66.4 0.9 %collective-permute-done.9 = f32[64,256]{1,0:T(8,128)S(1)} collective-permute-done((f32[64,256]{1,0:T(8,128)S(1)}, f32[64,256]{1,0:T(8,128)S(1)}, u32[]{:S(2)}, u32[]{:S(2)}) %collective-permute-start.9) | collective-permute-done | bytes 65568 | tf_op jit(solution)/shard_map/ppermute | solution.py:364
  67.3 0.6 add_convert_fusion
  (3 shorter events, 0.1 us)
Async XLA Ops:
  3.6 18.3 %collective-permute-start.1 = (bf16[2,2,64,2048]{3,2,1,0:T(8,128)(2,1)}, bf16[2,2,64,2048]{3,2,1,0:T(8,128)(2,1)S(1)}, u32[]{:S(2)}, u32[]{:S(2)}) collective-permute-start(bf16[2,2,64,2048]{3,2,1,0:T(8,128)(2,1)} %get-tuple-element.20), channel_id=1, source_target_pairs={{0,6},{1,3},{2,0},{3,5},{4,2},{5,7},{6,4},{7,1},{8,14},{9,11},{10,... | collective-permute-start | bytes 3145736 | tf_op jit(solution)/shard_map/ppermute | solution.py:246
  5.8 25.3 %all-to-all-start = ((bf16[32,8,1024]{2,1,0:T(8,128)(2,1)}), bf16[32,8,1024]{2,1,0:T(8,128)(2,1)S(1)}, u32[]{:S(2)}, u32[]{:S(2)}) async-start(bf16[32,8,1024]{2,1,0:T(8,128)(2,1)} %bitcast.6), calls=%async_computation | async-start | bytes 1048576 | tf_op jit(solution)/shard_map/all_to_all | solution.py:274
  18.0 6.7 %collective-permute-start.6 = (bf16[2,2,64,512]{3,2,1,0:T(8,128)(2,1)S(1)}, bf16[2,2,64,512]{3,2,1,0:T(8,128)(2,1)S(1)}, u32[]{:S(2)}, u32[]{:S(2)}) collective-permute-start(bf16[2,2,64,512]{3,2,1,0:T(8,128)(2,1)S(1)} %get-tuple-element.24), channel_id=1, source_target_pairs={{0,2},{1,3},{2,0},{3,1},{4,6},{5,7},{6,4},{7,5},{8,10},{9,11},{10,... | collective-permute-start | bytes 786440 | tf_op jit(solution)/shard_map/ppermute | solution.py:246
  20.5 9.8 %collective-permute-start = (bf16[2,64,2048]{2,1,0:T(8,128)(2,1)S(1)}, bf16[2,64,2048]{2,1,0:T(8,128)(2,1)S(1)}, u32[]{:S(2)}, u32[]{:S(2)}) collective-permute-start(bf16[2,64,2048]{2,1,0:T(8,128)(2,1)S(1)} %theirs.1), channel_id=1, source_target_pairs={{0,1},{1,0},{2,3},{3,2},{4,5},{5,4},{6,7},{7,6},{8,9},{9,8},{10,11... | collective-permute-start | bytes 1572872 | tf_op jit(solution)/shard_map/ppermute | solution.py:246
  22.0 9.1 %collective-permute-start.2 = (bf16[2,64,2048]{2,1,0:T(8,128)(2,1)S(1)}, bf16[2,64,2048]{2,1,0:T(8,128)(2,1)S(1)}, u32[]{:S(2)}, u32[]{:S(2)}) collective-permute-start(bf16[2,64,2048]{2,1,0:T(8,128)(2,1)S(1)} %get-tuple-element.22), channel_id=1, source_target_pairs={{0,1},{1,0},{2,3},{3,2},{4,5},{5,4},{6,7},{7,6},{8,9},{9,8},{10,11... | collective-permute-start | bytes 1572872 | tf_op jit(solution)/shard_map/ppermute | solution.py:246
  24.7 4.1 %collective-permute-start.7 = (bf16[2,2,64,512]{3,2,1,0:T(8,128)(2,1)S(1)}, bf16[2,2,64,512]{3,2,1,0:T(8,128)(2,1)S(1)}, u32[]{:S(2)}, u32[]{:S(2)}) collective-permute-start(bf16[2,2,64,512]{3,2,1,0:T(8,128)(2,1)S(1)} %give.1), channel_id=1, source_target_pairs={{0,1},{1,0},{2,3},{3,2},{4,5},{5,4},{6,7},{7,6},{8,9},{9,8},{10,11... | collective-permute-start | bytes 786440 | tf_op jit(solution)/shard_map/ppermute | solution.py:246
  29.5 9.6 %collective-permute-start.8 = (bf16[256,512]{1,0:T(8,128)(2,1)}, bf16[256,512]{1,0:T(8,128)(2,1)S(1)}, u32[]{:S(2)}, u32[]{:S(2)}) collective-permute-start(bf16[256,512]{1,0:T(8,128)(2,1)} %get-tuple-element.26), channel_id=1, source_target_pairs={{0,6},{1,7},{2,4},{3,5},{4,2},{5,3},{6,0},{7,1},{8,14},{9,15},{10,... | collective-permute-start | bytes 786440 | tf_op jit(solution)/shard_map/ppermute | solution.py:246
  33.1 6.0 %collective-permute-start.3 = (bf16[128,256]{1,0:T(8,128)(2,1)S(1)}, bf16[128,256]{1,0:T(8,128)(2,1)S(1)}, u32[]{:S(2)}, u32[]{:S(2)}) collective-permute-start(bf16[128,256]{1,0:T(8,128)(2,1)S(1)} %hidden.1.h_own), channel_id=1, source_target_pairs={{0,2},{1,3},{2,0},{3,1},{4,6},{5,7},{6,4},{7,5},{8,10},{9,11},{10,... | collective-permute-start | bytes 196616 | tf_op jit(solution)/shard_map/ppermute | solution.py:246
  37.2 4.3 %collective-permute-start.4 = (bf16[128,256]{1,0:T(8,128)(2,1)S(1)}, bf16[128,256]{1,0:T(8,128)(2,1)S(1)}, u32[]{:S(2)}, u32[]{:S(2)}) collective-permute-start(bf16[128,256]{1,0:T(8,128)(2,1)S(1)} %hidden.1.h_own), channel_id=1, source_target_pairs={{0,6},{1,7},{2,4},{3,5},{4,2},{5,3},{6,0},{7,1},{8,14},{9,15},{10,... | collective-permute-start | bytes 196616 | tf_op jit(solution)/shard_map/ppermute | solution.py:246
  38.6 4.6 %collective-permute-start.5 = (bf16[128,256]{1,0:T(8,128)(2,1)S(1)}, bf16[128,256]{1,0:T(8,128)(2,1)S(1)}, u32[]{:S(2)}, u32[]{:S(2)}) collective-permute-start(bf16[128,256]{1,0:T(8,128)(2,1)S(1)} %hidden.1.h_own), channel_id=1, source_target_pairs={{0,4},{1,5},{2,6},{3,7},{4,0},{5,1},{6,2},{7,3},{8,12},{9,13},{10,... | collective-permute-start | bytes 196616 | tf_op jit(solution)/shard_map/ppermute | solution.py:246
  62.3 5.0 %collective-permute-start.9 = (f32[64,256]{1,0:T(8,128)S(1)}, f32[64,256]{1,0:T(8,128)S(1)}, u32[]{:S(2)}, u32[]{:S(2)}) collective-permute-start(f32[64,256]{1,0:T(8,128)S(1)} %get-tuple-element.28), channel_id=1, source_target_pairs={{0,1},{1,0},{2,3},{3,2},{4,5},{5,4},{6,7},{7,6},{8,9},{9,8},{10,11... | collective-permute-start | bytes 196616 | tf_op jit(solution)/shard_map/ppermute | solution.py:364
where the time goes:
time: 68.3 us; the launch traced here: 67.9 us
  starting transfers between devices  30.6 us (45%)
  blocking collectives  18.1 us (27%)
  Pallas kernels  9.48 us (14%)
  waiting for transfers between devices  8.97 us (13%)
  other arithmetic  0.71 us (1%)
    all_to_all x1, blocking collectives, per_device(): lax.all_to_all(wire, 'ep', split_axis=0, concat_axis=0, tiled=True)  18.1 us
    ppermute x9, starting transfers between devices, ppermute(): return lax.ppermute(array, 'tp', pairs)  15.4 us
    all_to_all x1, starting transfers between devices, per_device(): lax.all_to_all(packed.reshape(ep_size, slots, features // 2), 'ep', split...  11 us
    ppermute x9, waiting for transfers between devices, ppermute(): return lax.ppermute(array, 'tp', pairs)  7.22 us
    ppermute x1, starting transfers between devices, per_device(): mixed_out = kept + lax.ppermute(sent, 'tp', swap)  4.09 us
    pallas_call x1, Pallas kernels, per_device(): pl.pallas_call(functools.partial(pack_kernel, slots=slots), out_shape=(pl...  3.62 us
    pallas_call x1, Pallas kernels, per_device(): pl.pallas_call(functools.partial(hidden_kernel, slots=slots), out_shape=p...  1.97 us
  transfers between devices with their start and end apart: 11, of which 7 were waited for; matrix products, arithmetic and copies ran while one was open for 0% of the time, Pallas kernels for 7%

commit v1 on v0

--- a/solution.py
+++ b/solution.py
@@ -61,17 +61,14 @@
         copy.wait()
 
 
-def pick_kernel(both, kept, giving):
-    _, core = position()
-    for i in range(2):
-        kept[i] = both[i, core]
-        giving[i] = both[i, 1 - core]
-
-
-def pack_kernel(
-    gate, up, tokens, gain, shift, ids, weights, stacked, packed, select_hi, select_lo, sems, *, slots
-):
-    copies = copy_all([(gate, stacked.at[0]), (up, stacked.at[1])], sems)
+def pick_kernel(gate, up, kept, giving):
+    _, core = position()
+    for i, ref in enumerate((gate, up)):
+        kept[i] = ref[core]
+        giving[i] = ref[1 - core]
+
+
+def pack_kernel(tokens, gain, shift, ids, weights, packed, select_hi, select_lo, *, slots):
     y, core = position()
     row_half = lax.bitwise_and(y, 1)
     top_count, rows = ids.shape
@@ -109,19 +106,15 @@
     high = factor.astype(jnp.bfloat16)
     select_hi[...] = high
     select_lo[...] = (factor - high.astype(jnp.float32)).astype(jnp.bfloat16)
-    for copy in copies:
-        copy.wait()
-
-
-def pieces_kernel(down, kept, sent, sems):
+
+
+def pieces_kernel(down, own, first, second, third, sems):
     y, _ = position()
-    share = kept.shape[-1]
-    near, same, across = others(y)
+    share = own.shape[-1]
     pairs = []
-    for chips, out in (((y, same), kept), ((near, across), sent)):
-        for i, chip in enumerate(chips):
-            columns = pl.ds(pl.multiple_of(chip * share, share), share)
-            pairs.append((down.at[:, :, columns], out.at[:, i]))
+    for chip, piece in zip((y, *others(y)), (own, first, second, third)):
+        columns = pl.ds(pl.multiple_of(chip * share, share), share)
+        pairs.append((down.at[:, :, columns], piece))
     for copy in copy_all(pairs, sems):
         copy.wait()
 
@@ -159,21 +152,13 @@
     hidden[...] = result.astype(jnp.bfloat16)
 
 
-def give_kernel(kept, near, giving):
-    _, core = position()
-    giving[0] = kept[1 - core]
-    giving[1] = near[1 - core]
-
-
-def join_kernel(kept, near, other, mine, sent):
-    _, core = position()
-    units = kept.shape[2]
-    for i, out in enumerate((mine, sent)):
-        for j, value in enumerate((kept[core, i], other[0, i], near[core, i], other[1, i])):
-            out[j * units : (j + 1) * units, :] = value
-
-
-def down_kernel(h_own, h_first, h_second, h_third, mine, same, out, *, slots):
+def give_kernel(own, first, second, third, giving):
+    _, core = position()
+    for i, ref in enumerate((own, first, second, third)):
+        giving[i] = ref[1 - core]
+
+
+def down_kernel(h_own, h_first, h_second, h_third, own, first, second, third, other, out, *, slots):
     y, core = position()
     row_half = lax.bitwise_and(y, 1)
     rows = out.shape[0]
@@ -199,7 +184,8 @@
     bottoms = (for_own, h_first[:, :units], h_second[:, :units], for_third)
     pieces = jnp.concatenate([jnp.concatenate(tops, axis=1), jnp.concatenate(bottoms, axis=1)])
     h = dot_nn(spread, pieces).astype(jnp.bfloat16)
-    total = dot_nn(h[:, : 2 * units], mine[...]) + dot_nn(h[:, 2 * units :], same[...])
+    w = [(ref[core], other[i]) for i, ref in enumerate((own, first, second, third))]
+    total = dot_nn(h, jnp.concatenate([block for pair in w for block in pair]))
     largest = jnp.max(jnp.abs(total), axis=1, keepdims=True)
     exponent = jnp.ceil(jnp.log2(jnp.maximum(largest, TINY)))
     width = total.shape[1]
@@ -246,22 +232,18 @@
         return lax.ppermute(array, "tp", pairs)
 
     gate_t, up_t = off_chip(expert_gate.transpose(0, 2, 1), expert_up.transpose(0, 2, 1))
-    stacked, packed, select_hi, select_lo = pl.pallas_call(
+    packed, select_hi, select_lo = pl.pallas_call(
         functools.partial(pack_kernel, slots=slots),
         out_shape=(
-            pltpu.VMEM((2, 2, units, features), jnp.bfloat16),
             pltpu.VMEM((rows, features // 2), jnp.bfloat16),
             pltpu.VMEM((rows, tok_rows), jnp.bfloat16),
             pltpu.VMEM((rows, tok_rows), jnp.bfloat16),
         ),
-        in_specs=[anywhere] * 2 + [VMEM] * 5,
-        out_specs=(VMEM,) * 4,
-        scratch_shapes=[pltpu.SemaphoreType.DMA((2,))],
+        in_specs=[VMEM] * 5,
+        out_specs=(VMEM,) * 3,
         compiler_params=PARAMS,
         name="pack",
     )(
-        gate_t,
-        up_t,
         *off_chip(
             tokens,
             norm_gain.reshape(1, features),
@@ -270,7 +252,8 @@
             gate_weights.T,
         )
     )
-    both = ppermute(stacked, turns)
+    gate_both = ppermute(expert_gate.transpose(0, 2, 1), turns)
+    up_both = ppermute(expert_up.transpose(0, 2, 1), turns)
     arrived = lax.all_to_all(
         packed.reshape(ep_size, slots, features // 2), "ep", split_axis=0, concat_axis=0, tiled=True
     ).reshape(rows, features // 2)
@@ -290,43 +273,34 @@
     kept, picked = pl.pallas_call(
         pick_kernel,
         out_shape=(pair, pair),
-        in_specs=[VMEM],
+        in_specs=[VMEM] * 2,
         out_specs=(VMEM, VMEM),
         compiler_params=PARAMS,
         name="pick",
-    )(*on_chip(both))
+    )(*on_chip(gate_both, up_both))
     passed = ppermute(picked, swap)
 
-    halves = pltpu.VMEM((2, 2, units, share), jnp.bfloat16)
-    whole = pltpu.VMEM((4 * units, share), jnp.bfloat16)
-    d_kept, d_sent = pl.pallas_call(
+    piece = pltpu.VMEM((2, units, share), jnp.bfloat16)
+    pieces = pl.pallas_call(
         pieces_kernel,
-        out_shape=(halves, halves),
+        out_shape=(piece,) * chips,
         in_specs=[anywhere],
-        out_specs=(VMEM, VMEM),
-        scratch_shapes=[pltpu.SemaphoreType.DMA((4,))],
+        out_specs=(VMEM,) * chips,
+        scratch_shapes=[pltpu.SemaphoreType.DMA((chips,))],
         compiler_params=PARAMS,
         name="pieces",
     )(*off_chip(expert_down))
-    d_near = ppermute(d_sent, near)
+    downs = [ppermute(p, pairs) for p, pairs in zip(pieces[1:], (near, same, across))]
+    downs = on_chip(pieces[0], *downs)
     d_giving = pl.pallas_call(
         give_kernel,
-        out_shape=halves,
-        in_specs=[VMEM] * 2,
+        out_shape=pltpu.VMEM((chips, units, share), jnp.bfloat16),
+        in_specs=[VMEM] * chips,
         out_specs=VMEM,
         compiler_params=PARAMS,
         name="give",
-    )(*on_chip(d_kept, d_near))
+    )(*downs)
     d_other = ppermute(d_giving, swap)
-    d_mine, d_passing = pl.pallas_call(
-        join_kernel,
-        out_shape=(whole, whole),
-        in_specs=[VMEM] * 3,
-        out_specs=(VMEM, VMEM),
-        compiler_params=PARAMS,
-        name="join",
-    )(*on_chip(d_kept, d_near, d_other))
-    d_same = ppermute(d_passing, same)
 
     hidden = pl.pallas_call(
         functools.partial(hidden_kernel, slots=slots),
@@ -344,11 +318,11 @@
     result = pl.pallas_call(
         functools.partial(down_kernel, slots=slots),
         out_shape=pltpu.VMEM((rows, share + LANES), jnp.float32),
-        in_specs=[VMEM] * (chips + 2),
+        in_specs=[VMEM] * (2 * chips + 1),
         out_specs=VMEM,
         compiler_params=PARAMS,
         name="down",
-    )(*on_chip(*hiddens, d_mine, d_same))
+    )(*on_chip(*hiddens), *downs, *on_chip(d_other))
     wire = result.astype(jnp.float16).reshape(ep_size, slots, share + LANES)
     returned = lax.all_to_all(wire, "ep", split_axis=0, concat_axis=0, tiled=True)
     returned = returned.astype(jnp.float32).reshape(rows, share + LANES)

time: 68.3 us -> 68.6 us (level)
  starting transfers between devices: 30.6 us -> 28.7 us
  blocking collectives: 18.1 us -> 19.9 us
  waiting for transfers between devices: 8.97 us -> 10.5 us
  Pallas kernels: 9.48 us -> 8.38 us
    ppermute x9 -> x11, waiting for transfers between devices: 7.22 us -> 9.61 us  [ppermute(): return lax.ppermute(array, 'tp', pairs)]
    ppermute x9 -> x11, starting transfers between devices: 15.4 us -> 13.4 us  [ppermute(): return lax.ppermute(array, 'tp', pairs)]
    all_to_all x1, blocking collectives: 18.1 us -> 19.9 us  [per_device(): lax.all_to_all(wire, 'ep', split_axis=0, concat_axis=0, tiled=True)]
    pallas_call x1, Pallas kernels: 3.62 us -> 2.45 us  [per_device(): pl.pallas_call(functools.partial(pack_kernel, slots=slots), out_shape=(pl...]
    all_to_all x1, waiting for transfers between devices: 0.85 us -> 0.01 us  [per_device(): lax.all_to_all(packed.reshape(ep_size, slots, features // 2), 'ep', split...]
    pallas_call x4 -> x3, Pallas kernels: 1.96 us -> 2.02 us  [the longest x1 1.13 us: per_device(): pl.pallas_call(pieces_kernel, out_shape=(piece,) * chips, in_specs=[anywh...]
  transfers between devices with their start and end apart: 11 -> 13, of which waited for: 7 -> 5; matrix products, arithmetic and copies ran while one was open for 0% -> 0% of each run, Pallas kernels for 7% -> 11%
where the time goes in v1:
time: 68.6 us; the launch traced here: 68.3 us
  starting transfers between devices  28.7 us (42%)
  blocking collectives  19.9 us (29%)
  waiting for transfers between devices  10.5 us (15%)
  Pallas kernels  8.38 us (12%)
  other arithmetic  0.71 us (1%)
    all_to_all x1, blocking collectives, per_device(): lax.all_to_all(wire, 'ep', split_axis=0, concat_axis=0, tiled=True)  19.9 us
    ppermute x11, starting transfers between devices, ppermute(): return lax.ppermute(array, 'tp', pairs)  13.4 us
    all_to_all x1, starting transfers between devices, per_device(): lax.all_to_all(packed.reshape(ep_size, slots, features // 2), 'ep', split...  11 us
    ppermute x11, waiting for transfers between devices, ppermute(): return lax.ppermute(array, 'tp', pairs)  9.61 us
    ppermute x1, starting transfers between devices, per_device(): mixed_out = kept + lax.ppermute(sent, 'tp', swap)  4.24 us
    pallas_call x1, Pallas kernels, per_device(): pl.pallas_call(functools.partial(pack_kernel, slots=slots), out_shape=(pl...  2.45 us
    pallas_call x1, Pallas kernels, per_device(): pl.pallas_call(functools.partial(hidden_kernel, slots=slots), out_shape=p...  1.98 us
  transfers between devices with their start and end apart: 13, of which 5 were waited for; matrix products, arithmetic and copies ran while one was open for 0% of the time, Pallas kernels for 11%

profile of v1, /device:TPU:1, one launch (start us, length us, event | category | flops | bytes accessed | tf_op | source)
XLA Modules:
  0.0 68.3 jit_solution(18311483535310982831)
XLA Ops:
  0.0 2.1 %collective-permute-start.1 = (bf16[2,64,2048]{2,1,0:T(8,128)(2,1)}, bf16[2,64,2048]{2,1,0:T(8,128)(2,1)S(1)}, u32[]{:S(2)}, u32[]{:S(2)}) collective-permute-start(bf16[2,64,2048]{2,1,0:T(8,128)(2,1)} %bitcast.14), channel_id=1, source_target_pairs={{0,6},{1,3},{2,0},{3,5},{4,2},{5,7},{6,4},{7,1},{8,14},{9,11},{10,... | collective-permute-start | bytes 1572872 | tf_op jit(solution)/shard_map/ppermute | solution.py:232
  2.1 1.3 %collective-permute-start.2 = (bf16[2,64,2048]{2,1,0:T(8,128)(2,1)}, bf16[2,64,2048]{2,1,0:T(8,128)(2,1)S(1)}, u32[]{:S(2)}, u32[]{:S(2)}) collective-permute-start(bf16[2,64,2048]{2,1,0:T(8,128)(2,1)} %bitcast.17), channel_id=1, source_target_pairs={{0,6},{1,3},{2,0},{3,5},{4,2},{5,7},{6,4},{7,1},{8,14},{9,11},{10,... | collective-permute-start | bytes 1572872 | tf_op jit(solution)/shard_map/ppermute | solution.py:232
  3.4 2.5 %pack.1 = (bf16[256,1024]{1,0:T(8,128)(2,1)}, bf16[256,64]{1,0:T(8,128)(2,1)S(1)}, bf16[256,64]{1,0:T(8,128)(2,1)S(1)}) custom-call(bf16[64,2048]{1,0:T(8,128)(2,1)} %tokens.1, f32[1,2048]{1,0:T(1,128)} %bitcast.20, f32[1,2048]{1,0:T(1,128)} %bitcast.21, s32[4,64]{1,0:T(4,128)} %bitcast.22, f32[4,64]{1,0:T(4,128)} %bitcast.23), custom_call_target="tpu_custom_call" | custom-call | tf_op jit(solution)/shard_map/pack/pallas_call | solution.py:235
  5.9 11.0 %all-to-all-start = ((bf16[32,8,1024]{2,1,0:T(8,128)(2,1)}), bf16[32,8,1024]{2,1,0:T(8,128)(2,1)S(1)}, u32[]{:S(2)}, u32[]{:S(2)}) async-start(bf16[32,8,1024]{2,1,0:T(8,128)(2,1)} %bitcast.6), calls=%async_computation | async-start | bytes 1048576 | tf_op jit(solution)/shard_map/all_to_all | solution.py:257
  16.9 1.1 %theirs.1 = bf16[2,64,2048]{2,1,0:T(8,128)(2,1)S(1)} custom-call(bf16[2,64,2048]{2,1,0:T(8,128)(2,1)} %bitcast.15, bf16[2,64,2048]{2,1,0:T(8,128)(2,1)} %bitcast.18), custom_call_target="tpu_custom_call" | custom-call | tf_op jit(solution)/shard_map/theirs/pallas_call | solution.py:261
  18.0 2.2 %collective-permute-start = (bf16[2,64,2048]{2,1,0:T(8,128)(2,1)S(1)}, bf16[2,64,2048]{2,1,0:T(8,128)(2,1)S(1)}, u32[]{:S(2)}, u32[]{:S(2)}) collective-permute-start(bf16[2,64,2048]{2,1,0:T(8,128)(2,1)S(1)} %theirs.1), channel_id=1, source_target_pairs={{0,1},{1,0},{2,3},{3,2},{4,5},{5,4},{6,7},{7,6},{8,9},{9,8},{10,11... | collective-permute-start | bytes 1572872 | tf_op jit(solution)/shard_map/ppermute | solution.py:232
  20.2 0.0 collective-permute-done.1.gate
  20.2 0.0 collective-permute-done.2.up
  20.2 0.9 %pick.1 = (bf16[2,64,2048]{2,1,0:T(8,128)(2,1)S(1)}, bf16[2,64,2048]{2,1,0:T(8,128)(2,1)}) custom-call(bf16[2,64,2048]{2,1,0:T(8,128)(2,1)S(1)} %collective-permute-done.1.gate, bf16[2,64,2048]{2,1,0:T(8,128)(2,1)S(1)} %collective-permute-done.2.up), custom_call_target="tpu_custom_call" | custom-call | tf_op jit(solution)/shard_map/pick/pallas_call | solution.py:273
  21.1 0.0 collective-permute-start.3
  21.1 1.1 %pieces.1 = (bf16[2,64,512]{2,1,0:T(8,128)(2,1)S(1)}, bf16[2,64,512]{2,1,0:T(8,128)(2,1)S(1)}, bf16[2,64,512]{2,1,0:T(8,128)(2,1)S(1)}, bf16[2,64,512]{2,1,0:T(8,128)(2,1)S(1)}) custom-call(bf16[2,64,2048]{2,1,0:T(8,128)(2,1)} %down.2), custom_call_target="tpu_custom_call" | custom-call | tf_op jit(solution)/shard_map/pieces/pallas_call | solution.py:284
  22.2 1.1 %collective-permute-start.7 = (bf16[2,64,512]{2,1,0:T(8,128)(2,1)S(1)}, bf16[2,64,512]{2,1,0:T(8,128)(2,1)S(1)}, u32[]{:S(2)}, u32[]{:S(2)}) collective-permute-start(bf16[2,64,512]{2,1,0:T(8,128)(2,1)S(1)} %get-tuple-element.22), channel_id=1, source_target_pairs={{0,2},{1,3},{2,0},{3,1},{4,6},{5,7},{6,4},{7,5},{8,10},{9,11},{10,... | collective-permute-start | bytes 393224 | tf_op jit(solution)/shard_map/ppermute | solution.py:232
  23.3 0.0 collective-permute-start.8
  23.3 2.2 %collective-permute-start.9 = (bf16[2,64,512]{2,1,0:T(8,128)(2,1)S(1)}, bf16[2,64,512]{2,1,0:T(8,128)(2,1)S(1)}, u32[]{:S(2)}, u32[]{:S(2)}) collective-permute-start(bf16[2,64,512]{2,1,0:T(8,128)(2,1)S(1)} %get-tuple-element.24), channel_id=1, source_target_pairs={{0,4},{1,5},{2,6},{3,7},{4,0},{5,1},{6,2},{7,3},{8,12},{9,13},{10,... | collective-permute-start | bytes 393224 | tf_op jit(solution)/shard_map/ppermute | solution.py:232
  25.6 1.3 %collective-permute-done.7.first = bf16[2,64,512]{2,1,0:T(8,128)(2,1)S(1)} collective-permute-done((bf16[2,64,512]{2,1,0:T(8,128)(2,1)S(1)}, bf16[2,64,512]{2,1,0:T(8,128)(2,1)S(1)}, u32[]{:S(2)}, u32[]{:S(2)}) %collective-permute-start.7) | collective-permute-done | bytes 131104 | tf_op jit(solution)/shard_map/ppermute | solution.py:232
  26.9 5.3 %collective-permute-done.8.second = bf16[2,64,512]{2,1,0:T(8,128)(2,1)S(1)} collective-permute-done((bf16[2,64,512]{2,1,0:T(8,128)(2,1)S(1)}, bf16[2,64,512]{2,1,0:T(8,128)(2,1)S(1)}, u32[]{:S(2)}, u32[]{:S(2)}) %collective-permute-start.8) | collective-permute-done | bytes 131104 | tf_op jit(solution)/shard_map/ppermute | solution.py:232
  32.2 0.0 collective-permute-done.9.third
  32.2 1.1 %collective-permute-start.10 = (bf16[4,64,512]{2,1,0:T(8,128)(2,1)S(1)}, bf16[4,64,512]{2,1,0:T(8,128)(2,1)S(1)}, u32[]{:S(2)}, u32[]{:S(2)}) collective-permute-start(bf16[4,64,512]{2,1,0:T(8,128)(2,1)S(1)} %give.1), channel_id=1, source_target_pairs={{0,1},{1,0},{2,3},{3,2},{4,5},{5,4},{6,7},{7,6},{8,9},{9,8},{10,11... | collective-permute-start | bytes 786440 | tf_op jit(solution)/shard_map/ppermute | solution.py:232
  33.4 0.0 collective-permute-done.swapped
  33.4 0.0 all-to-all-done
  33.4 0.0 collective-permute-done.3.passed
  33.4 2.0 %hidden.1.h_own = bf16[128,256]{1,0:T(8,128)(2,1)S(1)} custom-call(bf16[2,64,2048]{2,1,0:T(8,128)(2,1)} %bitcast.16, bf16[2,64,2048]{2,1,0:T(8,128)(2,1)} %bitcast.19, bf16[256,1024]{1,0:T(8,128)(2,1)S(1)} %bitcast.13, bf16[2,64,2048]{2,1,0:T(8,128)(2,1)S(1)} %collective-permute-done.swapped, bf16[2,64,2048]{2,1,0:T(8,128)(2,1)S(1)} %get-tuple-element.19.kept_in, ...), custom_call_target="tpu_custom_call" | custom-call | tf_op jit(solution)/shard_map/hidden/pallas_call | solution.py:305
  35.4 0.1 collective-permute-start.4
  35.5 1.6 %collective-permute-start.5 = (bf16[128,256]{1,0:T(8,128)(2,1)S(1)}, bf16[128,256]{1,0:T(8,128)(2,1)S(1)}, u32[]{:S(2)}, u32[]{:S(2)}) collective-permute-start(bf16[128,256]{1,0:T(8,128)(2,1)S(1)} %hidden.1.h_own), channel_id=1, source_target_pairs={{0,6},{1,7},{2,4},{3,5},{4,2},{5,3},{6,0},{7,1},{8,14},{9,15},{10,... | collective-permute-start | bytes 196616 | tf_op jit(solution)/shard_map/ppermute | solution.py:232
  37.0 1.7 %collective-permute-start.6 = (bf16[128,256]{1,0:T(8,128)(2,1)S(1)}, bf16[128,256]{1,0:T(8,128)(2,1)S(1)}, u32[]{:S(2)}, u32[]{:S(2)}) collective-permute-start(bf16[128,256]{1,0:T(8,128)(2,1)S(1)} %hidden.1.h_own), channel_id=1, source_target_pairs={{0,4},{1,5},{2,6},{3,7},{4,0},{5,1},{6,2},{7,3},{8,12},{9,13},{10,... | collective-permute-start | bytes 196616 | tf_op jit(solution)/shard_map/ppermute | solution.py:232
  38.7 0.0 collective-permute-done.10.other
  38.7 0.0 collective-permute-done.4.h_first
  38.7 1.2 %collective-permute-done.5.h_second = bf16[128,256]{1,0:T(8,128)(2,1)S(1)} collective-permute-done((bf16[128,256]{1,0:T(8,128)(2,1)S(1)}, bf16[128,256]{1,0:T(8,128)(2,1)S(1)}, u32[]{:S(2)}, u32[]{:S(2)}) %collective-permute-start.5) | collective-permute-done | bytes 65568 | tf_op jit(solution)/shard_map/ppermute | solution.py:232
  39.9 1.8 %collective-permute-done.6.h_third = bf16[128,256]{1,0:T(8,128)(2,1)S(1)} collective-permute-done((bf16[128,256]{1,0:T(8,128)(2,1)S(1)}, bf16[128,256]{1,0:T(8,128)(2,1)S(1)}, u32[]{:S(2)}, u32[]{:S(2)}) %collective-permute-start.6) | collective-permute-done | bytes 65568 | tf_op jit(solution)/shard_map/ppermute | solution.py:232
  41.7 0.5 down.3
  42.2 19.9 %all_to_all.10 = f16[32,8,640]{2,1,0:T(8,128)(2,1)S(1)} all-to-all(f16[32,8,640]{2,1,0:T(8,128)(2,1)S(1)} %convert_bitcast_fusion), channel_id=1, replica_groups=mesh['ep'=32,'tp'=8] {'ep'}, dimensions={0} | all-to-all | bytes 655360 | tf_op jit(solution)/shard_map/all_to_all | solution.py:327
  62.2 0.3 combine.1
  62.5 4.2 %collective-permute-start.11 = (f32[64,256]{1,0:T(8,128)S(1)}, f32[64,256]{1,0:T(8,128)S(1)}, u32[]{:S(2)}, u32[]{:S(2)}) collective-permute-start(f32[64,256]{1,0:T(8,128)S(1)} %get-tuple-element.26), channel_id=1, source_target_pairs={{0,1},{1,0},{2,3},{3,2},{4,5},{5,4},{6,7},{7,6},{8,9},{9,8},{10,11... | collective-permute-start | bytes 196616 | tf_op jit(solution)/shard_map/ppermute | solution.py:338
  66.8 0.9 %collective-permute-done.11 = f32[64,256]{1,0:T(8,128)S(1)} collective-permute-done((f32[64,256]{1,0:T(8,128)S(1)}, f32[64,256]{1,0:T(8,128)S(1)}, u32[]{:S(2)}, u32[]{:S(2)}) %collective-permute-start.11) | collective-permute-done | bytes 65568 | tf_op jit(solution)/shard_map/ppermute | solution.py:338
  67.7 0.6 add_convert_fusion
  (3 shorter events, 0.1 us)
Async XLA Ops:
  0.0 20.2 %collective-permute-start.1 = (bf16[2,64,2048]{2,1,0:T(8,128)(2,1)}, bf16[2,64,2048]{2,1,0:T(8,128)(2,1)S(1)}, u32[]{:S(2)}, u32[]{:S(2)}) collective-permute-start(bf16[2,64,2048]{2,1,0:T(8,128)(2,1)} %bitcast.14), channel_id=1, source_target_pairs={{0,6},{1,3},{2,0},{3,5},{4,2},{5,7},{6,4},{7,1},{8,14},{9,11},{10,... | collective-permute-start | bytes 1572872 | tf_op jit(solution)/shard_map/ppermute | solution.py:232
  2.1 18.1 %collective-permute-start.2 = (bf16[2,64,2048]{2,1,0:T(8,128)(2,1)}, bf16[2,64,2048]{2,1,0:T(8,128)(2,1)S(1)}, u32[]{:S(2)}, u32[]{:S(2)}) collective-permute-start(bf16[2,64,2048]{2,1,0:T(8,128)(2,1)} %bitcast.17), channel_id=1, source_target_pairs={{0,6},{1,3},{2,0},{3,5},{4,2},{5,7},{6,4},{7,1},{8,14},{9,11},{10,... | collective-permute-start | bytes 1572872 | tf_op jit(solution)/shard_map/ppermute | solution.py:232
  5.9 27.5 %all-to-all-start = ((bf16[32,8,1024]{2,1,0:T(8,128)(2,1)}), bf16[32,8,1024]{2,1,0:T(8,128)(2,1)S(1)}, u32[]{:S(2)}, u32[]{:S(2)}) async-start(bf16[32,8,1024]{2,1,0:T(8,128)(2,1)} %bitcast.6), calls=%async_computation | async-start | bytes 1048576 | tf_op jit(solution)/shard_map/all_to_all | solution.py:257
  18.0 15.4 %collective-permute-start = (bf16[2,64,2048]{2,1,0:T(8,128)(2,1)S(1)}, bf16[2,64,2048]{2,1,0:T(8,128)(2,1)S(1)}, u32[]{:S(2)}, u32[]{:S(2)}) collective-permute-start(bf16[2,64,2048]{2,1,0:T(8,128)(2,1)S(1)} %theirs.1), channel_id=1, source_target_pairs={{0,1},{1,0},{2,3},{3,2},{4,5},{5,4},{6,7},{7,6},{8,9},{9,8},{10,11... | collective-permute-start | bytes 1572872 | tf_op jit(solution)/shard_map/ppermute | solution.py:232
  21.1 12.3 %collective-permute-start.3 = (bf16[2,64,2048]{2,1,0:T(8,128)(2,1)}, bf16[2,64,2048]{2,1,0:T(8,128)(2,1)S(1)}, u32[]{:S(2)}, u32[]{:S(2)}) collective-permute-start(bf16[2,64,2048]{2,1,0:T(8,128)(2,1)} %get-tuple-element.20), channel_id=1, source_target_pairs={{0,1},{1,0},{2,3},{3,2},{4,5},{5,4},{6,7},{7,6},{8,9},{9,8},{10,11... | collective-permute-start | bytes 1572872 | tf_op jit(solution)/shard_map/ppermute | solution.py:232
  22.2 4.7 %collective-permute-start.7 = (bf16[2,64,512]{2,1,0:T(8,128)(2,1)S(1)}, bf16[2,64,512]{2,1,0:T(8,128)(2,1)S(1)}, u32[]{:S(2)}, u32[]{:S(2)}) collective-permute-start(bf16[2,64,512]{2,1,0:T(8,128)(2,1)S(1)} %get-tuple-element.22), channel_id=1, source_target_pairs={{0,2},{1,3},{2,0},{3,1},{4,6},{5,7},{6,4},{7,5},{8,10},{9,11},{10,... | collective-permute-start | bytes 393224 | tf_op jit(solution)/shard_map/ppermute | solution.py:232
  23.3 8.9 %collective-permute-start.8 = (bf16[2,64,512]{2,1,0:T(8,128)(2,1)S(1)}, bf16[2,64,512]{2,1,0:T(8,128)(2,1)S(1)}, u32[]{:S(2)}, u32[]{:S(2)}) collective-permute-start(bf16[2,64,512]{2,1,0:T(8,128)(2,1)S(1)} %get-tuple-element.23), channel_id=1, source_target_pairs={{0,6},{1,7},{2,4},{3,5},{4,2},{5,3},{6,0},{7,1},{8,14},{9,15},{10,... | collective-permute-start | bytes 393224 | tf_op jit(solution)/shard_map/ppermute | solution.py:232
  23.3 8.9 %collective-permute-start.9 = (bf16[2,64,512]{2,1,0:T(8,128)(2,1)S(1)}, bf16[2,64,512]{2,1,0:T(8,128)(2,1)S(1)}, u32[]{:S(2)}, u32[]{:S(2)}) collective-permute-start(bf16[2,64,512]{2,1,0:T(8,128)(2,1)S(1)} %get-tuple-element.24), channel_id=1, source_target_pairs={{0,4},{1,5},{2,6},{3,7},{4,0},{5,1},{6,2},{7,3},{8,12},{9,13},{10,... | collective-permute-start | bytes 393224 | tf_op jit(solution)/shard_map/ppermute | solution.py:232
  32.2 6.5 %collective-permute-start.10 = (bf16[4,64,512]{2,1,0:T(8,128)(2,1)S(1)}, bf16[4,64,512]{2,1,0:T(8,128)(2,1)S(1)}, u32[]{:S(2)}, u32[]{:S(2)}) collective-permute-start(bf16[4,64,512]{2,1,0:T(8,128)(2,1)S(1)} %give.1), channel_id=1, source_target_pairs={{0,1},{1,0},{2,3},{3,2},{4,5},{5,4},{6,7},{7,6},{8,9},{9,8},{10,11... | collective-permute-start | bytes 786440 | tf_op jit(solution)/shard_map/ppermute | solution.py:232
  35.4 3.3 %collective-permute-start.4 = (bf16[128,256]{1,0:T(8,128)(2,1)S(1)}, bf16[128,256]{1,0:T(8,128)(2,1)S(1)}, u32[]{:S(2)}, u32[]{:S(2)}) collective-permute-start(bf16[128,256]{1,0:T(8,128)(2,1)S(1)} %hidden.1.h_own), channel_id=1, source_target_pairs={{0,2},{1,3},{2,0},{3,1},{4,6},{5,7},{6,4},{7,5},{8,10},{9,11},{10,... | collective-permute-start | bytes 196616 | tf_op jit(solution)/shard_map/ppermute | solution.py:232
  35.5 4.4 %collective-permute-start.5 = (bf16[128,256]{1,0:T(8,128)(2,1)S(1)}, bf16[128,256]{1,0:T(8,128)(2,1)S(1)}, u32[]{:S(2)}, u32[]{:S(2)}) collective-permute-start(bf16[128,256]{1,0:T(8,128)(2,1)S(1)} %hidden.1.h_own), channel_id=1, source_target_pairs={{0,6},{1,7},{2,4},{3,5},{4,2},{5,3},{6,0},{7,1},{8,14},{9,15},{10,... | collective-permute-start | bytes 196616 | tf_op jit(solution)/shard_map/ppermute | solution.py:232
  37.0 4.6 %collective-permute-start.6 = (bf16[128,256]{1,0:T(8,128)(2,1)S(1)}, bf16[128,256]{1,0:T(8,128)(2,1)S(1)}, u32[]{:S(2)}, u32[]{:S(2)}) collective-permute-start(bf16[128,256]{1,0:T(8,128)(2,1)S(1)} %hidden.1.h_own), channel_id=1, source_target_pairs={{0,4},{1,5},{2,6},{3,7},{4,0},{5,1},{6,2},{7,3},{8,12},{9,13},{10,... | collective-permute-start | bytes 196616 | tf_op jit(solution)/shard_map/ppermute | solution.py:232
  62.5 5.1 %collective-permute-start.11 = (f32[64,256]{1,0:T(8,128)S(1)}, f32[64,256]{1,0:T(8,128)S(1)}, u32[]{:S(2)}, u32[]{:S(2)}) collective-permute-start(f32[64,256]{1,0:T(8,128)S(1)} %get-tuple-element.26), channel_id=1, source_target_pairs={{0,1},{1,0},{2,3},{3,2},{4,5},{5,4},{6,7},{7,6},{8,9},{9,8},{10,11... | collective-permute-start | bytes 196616 | tf_op jit(solution)/shard_map/ppermute | solution.py:338

commit v2 on v1

--- a/solution.py
+++ b/solution.py
@@ -68,41 +68,54 @@
         giving[i] = ref[1 - core]
 
 
-def pack_kernel(tokens, gain, shift, ids, weights, packed, select_hi, select_lo, *, slots):
+def slots_of(ids, core, experts, copies):
+    top_count, rows = ids.shape
+    ids = jnp.concatenate([ids] * copies, axis=1)
+    shape = (experts, rows * copies)
+    expert = CORES * iota(shape, 0) + core
+    hits = [ids[k : k + 1, :] == expert for k in range(top_count)]
+    named = functools.reduce(jnp.logical_or, hits)
+    ones = jnp.where(named, 1.0, 0.0).astype(jnp.bfloat16)
+    steps = (rows, rows * copies)
+    earlier = jnp.where(iota(steps, 0) < lax.rem(iota(steps, 1), rows), 1.0, 0.0)
+    rank = dot_nn(ones[:, :rows], earlier.astype(jnp.bfloat16))
+    return jnp.where(named, rank, -1.0), hits
+
+
+def pack_kernel(tokens, gain, shift, ids, packed, *, slots):
     y, core = position()
     row_half = lax.bitwise_and(y, 1)
-    top_count, rows = ids.shape
-    total = packed.shape[0]
-    experts = total // slots
-    width = packed.shape[1]
+    rows = ids.shape[1]
+    total, width = packed.shape
+    experts, count = total // slots, slots // 2
+    slot, _ = slots_of(ids[...], core, experts, 2)
+    cube = (experts, slots, 2 * rows)
+    place = iota(cube, 1)
+    sent = jnp.where(
+        (place < count) == (iota(cube, 2) < rows), row_half * count + lax.rem(place, count), -2
+    )
+    chosen = jnp.broadcast_to(slot[:, None, :], cube) == sent.astype(jnp.float32)
+    one_hot = jnp.where(chosen, 1.0, 0.0).reshape(total, 2 * rows).astype(jnp.bfloat16)
     values = tokens[...].astype(jnp.float32)
     centre = jnp.mean(values, axis=-1, keepdims=True)
     spread = jnp.mean(jnp.square(values - centre), axis=-1, keepdims=True)
     scaled = (values - centre) * lax.rsqrt(spread + EPSILON) * gain[...] + shift[...]
     normed = scaled.astype(jnp.bfloat16)
-    expert = CORES * iota((experts, rows), 0) + core
-    named = jnp.zeros((experts, rows), jnp.float32)
+    normed = jnp.concatenate([normed[:, :width], normed[:, width:]])
+    packed[...] = dot_nn(one_hot, normed).astype(jnp.bfloat16)
+
+
+def factors_kernel(ids, weights, select_hi, select_lo, *, slots):
+    _, core = position()
+    total, rows = select_hi.shape
+    experts = total // slots
+    slot, hits = slots_of(ids[...], core, experts, 1)
     weight = jnp.zeros((experts, rows), jnp.float32)
-    for k in range(top_count):
-        hit = ids[k : k + 1, :] == expert
-        named = jnp.where(hit, 1.0, named)
+    for k, hit in enumerate(hits):
         weight = jnp.where(hit, weights[k : k + 1, :], weight)
-    earlier = jnp.where(iota((rows, rows), 0) < iota((rows, rows), 1), 1.0, 0.0)
-    rank = dot_nn(named.astype(jnp.bfloat16), earlier.astype(jnp.bfloat16))
-    slot = jnp.where(named > 0.0, rank, -1.0)
     cube = (experts, slots, rows)
-    slot = jnp.broadcast_to(slot[:, None, :], cube)
-    place = iota(cube, 1)
-    sent = row_half * (slots // 2) + lax.rem(place, slots // 2)
-    one_hot = jnp.where(slot == sent.astype(jnp.float32), 1.0, 0.0)
-    one_hot = one_hot.reshape(total, rows).astype(jnp.bfloat16)
-    first = dot_nn(one_hot, normed[:, :width])
-    second = dot_nn(one_hot, normed[:, width:])
-    front = lax.rem(iota((total, width), 0), slots) < slots // 2
-    packed[...] = jnp.where(front, first, second).astype(jnp.bfloat16)
-    factor = jnp.where(
-        slot == place.astype(jnp.float32), jnp.broadcast_to(weight[:, None, :], cube), 0.0
-    ).reshape(total, rows)
+    chosen = jnp.broadcast_to(slot[:, None, :], cube) == iota(cube, 1).astype(jnp.float32)
+    factor = jnp.where(chosen, jnp.broadcast_to(weight[:, None, :], cube), 0.0).reshape(total, rows)
     high = factor.astype(jnp.bfloat16)
     select_hi[...] = high
     select_lo[...] = (factor - high.astype(jnp.float32)).astype(jnp.bfloat16)
@@ -136,19 +149,23 @@
     for q in range(2):
         pick = jnp.where(j == source + q * count, 1.0, 0.0).astype(jnp.bfloat16)
         xs.append(dot_nn(pick, values).astype(jnp.bfloat16))
+
+    def products(*refs):
+        total = None
+        for q, x in enumerate(xs):
+            at = slice(q * width, (q + 1) * width)
+            w = jnp.concatenate([ref[m, :, at] for m in range(2) for ref in refs])
+            product = dot_nt(x, w)
+            total = product if total is None else total + product
+        units = total.shape[1] // 2
+        return total[:, :units], total[:, units:]
+
+    others = products(swapped, kept_in, passed)
     for copy in copies:
         copy.wait()
-    total = None
-    for q, x in enumerate(xs):
-        at = slice(q * width, (q + 1) * width)
-        w = jnp.concatenate(
-            [ref[m, :, at] for m in range(2) for ref in (local, swapped, kept_in, passed)]
-        )
-        product = dot_nt(x, w)
-        total = product if total is None else total + product
-    units = total.shape[1] // 2
-    value = total[:, :units]
-    result = value / (1.0 + jnp.exp(-value)) * total[:, units:]
+    own = products(local)
+    value, upward = (jnp.concatenate(parts, axis=1) for parts in zip(own, others))
+    result = value / (1.0 + jnp.exp(-value)) * upward
     hidden[...] = result.astype(jnp.bfloat16)
 
 
@@ -232,26 +249,27 @@
         return lax.ppermute(array, "tp", pairs)
 
     gate_t, up_t = off_chip(expert_gate.transpose(0, 2, 1), expert_up.transpose(0, 2, 1))
-    packed, select_hi, select_lo = pl.pallas_call(
+    packed = pl.pallas_call(
         functools.partial(pack_kernel, slots=slots),
-        out_shape=(
-            pltpu.VMEM((rows, features // 2), jnp.bfloat16),
-            pltpu.VMEM((rows, tok_rows), jnp.bfloat16),
-            pltpu.VMEM((rows, tok_rows), jnp.bfloat16),
-        ),
-        in_specs=[VMEM] * 5,
-        out_specs=(VMEM,) * 3,
+        out_shape=pltpu.VMEM((rows, features // 2), jnp.bfloat16),
+        in_specs=[VMEM] * 4,
+        out_specs=VMEM,
         compiler_params=PARAMS,
         name="pack",
     )(
         *off_chip(
-            tokens,
-            norm_gain.reshape(1, features),
-            norm_shift.reshape(1, features),
-            expert_ids.T,
-            gate_weights.T,
+            tokens, norm_gain.reshape(1, features), norm_shift.reshape(1, features), expert_ids.T
         )
     )
+    factor = pltpu.VMEM((rows, tok_rows), jnp.bfloat16)
+    select_hi, select_lo = pl.pallas_call(
+        functools.partial(factors_kernel, slots=slots),
+        out_shape=(factor, factor),
+        in_specs=[VMEM] * 2,
+        out_specs=(VMEM,) * 2,
+        compiler_params=PARAMS,
+        name="factors",
+    )(*off_chip(expert_ids.T, gate_weights.T))
     gate_both = ppermute(expert_gate.transpose(0, 2, 1), turns)
     up_both = ppermute(expert_up.transpose(0, 2, 1), turns)
     arrived = lax.all_to_all(

time: 68.6 us -> 69.7 us (1.016)
  blocking collectives: 19.9 us -> 0 us
  waiting for transfers between devices: 10.5 us -> 20.3 us
  starting transfers between devices: 28.7 us -> 38.2 us
  Pallas kernels: 8.38 us -> 9.43 us
  other arithmetic: 0.71 us -> 1.43 us
    all_to_all x1 -> x0, blocking collectives: 19.9 us -> none  [per_device(): lax.all_to_all(wire, 'ep', split_axis=0, concat_axis=0, tiled=True)]
    all_to_all x0 -> x1, waiting for transfers between devices: none -> 9.87 us  [per_device(): lax.all_to_all(wire, 'ep', split_axis=0, concat_axis=0, tiled=True)]
    all_to_all x0 -> x1, starting transfers between devices: none -> 9.1 us  [per_device(): lax.all_to_all(wire, 'ep', split_axis=0, concat_axis=0, tiled=True)]
    pallas_call x1 -> x2, Pallas kernels: 2.45 us -> 3.2 us  [the longest x1 2.32 us: per_device(): pl.pallas_call(functools.partial(pack_kernel, slots=slots), out_shape=plt...]
    reshape x1, other arithmetic: 0.04 us -> 0.77 us  [per_device(): wire = result.astype(jnp.float16).reshape(ep_size, slots, share + LANES)]
  transfers between devices with their start and end apart: 13 -> 14, of which waited for: 5 -> 6; matrix products, arithmetic and copies ran while one was open for 0% -> 0% of each run, Pallas kernels for 11% -> 12%
where the time goes in v2:
time: 69.7 us; the launch traced here: 69.4 us
  starting transfers between devices  38.2 us (55%)
  waiting for transfers between devices  20.3 us (29%)
  Pallas kernels  9.43 us (14%)
  other arithmetic  1.43 us (2%)
    ppermute x11, starting transfers between devices, ppermute(): return lax.ppermute(array, 'tp', pairs)  13.6 us
    all_to_all x1, starting transfers between devices, per_device(): lax.all_to_all(packed.reshape(ep_size, slots, features // 2), 'ep', split...  11 us
    all_to_all x1, waiting for transfers between devices, per_device(): lax.all_to_all(wire, 'ep', split_axis=0, concat_axis=0, tiled=True)  9.87 us
    ppermute x11, waiting for transfers between devices, ppermute(): return lax.ppermute(array, 'tp', pairs)  9.49 us
    all_to_all x1, starting transfers between devices, per_device(): lax.all_to_all(wire, 'ep', split_axis=0, concat_axis=0, tiled=True)  9.1 us
    ppermute x1, starting transfers between devices, per_device(): mixed_out = kept + lax.ppermute(sent, 'tp', swap)  4.46 us
    pallas_call x1, Pallas kernels, per_device(): pl.pallas_call(functools.partial(pack_kernel, slots=slots), out_shape=plt...  2.32 us
    pallas_call x1, Pallas kernels, per_device(): pl.pallas_call(functools.partial(hidden_kernel, slots=slots), out_shape=p...  2.29 us
  transfers between devices with their start and end apart: 14, of which 6 were waited for; matrix products, arithmetic and copies ran while one was open for 0% of the time, Pallas kernels for 12%

profile of v2, /device:TPU:1, one launch (start us, length us, event | category | flops | bytes accessed | tf_op | source)
XLA Modules:
  0.0 69.4 jit_solution(16878876717506971621)
XLA Ops:
  0.0 2.1 %collective-permute-start.1 = (bf16[2,64,2048]{2,1,0:T(8,128)(2,1)}, bf16[2,64,2048]{2,1,0:T(8,128)(2,1)S(1)}, u32[]{:S(2)}, u32[]{:S(2)}) collective-permute-start(bf16[2,64,2048]{2,1,0:T(8,128)(2,1)} %bitcast.14), channel_id=1, source_target_pairs={{0,6},{1,3},{2,0},{3,5},{4,2},{5,7},{6,4},{7,1},{8,14},{9,11},{10,... | collective-permute-start | bytes 1572872 | tf_op jit(solution)/shard_map/ppermute | solution.py:249
  2.1 1.3 %collective-permute-start.2 = (bf16[2,64,2048]{2,1,0:T(8,128)(2,1)}, bf16[2,64,2048]{2,1,0:T(8,128)(2,1)S(1)}, u32[]{:S(2)}, u32[]{:S(2)}) collective-permute-start(bf16[2,64,2048]{2,1,0:T(8,128)(2,1)} %bitcast.17), channel_id=1, source_target_pairs={{0,6},{1,3},{2,0},{3,5},{4,2},{5,7},{6,4},{7,1},{8,14},{9,11},{10,... | collective-permute-start | bytes 1572872 | tf_op jit(solution)/shard_map/ppermute | solution.py:249
  3.4 2.3 %pack.1 = bf16[256,1024]{1,0:T(8,128)(2,1)} custom-call(bf16[64,2048]{1,0:T(8,128)(2,1)} %tokens.1, f32[1,2048]{1,0:T(1,128)} %bitcast.20, f32[1,2048]{1,0:T(1,128)} %bitcast.21, s32[4,64]{1,0:T(4,128)} %bitcast.22), custom_call_target="tpu_custom_call" | custom-call | tf_op jit(solution)/shard_map/pack/pallas_call | solution.py:252
  5.7 11.0 %all-to-all-start = ((bf16[32,8,1024]{2,1,0:T(8,128)(2,1)}), bf16[32,8,1024]{2,1,0:T(8,128)(2,1)S(1)}, u32[]{:S(2)}, u32[]{:S(2)}) async-start(bf16[32,8,1024]{2,1,0:T(8,128)(2,1)} %bitcast.6), calls=%async_computation | async-start | bytes 1048576 | tf_op jit(solution)/shard_map/all_to_all | solution.py:275
  16.8 1.1 %theirs.1 = bf16[2,64,2048]{2,1,0:T(8,128)(2,1)S(1)} custom-call(bf16[2,64,2048]{2,1,0:T(8,128)(2,1)} %bitcast.15, bf16[2,64,2048]{2,1,0:T(8,128)(2,1)} %bitcast.18), custom_call_target="tpu_custom_call" | custom-call | tf_op jit(solution)/shard_map/theirs/pallas_call | solution.py:279
  17.8 2.2 %collective-permute-start = (bf16[2,64,2048]{2,1,0:T(8,128)(2,1)S(1)}, bf16[2,64,2048]{2,1,0:T(8,128)(2,1)S(1)}, u32[]{:S(2)}, u32[]{:S(2)}) collective-permute-start(bf16[2,64,2048]{2,1,0:T(8,128)(2,1)S(1)} %theirs.1), channel_id=1, source_target_pairs={{0,1},{1,0},{2,3},{3,2},{4,5},{5,4},{6,7},{7,6},{8,9},{9,8},{10,11... | collective-permute-start | bytes 1572872 | tf_op jit(solution)/shard_map/ppermute | solution.py:249
  20.0 0.0 collective-permute-done.1.gate
  20.0 0.0 collective-permute-done.2.up
  20.1 0.9 %pick.1 = (bf16[2,64,2048]{2,1,0:T(8,128)(2,1)S(1)}, bf16[2,64,2048]{2,1,0:T(8,128)(2,1)}) custom-call(bf16[2,64,2048]{2,1,0:T(8,128)(2,1)S(1)} %collective-permute-done.1.gate, bf16[2,64,2048]{2,1,0:T(8,128)(2,1)S(1)} %collective-permute-done.2.up), custom_call_target="tpu_custom_call" | custom-call | tf_op jit(solution)/shard_map/pick/pallas_call | solution.py:291
  20.9 0.0 collective-permute-start.3
  21.0 1.1 %pieces.1 = (bf16[2,64,512]{2,1,0:T(8,128)(2,1)S(1)}, bf16[2,64,512]{2,1,0:T(8,128)(2,1)S(1)}, bf16[2,64,512]{2,1,0:T(8,128)(2,1)S(1)}, bf16[2,64,512]{2,1,0:T(8,128)(2,1)S(1)}) custom-call(bf16[2,64,2048]{2,1,0:T(8,128)(2,1)} %down.2), custom_call_target="tpu_custom_call" | custom-call | tf_op jit(solution)/shard_map/pieces/pallas_call | solution.py:302
  22.1 1.1 %collective-permute-start.7 = (bf16[2,64,512]{2,1,0:T(8,128)(2,1)S(1)}, bf16[2,64,512]{2,1,0:T(8,128)(2,1)S(1)}, u32[]{:S(2)}, u32[]{:S(2)}) collective-permute-start(bf16[2,64,512]{2,1,0:T(8,128)(2,1)S(1)} %get-tuple-element.20), channel_id=1, source_target_pairs={{0,2},{1,3},{2,0},{3,1},{4,6},{5,7},{6,4},{7,5},{8,10},{9,11},{10,... | collective-permute-start | bytes 393224 | tf_op jit(solution)/shard_map/ppermute | solution.py:249
  23.2 0.0 collective-permute-start.8
  23.2 2.2 %collective-permute-start.9 = (bf16[2,64,512]{2,1,0:T(8,128)(2,1)S(1)}, bf16[2,64,512]{2,1,0:T(8,128)(2,1)S(1)}, u32[]{:S(2)}, u32[]{:S(2)}) collective-permute-start(bf16[2,64,512]{2,1,0:T(8,128)(2,1)S(1)} %get-tuple-element.22), channel_id=1, source_target_pairs={{0,4},{1,5},{2,6},{3,7},{4,0},{5,1},{6,2},{7,3},{8,12},{9,13},{10,... | collective-permute-start | bytes 393224 | tf_op jit(solution)/shard_map/ppermute | solution.py:249
  25.4 1.3 %collective-permute-done.7.first = bf16[2,64,512]{2,1,0:T(8,128)(2,1)S(1)} collective-permute-done((bf16[2,64,512]{2,1,0:T(8,128)(2,1)S(1)}, bf16[2,64,512]{2,1,0:T(8,128)(2,1)S(1)}, u32[]{:S(2)}, u32[]{:S(2)}) %collective-permute-start.7) | collective-permute-done | bytes 131104 | tf_op jit(solution)/shard_map/ppermute | solution.py:249
  26.8 5.2 %collective-permute-done.8.second = bf16[2,64,512]{2,1,0:T(8,128)(2,1)S(1)} collective-permute-done((bf16[2,64,512]{2,1,0:T(8,128)(2,1)S(1)}, bf16[2,64,512]{2,1,0:T(8,128)(2,1)S(1)}, u32[]{:S(2)}, u32[]{:S(2)}) %collective-permute-start.8) | collective-permute-done | bytes 131104 | tf_op jit(solution)/shard_map/ppermute | solution.py:249
  31.9 0.0 collective-permute-done.9.third
  32.0 1.3 %collective-permute-start.10 = (bf16[4,64,512]{2,1,0:T(8,128)(2,1)S(1)}, bf16[4,64,512]{2,1,0:T(8,128)(2,1)S(1)}, u32[]{:S(2)}, u32[]{:S(2)}) collective-permute-start(bf16[4,64,512]{2,1,0:T(8,128)(2,1)S(1)} %give.1), channel_id=1, source_target_pairs={{0,1},{1,0},{2,3},{3,2},{4,5},{5,4},{6,7},{7,6},{8,9},{9,8},{10,11... | collective-permute-start | bytes 786440 | tf_op jit(solution)/shard_map/ppermute | solution.py:249
  33.2 0.0 collective-permute-done.swapped
  33.2 0.0 all-to-all-done
  33.2 0.0 collective-permute-done.3.passed
  33.2 2.3 %hidden.1.h_own = bf16[128,256]{1,0:T(8,128)(2,1)S(1)} custom-call(bf16[2,64,2048]{2,1,0:T(8,128)(2,1)} %bitcast.16, bf16[2,64,2048]{2,1,0:T(8,128)(2,1)} %bitcast.19, bf16[256,1024]{1,0:T(8,128)(2,1)S(1)} %bitcast.13, bf16[2,64,2048]{2,1,0:T(8,128)(2,1)S(1)} %collective-permute-done.swapped, bf16[2,64,2048]{2,1,0:T(8,128)(2,1)S(1)} %get-tuple-element.17.kept_in, ...), custom_call_target="tpu_custom_call" | custom-call | tf_op jit(solution)/shard_map/hidden/pallas_call | solution.py:323
  35.5 0.1 collective-permute-start.4
  35.6 1.6 %collective-permute-start.5 = (bf16[128,256]{1,0:T(8,128)(2,1)S(1)}, bf16[128,256]{1,0:T(8,128)(2,1)S(1)}, u32[]{:S(2)}, u32[]{:S(2)}) collective-permute-start(bf16[128,256]{1,0:T(8,128)(2,1)S(1)} %hidden.1.h_own), channel_id=1, source_target_pairs={{0,6},{1,7},{2,4},{3,5},{4,2},{5,3},{6,0},{7,1},{8,14},{9,15},{10,... | collective-permute-start | bytes 196616 | tf_op jit(solution)/shard_map/ppermute | solution.py:249
  37.2 1.6 %collective-permute-start.6 = (bf16[128,256]{1,0:T(8,128)(2,1)S(1)}, bf16[128,256]{1,0:T(8,128)(2,1)S(1)}, u32[]{:S(2)}, u32[]{:S(2)}) collective-permute-start(bf16[128,256]{1,0:T(8,128)(2,1)S(1)} %hidden.1.h_own), channel_id=1, source_target_pairs={{0,4},{1,5},{2,6},{3,7},{4,0},{5,1},{6,2},{7,3},{8,12},{9,13},{10,... | collective-permute-start | bytes 196616 | tf_op jit(solution)/shard_map/ppermute | solution.py:249
  38.9 0.0 collective-permute-done.10.other
  38.9 0.0 collective-permute-done.4.h_first
  38.9 1.2 %collective-permute-done.5.h_second = bf16[128,256]{1,0:T(8,128)(2,1)S(1)} collective-permute-done((bf16[128,256]{1,0:T(8,128)(2,1)S(1)}, bf16[128,256]{1,0:T(8,128)(2,1)S(1)}, u32[]{:S(2)}, u32[]{:S(2)}) %collective-permute-start.5) | collective-permute-done | bytes 65568 | tf_op jit(solution)/shard_map/ppermute | solution.py:249
  40.0 1.8 %collective-permute-done.6.h_third = bf16[128,256]{1,0:T(8,128)(2,1)S(1)} collective-permute-done((bf16[128,256]{1,0:T(8,128)(2,1)S(1)}, bf16[128,256]{1,0:T(8,128)(2,1)S(1)}, u32[]{:S(2)}, u32[]{:S(2)}) %collective-permute-start.6) | collective-permute-done | bytes 65568 | tf_op jit(solution)/shard_map/ppermute | solution.py:249
  41.8 0.5 down.3
  42.4 0.8 %convert_bitcast_fusion = f16[32,8,640]{2,1,0:T(8,128)(2,1)} fusion(f32[256,640]{1,0:T(8,128)S(1)} %down.3), kind=kLoop, calls=%fused_computation.1 | loop fusion | flops 163840 | bytes 983040 | tf_op jit(solution)/shard_map/reshape | solution.py:344
  43.2 9.1 %all-to-all-start.1 = ((f16[32,8,640]{2,1,0:T(8,128)(2,1)}), f16[32,8,640]{2,1,0:T(8,128)(2,1)S(1)}, u32[]{:S(2)}, u32[]{:S(2)}) async-start(f16[32,8,640]{2,1,0:T(8,128)(2,1)} %convert_bitcast_fusion), calls=%async_computation.1 | async-start | bytes 655360 | tf_op jit(solution)/shard_map/all_to_all | solution.py:345
  52.3 0.9 %factors.1 = (bf16[256,64]{1,0:T(8,128)(2,1)S(1)}, bf16[256,64]{1,0:T(8,128)(2,1)S(1)}) custom-call(s32[4,64]{1,0:T(4,128)} %bitcast.23, f32[4,64]{1,0:T(4,128)} %bitcast.24), custom_call_target="tpu_custom_call" | custom-call | tf_op jit(solution)/shard_map/factors/pallas_call | solution.py:265
  53.1 9.9 %all-to-all-done.1 = f16[32,8,640]{2,1,0:T(8,128)(2,1)S(1)} async-done(((f16[32,8,640]{2,1,0:T(8,128)(2,1)}), f16[32,8,640]{2,1,0:T(8,128)(2,1)S(1)}, u32[]{:S(2)}, u32[]{:S(2)}) %all-to-all-start.1) | async-done | bytes 327712 | tf_op jit(solution)/shard_map/all_to_all | solution.py:345
  63.1 0.3 combine.1
  63.4 4.5 %collective-permute-start.11 = (f32[64,256]{1,0:T(8,128)S(1)}, f32[64,256]{1,0:T(8,128)S(1)}, u32[]{:S(2)}, u32[]{:S(2)}) collective-permute-start(f32[64,256]{1,0:T(8,128)S(1)} %get-tuple-element.24), channel_id=1, source_target_pairs={{0,1},{1,0},{2,3},{3,2},{4,5},{5,4},{6,7},{7,6},{8,9},{9,8},{10,11... | collective-permute-start | bytes 196616 | tf_op jit(solution)/shard_map/ppermute | solution.py:356
  67.9 0.9 %collective-permute-done.11 = f32[64,256]{1,0:T(8,128)S(1)} collective-permute-done((f32[64,256]{1,0:T(8,128)S(1)}, f32[64,256]{1,0:T(8,128)S(1)}, u32[]{:S(2)}, u32[]{:S(2)}) %collective-permute-start.11) | collective-permute-done | bytes 65568 | tf_op jit(solution)/shard_map/ppermute | solution.py:356
  68.8 0.6 add_convert_fusion
  (2 shorter events, 0.1 us)
Async XLA Ops:
  0.0 20.0 %collective-permute-start.1 = (bf16[2,64,2048]{2,1,0:T(8,128)(2,1)}, bf16[2,64,2048]{2,1,0:T(8,128)(2,1)S(1)}, u32[]{:S(2)}, u32[]{:S(2)}) collective-permute-start(bf16[2,64,2048]{2,1,0:T(8,128)(2,1)} %bitcast.14), channel_id=1, source_target_pairs={{0,6},{1,3},{2,0},{3,5},{4,2},{5,7},{6,4},{7,1},{8,14},{9,11},{10,... | collective-permute-start | bytes 1572872 | tf_op jit(solution)/shard_map/ppermute | solution.py:249
  2.1 17.9 %collective-permute-start.2 = (bf16[2,64,2048]{2,1,0:T(8,128)(2,1)}, bf16[2,64,2048]{2,1,0:T(8,128)(2,1)S(1)}, u32[]{:S(2)}, u32[]{:S(2)}) collective-permute-start(bf16[2,64,2048]{2,1,0:T(8,128)(2,1)} %bitcast.17), channel_id=1, source_target_pairs={{0,6},{1,3},{2,0},{3,5},{4,2},{5,7},{6,4},{7,1},{8,14},{9,11},{10,... | collective-permute-start | bytes 1572872 | tf_op jit(solution)/shard_map/ppermute | solution.py:249
  5.7 27.5 %all-to-all-start = ((bf16[32,8,1024]{2,1,0:T(8,128)(2,1)}), bf16[32,8,1024]{2,1,0:T(8,128)(2,1)S(1)}, u32[]{:S(2)}, u32[]{:S(2)}) async-start(bf16[32,8,1024]{2,1,0:T(8,128)(2,1)} %bitcast.6), calls=%async_computation | async-start | bytes 1048576 | tf_op jit(solution)/shard_map/all_to_all | solution.py:275
  17.8 15.4 %collective-permute-start = (bf16[2,64,2048]{2,1,0:T(8,128)(2,1)S(1)}, bf16[2,64,2048]{2,1,0:T(8,128)(2,1)S(1)}, u32[]{:S(2)}, u32[]{:S(2)}) collective-permute-start(bf16[2,64,2048]{2,1,0:T(8,128)(2,1)S(1)} %theirs.1), channel_id=1, source_target_pairs={{0,1},{1,0},{2,3},{3,2},{4,5},{5,4},{6,7},{7,6},{8,9},{9,8},{10,11... | collective-permute-start | bytes 1572872 | tf_op jit(solution)/shard_map/ppermute | solution.py:249
  20.9 12.3 %collective-permute-start.3 = (bf16[2,64,2048]{2,1,0:T(8,128)(2,1)}, bf16[2,64,2048]{2,1,0:T(8,128)(2,1)S(1)}, u32[]{:S(2)}, u32[]{:S(2)}) collective-permute-start(bf16[2,64,2048]{2,1,0:T(8,128)(2,1)} %get-tuple-element.18), channel_id=1, source_target_pairs={{0,1},{1,0},{2,3},{3,2},{4,5},{5,4},{6,7},{7,6},{8,9},{9,8},{10,11... | collective-permute-start | bytes 1572872 | tf_op jit(solution)/shard_map/ppermute | solution.py:249
  22.1 4.7 %collective-permute-start.7 = (bf16[2,64,512]{2,1,0:T(8,128)(2,1)S(1)}, bf16[2,64,512]{2,1,0:T(8,128)(2,1)S(1)}, u32[]{:S(2)}, u32[]{:S(2)}) collective-permute-start(bf16[2,64,512]{2,1,0:T(8,128)(2,1)S(1)} %get-tuple-element.20), channel_id=1, source_target_pairs={{0,2},{1,3},{2,0},{3,1},{4,6},{5,7},{6,4},{7,5},{8,10},{9,11},{10,... | collective-permute-start | bytes 393224 | tf_op jit(solution)/shard_map/ppermute | solution.py:249
  23.2 8.8 %collective-permute-start.8 = (bf16[2,64,512]{2,1,0:T(8,128)(2,1)S(1)}, bf16[2,64,512]{2,1,0:T(8,128)(2,1)S(1)}, u32[]{:S(2)}, u32[]{:S(2)}) collective-permute-start(bf16[2,64,512]{2,1,0:T(8,128)(2,1)S(1)} %get-tuple-element.21), channel_id=1, source_target_pairs={{0,6},{1,7},{2,4},{3,5},{4,2},{5,3},{6,0},{7,1},{8,14},{9,15},{10,... | collective-permute-start | bytes 393224 | tf_op jit(solution)/shard_map/ppermute | solution.py:249
  23.2 8.8 %collective-permute-start.9 = (bf16[2,64,512]{2,1,0:T(8,128)(2,1)S(1)}, bf16[2,64,512]{2,1,0:T(8,128)(2,1)S(1)}, u32[]{:S(2)}, u32[]{:S(2)}) collective-permute-start(bf16[2,64,512]{2,1,0:T(8,128)(2,1)S(1)} %get-tuple-element.22), channel_id=1, source_target_pairs={{0,4},{1,5},{2,6},{3,7},{4,0},{5,1},{6,2},{7,3},{8,12},{9,13},{10,... | collective-permute-start | bytes 393224 | tf_op jit(solution)/shard_map/ppermute | solution.py:249
  32.0 6.9 %collective-permute-start.10 = (bf16[4,64,512]{2,1,0:T(8,128)(2,1)S(1)}, bf16[4,64,512]{2,1,0:T(8,128)(2,1)S(1)}, u32[]{:S(2)}, u32[]{:S(2)}) collective-permute-start(bf16[4,64,512]{2,1,0:T(8,128)(2,1)S(1)} %give.1), channel_id=1, source_target_pairs={{0,1},{1,0},{2,3},{3,2},{4,5},{5,4},{6,7},{7,6},{8,9},{9,8},{10,11... | collective-permute-start | bytes 786440 | tf_op jit(solution)/shard_map/ppermute | solution.py:249
  35.5 3.3 %collective-permute-start.4 = (bf16[128,256]{1,0:T(8,128)(2,1)S(1)}, bf16[128,256]{1,0:T(8,128)(2,1)S(1)}, u32[]{:S(2)}, u32[]{:S(2)}) collective-permute-start(bf16[128,256]{1,0:T(8,128)(2,1)S(1)} %hidden.1.h_own), channel_id=1, source_target_pairs={{0,2},{1,3},{2,0},{3,1},{4,6},{5,7},{6,4},{7,5},{8,10},{9,11},{10,... | collective-permute-start | bytes 196616 | tf_op jit(solution)/shard_map/ppermute | solution.py:249
  35.6 4.4 %collective-permute-start.5 = (bf16[128,256]{1,0:T(8,128)(2,1)S(1)}, bf16[128,256]{1,0:T(8,128)(2,1)S(1)}, u32[]{:S(2)}, u32[]{:S(2)}) collective-permute-start(bf16[128,256]{1,0:T(8,128)(2,1)S(1)} %hidden.1.h_own), channel_id=1, source_target_pairs={{0,6},{1,7},{2,4},{3,5},{4,2},{5,3},{6,0},{7,1},{8,14},{9,15},{10,... | collective-permute-start | bytes 196616 | tf_op jit(solution)/shard_map/ppermute | solution.py:249
  37.2 4.6 %collective-permute-start.6 = (bf16[128,256]{1,0:T(8,128)(2,1)S(1)}, bf16[128,256]{1,0:T(8,128)(2,1)S(1)}, u32[]{:S(2)}, u32[]{:S(2)}) collective-permute-start(bf16[128,256]{1,0:T(8,128)(2,1)S(1)} %hidden.1.h_own), channel_id=1, source_target_pairs={{0,4},{1,5},{2,6},{3,7},{4,0},{5,1},{6,2},{7,3},{8,12},{9,13},{10,... | collective-permute-start | bytes 196616 | tf_op jit(solution)/shard_map/ppermute | solution.py:249
  43.2 19.9 %all-to-all-start.1 = ((f16[32,8,640]{2,1,0:T(8,128)(2,1)}), f16[32,8,640]{2,1,0:T(8,128)(2,1)S(1)}, u32[]{:S(2)}, u32[]{:S(2)}) async-start(f16[32,8,640]{2,1,0:T(8,128)(2,1)} %convert_bitcast_fusion), calls=%async_computation.1 | async-start | bytes 655360 | tf_op jit(solution)/shard_map/all_to_all | solution.py:345
  63.4 5.4 %collective-permute-start.11 = (f32[64,256]{1,0:T(8,128)S(1)}, f32[64,256]{1,0:T(8,128)S(1)}, u32[]{:S(2)}, u32[]{:S(2)}) collective-permute-start(f32[64,256]{1,0:T(8,128)S(1)} %get-tuple-element.24), channel_id=1, source_target_pairs={{0,1},{1,0},{2,3},{3,2},{4,5},{5,4},{6,7},{7,6},{8,9},{9,8},{10,11... | collective-permute-start | bytes 196616 | tf_op jit(solution)/shard_map/ppermute | solution.py:356

commit v3 on v2

--- a/solution.py
+++ b/solution.py
@@ -55,9 +55,11 @@
     return copies
 
 
-def theirs_kernel(gate, up, out, sems):
-    _, core = position()
-    for copy in copy_all([(ref.at[1 - core], out.at[i]) for i, ref in enumerate((gate, up))], sems):
+def theirs_kernel(gate, up, giving, mine, sems):
+    _, core = position()
+    pairs = [(ref.at[1 - core], giving.at[i]) for i, ref in enumerate((gate, up))]
+    pairs += [(ref.at[core], mine.at[i]) for i, ref in enumerate((gate, up))]
+    for copy in copy_all(pairs, sems):
         copy.wait()
 
 
@@ -136,9 +138,7 @@
     return lax.bitwise_xor(y, 1), 3 - y, lax.bitwise_xor(y, 2)
 
 
-def hidden_kernel(own_gate, own_up, arrived, swapped, kept_in, passed, hidden, local, sems, *, slots):
-    _, core = position()
-    copies = copy_all([(ref.at[core], local.at[i]) for i, ref in enumerate((own_gate, own_up))], sems)
+def hidden_kernel(arrived, mine, swapped, kept_in, passed, hidden, *, slots):
     rows, width = arrived.shape
     kept = rows // 2
     count = slots // 2
@@ -149,23 +149,15 @@
     for q in range(2):
         pick = jnp.where(j == source + q * count, 1.0, 0.0).astype(jnp.bfloat16)
         xs.append(dot_nn(pick, values).astype(jnp.bfloat16))
-
-    def products(*refs):
-        total = None
-        for q, x in enumerate(xs):
-            at = slice(q * width, (q + 1) * width)
-            w = jnp.concatenate([ref[m, :, at] for m in range(2) for ref in refs])
-            product = dot_nt(x, w)
-            total = product if total is None else total + product
-        units = total.shape[1] // 2
-        return total[:, :units], total[:, units:]
-
-    others = products(swapped, kept_in, passed)
-    for copy in copies:
-        copy.wait()
-    own = products(local)
-    value, upward = (jnp.concatenate(parts, axis=1) for parts in zip(own, others))
-    result = value / (1.0 + jnp.exp(-value)) * upward
+    total = None
+    for q, x in enumerate(xs):
+        at = slice(q * width, (q + 1) * width)
+        refs = (mine, swapped, kept_in, passed)
+        product = dot_nt(x, jnp.concatenate([ref[m, :, at] for m in range(2) for ref in refs]))
+        total = product if total is None else total + product
+    units = total.shape[1] // 2
+    value = total[:, :units]
+    result = value / (1.0 + jnp.exp(-value)) * total[:, units:]
     hidden[...] = result.astype(jnp.bfloat16)
 
 
@@ -276,18 +268,18 @@
         packed.reshape(ep_size, slots, features // 2), "ep", split_axis=0, concat_axis=0, tiled=True
     ).reshape(rows, features // 2)
 
-    giving = pl.pallas_call(
+    pair = pltpu.VMEM((2, units, features), jnp.bfloat16)
+    giving, mine = pl.pallas_call(
         theirs_kernel,
-        out_shape=pltpu.VMEM((2, units, features), jnp.bfloat16),
+        out_shape=(pair, pair),
         in_specs=[anywhere] * 2,
-        out_specs=VMEM,
-        scratch_shapes=[pltpu.SemaphoreType.DMA((2,))],
+        out_specs=(VMEM, VMEM),
+        scratch_shapes=[pltpu.SemaphoreType.DMA((4,))],
         compiler_params=PARAMS,
         name="theirs",
     )(gate_t, up_t)
     swapped = ppermute(giving, swap)
 
-    pair = pltpu.VMEM((2, units, features), jnp.bfloat16)
     kept, picked = pl.pallas_call(
         pick_kernel,
         out_shape=(pair, pair),
@@ -323,15 +315,11 @@
     hidden = pl.pallas_call(
         functools.partial(hidden_kernel, slots=slots),
         out_shape=pltpu.VMEM((rows // 2, 2 * CORES * units), jnp.bfloat16),
-        in_specs=[anywhere] * 2 + [VMEM] * 4,
+        in_specs=[VMEM] * 5,
         out_specs=VMEM,
-        scratch_shapes=[
-            pltpu.VMEM((2, units, features), jnp.bfloat16),
-            pltpu.SemaphoreType.DMA((2,)),
-        ],
         compiler_params=PARAMS,
         name="hidden",
-    )(gate_t, up_t, *on_chip(arrived, swapped, kept, passed))
+    )(*on_chip(arrived, mine, swapped, kept, passed))
     hiddens = [hidden] + [ppermute(hidden, pairs) for pairs in (near, same, across)]
     result = pl.pallas_call(
         functools.partial(down_kernel, slots=slots),

time: 69.7 us -> 69.6 us (level)
    pallas_call x1, Pallas kernels: 2.29 us -> 1.02 us  [per_device(): pl.pallas_call(functools.partial(hidden_kernel, slots=slots), out_shape=p...]
    pallas_call x1, Pallas kernels: 0.53 us -> 1.48 us  [per_device(): pl.pallas_call(functools.partial(down_kernel, slots=slots), out_shape=plt...]
  transfers between devices with their start and end apart: 14 -> 14, of which waited for: 6 -> 6; matrix products, arithmetic and copies ran while one was open for 0% -> 0% of each run, Pallas kernels for 12% -> 11%
where the time goes in v3:
time: 69.6 us; the launch traced here: 69.2 us
  starting transfers between devices  37.8 us (54%)
  waiting for transfers between devices  20.6 us (30%)
  Pallas kernels  9.28 us (13%)
  other arithmetic  1.44 us (2%)
    ppermute x11, starting transfers between devices, ppermute(): return lax.ppermute(array, 'tp', pairs)  13.4 us
    all_to_all x1, starting transfers between devices, per_device(): lax.all_to_all(packed.reshape(ep_size, slots, features // 2), 'ep', split...  11 us
    all_to_all x1, waiting for transfers between devices, per_device(): lax.all_to_all(wire, 'ep', split_axis=0, concat_axis=0, tiled=True)  10.2 us
    ppermute x11, waiting for transfers between devices, ppermute(): return lax.ppermute(array, 'tp', pairs)  9.49 us
    all_to_all x1, starting transfers between devices, per_device(): lax.all_to_all(wire, 'ep', split_axis=0, concat_axis=0, tiled=True)  9.15 us
    ppermute x1, starting transfers between devices, per_device(): mixed_out = kept + lax.ppermute(sent, 'tp', swap)  4.23 us
    pallas_call x1, Pallas kernels, per_device(): pl.pallas_call(functools.partial(pack_kernel, slots=slots), out_shape=plt...  2.31 us
    pallas_call x1, Pallas kernels, per_device(): pl.pallas_call(functools.partial(down_kernel, slots=slots), out_shape=plt...  1.48 us
  transfers between devices with their start and end apart: 14, of which 6 were waited for; matrix products, arithmetic and copies ran while one was open for 0% of the time, Pallas kernels for 11%

profile of v3, /device:TPU:1, one launch (start us, length us, event | category | flops | bytes accessed | tf_op | source)
XLA Modules:
  0.0 69.2 jit_solution(15698437222627491131)
XLA Ops:
  0.0 2.1 %collective-permute-start.1 = (bf16[2,64,2048]{2,1,0:T(8,128)(2,1)}, bf16[2,64,2048]{2,1,0:T(8,128)(2,1)S(1)}, u32[]{:S(2)}, u32[]{:S(2)}) collective-permute-start(bf16[2,64,2048]{2,1,0:T(8,128)(2,1)} %bitcast.14), channel_id=1, source_target_pairs={{0,6},{1,3},{2,0},{3,5},{4,2},{5,7},{6,4},{7,1},{8,14},{9,11},{10,... | collective-permute-start | bytes 1572872 | tf_op jit(solution)/shard_map/ppermute | solution.py:241
  2.1 1.3 %collective-permute-start.2 = (bf16[2,64,2048]{2,1,0:T(8,128)(2,1)}, bf16[2,64,2048]{2,1,0:T(8,128)(2,1)S(1)}, u32[]{:S(2)}, u32[]{:S(2)}) collective-permute-start(bf16[2,64,2048]{2,1,0:T(8,128)(2,1)} %bitcast.16), channel_id=1, source_target_pairs={{0,6},{1,3},{2,0},{3,5},{4,2},{5,7},{6,4},{7,1},{8,14},{9,11},{10,... | collective-permute-start | bytes 1572872 | tf_op jit(solution)/shard_map/ppermute | solution.py:241
  3.4 2.3 %pack.1 = bf16[256,1024]{1,0:T(8,128)(2,1)} custom-call(bf16[64,2048]{1,0:T(8,128)(2,1)} %tokens.1, f32[1,2048]{1,0:T(1,128)} %bitcast.18, f32[1,2048]{1,0:T(1,128)} %bitcast.19, s32[4,64]{1,0:T(4,128)} %bitcast.20), custom_call_target="tpu_custom_call" | custom-call | tf_op jit(solution)/shard_map/pack/pallas_call | solution.py:244
  5.7 11.0 %all-to-all-start = ((bf16[32,8,1024]{2,1,0:T(8,128)(2,1)}), bf16[32,8,1024]{2,1,0:T(8,128)(2,1)S(1)}, u32[]{:S(2)}, u32[]{:S(2)}) async-start(bf16[32,8,1024]{2,1,0:T(8,128)(2,1)} %bitcast.4), calls=%async_computation | async-start | bytes 1048576 | tf_op jit(solution)/shard_map/all_to_all | solution.py:267
  16.8 1.2 %theirs.1 = (bf16[2,64,2048]{2,1,0:T(8,128)(2,1)S(1)}, bf16[2,64,2048]{2,1,0:T(8,128)(2,1)S(1)}) custom-call(bf16[2,64,2048]{2,1,0:T(8,128)(2,1)} %bitcast.15, bf16[2,64,2048]{2,1,0:T(8,128)(2,1)} %bitcast.17), custom_call_target="tpu_custom_call" | custom-call | tf_op jit(solution)/shard_map/theirs/pallas_call | solution.py:272
  18.0 2.2 %collective-permute-start = (bf16[2,64,2048]{2,1,0:T(8,128)(2,1)S(1)}, bf16[2,64,2048]{2,1,0:T(8,128)(2,1)S(1)}, u32[]{:S(2)}, u32[]{:S(2)}) collective-permute-start(bf16[2,64,2048]{2,1,0:T(8,128)(2,1)S(1)} %get-tuple-element.20), channel_id=1, source_target_pairs={{0,1},{1,0},{2,3},{3,2},{4,5},{5,4},{6,7},{7,6},{8,9},{9,8},{10,11... | collective-permute-start | bytes 1572872 | tf_op jit(solution)/shard_map/ppermute | solution.py:241
  20.2 0.0 collective-permute-done.1.gate
  20.2 0.0 collective-permute-done.2.up
  20.2 0.9 %pick.1 = (bf16[2,64,2048]{2,1,0:T(8,128)(2,1)S(1)}, bf16[2,64,2048]{2,1,0:T(8,128)(2,1)}) custom-call(bf16[2,64,2048]{2,1,0:T(8,128)(2,1)S(1)} %collective-permute-done.1.gate, bf16[2,64,2048]{2,1,0:T(8,128)(2,1)S(1)} %collective-permute-done.2.up), custom_call_target="tpu_custom_call" | custom-call | tf_op jit(solution)/shard_map/pick/pallas_call | solution.py:283
  21.1 0.0 collective-permute-start.3
  21.1 1.1 %pieces.1 = (bf16[2,64,512]{2,1,0:T(8,128)(2,1)S(1)}, bf16[2,64,512]{2,1,0:T(8,128)(2,1)S(1)}, bf16[2,64,512]{2,1,0:T(8,128)(2,1)S(1)}, bf16[2,64,512]{2,1,0:T(8,128)(2,1)S(1)}) custom-call(bf16[2,64,2048]{2,1,0:T(8,128)(2,1)} %down.2), custom_call_target="tpu_custom_call" | custom-call | tf_op jit(solution)/shard_map/pieces/pallas_call | solution.py:294
  22.3 1.1 %collective-permute-start.7 = (bf16[2,64,512]{2,1,0:T(8,128)(2,1)S(1)}, bf16[2,64,512]{2,1,0:T(8,128)(2,1)S(1)}, u32[]{:S(2)}, u32[]{:S(2)}) collective-permute-start(bf16[2,64,512]{2,1,0:T(8,128)(2,1)S(1)} %get-tuple-element.24), channel_id=1, source_target_pairs={{0,2},{1,3},{2,0},{3,1},{4,6},{5,7},{6,4},{7,5},{8,10},{9,11},{10,... | collective-permute-start | bytes 393224 | tf_op jit(solution)/shard_map/ppermute | solution.py:241
  23.3 0.0 collective-permute-start.8
  23.4 2.2 %collective-permute-start.9 = (bf16[2,64,512]{2,1,0:T(8,128)(2,1)S(1)}, bf16[2,64,512]{2,1,0:T(8,128)(2,1)S(1)}, u32[]{:S(2)}, u32[]{:S(2)}) collective-permute-start(bf16[2,64,512]{2,1,0:T(8,128)(2,1)S(1)} %get-tuple-element.26), channel_id=1, source_target_pairs={{0,4},{1,5},{2,6},{3,7},{4,0},{5,1},{6,2},{7,3},{8,12},{9,13},{10,... | collective-permute-start | bytes 393224 | tf_op jit(solution)/shard_map/ppermute | solution.py:241
  25.6 1.3 %collective-permute-done.7.first = bf16[2,64,512]{2,1,0:T(8,128)(2,1)S(1)} collective-permute-done((bf16[2,64,512]{2,1,0:T(8,128)(2,1)S(1)}, bf16[2,64,512]{2,1,0:T(8,128)(2,1)S(1)}, u32[]{:S(2)}, u32[]{:S(2)}) %collective-permute-start.7) | collective-permute-done | bytes 131104 | tf_op jit(solution)/shard_map/ppermute | solution.py:241
  26.9 5.4 %collective-permute-done.8.second = bf16[2,64,512]{2,1,0:T(8,128)(2,1)S(1)} collective-permute-done((bf16[2,64,512]{2,1,0:T(8,128)(2,1)S(1)}, bf16[2,64,512]{2,1,0:T(8,128)(2,1)S(1)}, u32[]{:S(2)}, u32[]{:S(2)}) %collective-permute-start.8) | collective-permute-done | bytes 131104 | tf_op jit(solution)/shard_map/ppermute | solution.py:241
  32.3 0.0 collective-permute-done.9.third
  32.3 1.1 %collective-permute-start.10 = (bf16[4,64,512]{2,1,0:T(8,128)(2,1)S(1)}, bf16[4,64,512]{2,1,0:T(8,128)(2,1)}, u32[]{:S(2)}, u32[]{:S(2)}) collective-permute-start(bf16[4,64,512]{2,1,0:T(8,128)(2,1)S(1)} %give.1), channel_id=1, source_target_pairs={{0,1},{1,0},{2,3},{3,2},{4,5},{5,4},{6,7},{7,6},{8,9},{9,8},{10,11... | collective-permute-start | bytes 786440 | tf_op jit(solution)/shard_map/ppermute | solution.py:241
  33.4 0.0 collective-permute-done.swapped
  33.4 0.0 all-to-all-done
  33.4 0.0 collective-permute-done.3.passed
  33.4 1.0 %hidden.1.h_own = bf16[128,256]{1,0:T(8,128)(2,1)S(1)} custom-call(bf16[256,1024]{1,0:T(8,128)(2,1)S(1)} %bitcast.13, bf16[2,64,2048]{2,1,0:T(8,128)(2,1)S(1)} %get-tuple-element.19.mine, bf16[2,64,2048]{2,1,0:T(8,128)(2,1)S(1)} %collective-permute-done.swapped, bf16[2,64,2048]{2,1,0:T(8,128)(2,1)S(1)} %get-tuple-element.21.kept_in, ...), custom_call_target="tpu_custom_call" | custom-call | tf_op jit(solution)/shard_map/hidden/pallas_call | solution.py:315
  34.4 0.1 collective-permute-start.4
  34.5 1.4 %collective-permute-start.5 = (bf16[128,256]{1,0:T(8,128)(2,1)S(1)}, bf16[128,256]{1,0:T(8,128)(2,1)S(1)}, u32[]{:S(2)}, u32[]{:S(2)}) collective-permute-start(bf16[128,256]{1,0:T(8,128)(2,1)S(1)} %hidden.1.h_own), channel_id=1, source_target_pairs={{0,6},{1,7},{2,4},{3,5},{4,2},{5,3},{6,0},{7,1},{8,14},{9,15},{10,... | collective-permute-start | bytes 196616 | tf_op jit(solution)/shard_map/ppermute | solution.py:241
  36.0 1.8 %collective-permute-start.6 = (bf16[128,256]{1,0:T(8,128)(2,1)S(1)}, bf16[128,256]{1,0:T(8,128)(2,1)S(1)}, u32[]{:S(2)}, u32[]{:S(2)}) collective-permute-start(bf16[128,256]{1,0:T(8,128)(2,1)S(1)} %hidden.1.h_own), channel_id=1, source_target_pairs={{0,4},{1,5},{2,6},{3,7},{4,0},{5,1},{6,2},{7,3},{8,12},{9,13},{10,... | collective-permute-start | bytes 196616 | tf_op jit(solution)/shard_map/ppermute | solution.py:241
  37.8 0.0 collective-permute-done.10.other
  37.8 0.0 collective-permute-done.4.h_first
  37.8 1.2 %collective-permute-done.5.h_second = bf16[128,256]{1,0:T(8,128)(2,1)S(1)} collective-permute-done((bf16[128,256]{1,0:T(8,128)(2,1)S(1)}, bf16[128,256]{1,0:T(8,128)(2,1)S(1)}, u32[]{:S(2)}, u32[]{:S(2)}) %collective-permute-start.5) | collective-permute-done | bytes 65568 | tf_op jit(solution)/shard_map/ppermute | solution.py:241
  38.9 1.6 %collective-permute-done.6.h_third = bf16[128,256]{1,0:T(8,128)(2,1)S(1)} collective-permute-done((bf16[128,256]{1,0:T(8,128)(2,1)S(1)}, bf16[128,256]{1,0:T(8,128)(2,1)S(1)}, u32[]{:S(2)}, u32[]{:S(2)}) %collective-permute-start.6) | collective-permute-done | bytes 65568 | tf_op jit(solution)/shard_map/ppermute | solution.py:241
  40.6 1.5 %down.3 = f32[256,640]{1,0:T(8,128)S(1)} custom-call(bf16[128,256]{1,0:T(8,128)(2,1)S(1)} %hidden.1.h_own, bf16[128,256]{1,0:T(8,128)(2,1)S(1)} %collective-permute-done.4.h_first, bf16[128,256]{1,0:T(8,128)(2,1)S(1)} %collective-permute-done.5.h_second, bf16[128,256]{1,0:T(8,128)(2,1)S(1)} %collective-permute-done.6.h_third, ...), custom_call_target="tpu_custom_call" | custom-call | tf_op jit(solution)/shard_map/down/pallas_call | solution.py:324
  42.1 0.8 %convert_bitcast_fusion = f16[32,8,640]{2,1,0:T(8,128)(2,1)} fusion(f32[256,640]{1,0:T(8,128)S(1)} %down.3), kind=kLoop, calls=%fused_computation.1 | loop fusion | flops 163840 | bytes 983040 | tf_op jit(solution)/shard_map/reshape | solution.py:332
  42.8 9.2 %all-to-all-start.1 = ((f16[32,8,640]{2,1,0:T(8,128)(2,1)}), f16[32,8,640]{2,1,0:T(8,128)(2,1)S(1)}, u32[]{:S(2)}, u32[]{:S(2)}) async-start(f16[32,8,640]{2,1,0:T(8,128)(2,1)} %convert_bitcast_fusion), calls=%async_computation.1 | async-start | bytes 655360 | tf_op jit(solution)/shard_map/all_to_all | solution.py:333
  52.0 0.9 %factors.1 = (bf16[256,64]{1,0:T(8,128)(2,1)S(1)}, bf16[256,64]{1,0:T(8,128)(2,1)S(1)}) custom-call(s32[4,64]{1,0:T(4,128)} %bitcast.21, f32[4,64]{1,0:T(4,128)} %bitcast.22), custom_call_target="tpu_custom_call" | custom-call | tf_op jit(solution)/shard_map/factors/pallas_call | solution.py:257
  52.9 10.2 %all-to-all-done.1 = f16[32,8,640]{2,1,0:T(8,128)(2,1)S(1)} async-done(((f16[32,8,640]{2,1,0:T(8,128)(2,1)}), f16[32,8,640]{2,1,0:T(8,128)(2,1)S(1)}, u32[]{:S(2)}, u32[]{:S(2)}) %all-to-all-start.1) | async-done | bytes 327712 | tf_op jit(solution)/shard_map/all_to_all | solution.py:333
  63.1 0.3 combine.1
  63.5 4.2 %collective-permute-start.11 = (f32[64,256]{1,0:T(8,128)S(1)}, f32[64,256]{1,0:T(8,128)S(1)}, u32[]{:S(2)}, u32[]{:S(2)}) collective-permute-start(f32[64,256]{1,0:T(8,128)S(1)} %get-tuple-element.28), channel_id=1, source_target_pairs={{0,1},{1,0},{2,3},{3,2},{4,5},{5,4},{6,7},{7,6},{8,9},{9,8},{10,11... | collective-permute-start | bytes 196616 | tf_op jit(solution)/shard_map/ppermute | solution.py:344
  67.7 0.9 %collective-permute-done.11 = f32[64,256]{1,0:T(8,128)S(1)} collective-permute-done((f32[64,256]{1,0:T(8,128)S(1)}, f32[64,256]{1,0:T(8,128)S(1)}, u32[]{:S(2)}, u32[]{:S(2)}) %collective-permute-start.11) | collective-permute-done | bytes 65568 | tf_op jit(solution)/shard_map/ppermute | solution.py:344
  68.6 0.6 add_convert_fusion
  (2 shorter events, 0.1 us)
Async XLA Ops:
  0.0 20.2 %collective-permute-start.1 = (bf16[2,64,2048]{2,1,0:T(8,128)(2,1)}, bf16[2,64,2048]{2,1,0:T(8,128)(2,1)S(1)}, u32[]{:S(2)}, u32[]{:S(2)}) collective-permute-start(bf16[2,64,2048]{2,1,0:T(8,128)(2,1)} %bitcast.14), channel_id=1, source_target_pairs={{0,6},{1,3},{2,0},{3,5},{4,2},{5,7},{6,4},{7,1},{8,14},{9,11},{10,... | collective-permute-start | bytes 1572872 | tf_op jit(solution)/shard_map/ppermute | solution.py:241
  2.1 18.1 %collective-permute-start.2 = (bf16[2,64,2048]{2,1,0:T(8,128)(2,1)}, bf16[2,64,2048]{2,1,0:T(8,128)(2,1)S(1)}, u32[]{:S(2)}, u32[]{:S(2)}) collective-permute-start(bf16[2,64,2048]{2,1,0:T(8,128)(2,1)} %bitcast.16), channel_id=1, source_target_pairs={{0,6},{1,3},{2,0},{3,5},{4,2},{5,7},{6,4},{7,1},{8,14},{9,11},{10,... | collective-permute-start | bytes 1572872 | tf_op jit(solution)/shard_map/ppermute | solution.py:241
  5.7 27.7 %all-to-all-start = ((bf16[32,8,1024]{2,1,0:T(8,128)(2,1)}), bf16[32,8,1024]{2,1,0:T(8,128)(2,1)S(1)}, u32[]{:S(2)}, u32[]{:S(2)}) async-start(bf16[32,8,1024]{2,1,0:T(8,128)(2,1)} %bitcast.4), calls=%async_computation | async-start | bytes 1048576 | tf_op jit(solution)/shard_map/all_to_all | solution.py:267
  18.0 15.4 %collective-permute-start = (bf16[2,64,2048]{2,1,0:T(8,128)(2,1)S(1)}, bf16[2,64,2048]{2,1,0:T(8,128)(2,1)S(1)}, u32[]{:S(2)}, u32[]{:S(2)}) collective-permute-start(bf16[2,64,2048]{2,1,0:T(8,128)(2,1)S(1)} %get-tuple-element.20), channel_id=1, source_target_pairs={{0,1},{1,0},{2,3},{3,2},{4,5},{5,4},{6,7},{7,6},{8,9},{9,8},{10,11... | collective-permute-start | bytes 1572872 | tf_op jit(solution)/shard_map/ppermute | solution.py:241
  21.1 12.3 %collective-permute-start.3 = (bf16[2,64,2048]{2,1,0:T(8,128)(2,1)}, bf16[2,64,2048]{2,1,0:T(8,128)(2,1)S(1)}, u32[]{:S(2)}, u32[]{:S(2)}) collective-permute-start(bf16[2,64,2048]{2,1,0:T(8,128)(2,1)} %get-tuple-element.22), channel_id=1, source_target_pairs={{0,1},{1,0},{2,3},{3,2},{4,5},{5,4},{6,7},{7,6},{8,9},{9,8},{10,11... | collective-permute-start | bytes 1572872 | tf_op jit(solution)/shard_map/ppermute | solution.py:241
  22.3 4.7 %collective-permute-start.7 = (bf16[2,64,512]{2,1,0:T(8,128)(2,1)S(1)}, bf16[2,64,512]{2,1,0:T(8,128)(2,1)S(1)}, u32[]{:S(2)}, u32[]{:S(2)}) collective-permute-start(bf16[2,64,512]{2,1,0:T(8,128)(2,1)S(1)} %get-tuple-element.24), channel_id=1, source_target_pairs={{0,2},{1,3},{2,0},{3,1},{4,6},{5,7},{6,4},{7,5},{8,10},{9,11},{10,... | collective-permute-start | bytes 393224 | tf_op jit(solution)/shard_map/ppermute | solution.py:241
  23.3 8.9 %collective-permute-start.8 = (bf16[2,64,512]{2,1,0:T(8,128)(2,1)S(1)}, bf16[2,64,512]{2,1,0:T(8,128)(2,1)S(1)}, u32[]{:S(2)}, u32[]{:S(2)}) collective-permute-start(bf16[2,64,512]{2,1,0:T(8,128)(2,1)S(1)} %get-tuple-element.25), channel_id=1, source_target_pairs={{0,6},{1,7},{2,4},{3,5},{4,2},{5,3},{6,0},{7,1},{8,14},{9,15},{10,... | collective-permute-start | bytes 393224 | tf_op jit(solution)/shard_map/ppermute | solution.py:241
  23.4 8.9 %collective-permute-start.9 = (bf16[2,64,512]{2,1,0:T(8,128)(2,1)S(1)}, bf16[2,64,512]{2,1,0:T(8,128)(2,1)S(1)}, u32[]{:S(2)}, u32[]{:S(2)}) collective-permute-start(bf16[2,64,512]{2,1,0:T(8,128)(2,1)S(1)} %get-tuple-element.26), channel_id=1, source_target_pairs={{0,4},{1,5},{2,6},{3,7},{4,0},{5,1},{6,2},{7,3},{8,12},{9,13},{10,... | collective-permute-start | bytes 393224 | tf_op jit(solution)/shard_map/ppermute | solution.py:241
  32.3 5.5 %collective-permute-start.10 = (bf16[4,64,512]{2,1,0:T(8,128)(2,1)S(1)}, bf16[4,64,512]{2,1,0:T(8,128)(2,1)}, u32[]{:S(2)}, u32[]{:S(2)}) collective-permute-start(bf16[4,64,512]{2,1,0:T(8,128)(2,1)S(1)} %give.1), channel_id=1, source_target_pairs={{0,1},{1,0},{2,3},{3,2},{4,5},{5,4},{6,7},{7,6},{8,9},{9,8},{10,11... | collective-permute-start | bytes 786440 | tf_op jit(solution)/shard_map/ppermute | solution.py:241
  34.4 3.3 %collective-permute-start.4 = (bf16[128,256]{1,0:T(8,128)(2,1)S(1)}, bf16[128,256]{1,0:T(8,128)(2,1)S(1)}, u32[]{:S(2)}, u32[]{:S(2)}) collective-permute-start(bf16[128,256]{1,0:T(8,128)(2,1)S(1)} %hidden.1.h_own), channel_id=1, source_target_pairs={{0,2},{1,3},{2,0},{3,1},{4,6},{5,7},{6,4},{7,5},{8,10},{9,11},{10,... | collective-permute-start | bytes 196616 | tf_op jit(solution)/shard_map/ppermute | solution.py:241
  34.5 4.4 %collective-permute-start.5 = (bf16[128,256]{1,0:T(8,128)(2,1)S(1)}, bf16[128,256]{1,0:T(8,128)(2,1)S(1)}, u32[]{:S(2)}, u32[]{:S(2)}) collective-permute-start(bf16[128,256]{1,0:T(8,128)(2,1)S(1)} %hidden.1.h_own), channel_id=1, source_target_pairs={{0,6},{1,7},{2,4},{3,5},{4,2},{5,3},{6,0},{7,1},{8,14},{9,15},{10,... | collective-permute-start | bytes 196616 | tf_op jit(solution)/shard_map/ppermute | solution.py:241
  36.0 4.6 %collective-permute-start.6 = (bf16[128,256]{1,0:T(8,128)(2,1)S(1)}, bf16[128,256]{1,0:T(8,128)(2,1)S(1)}, u32[]{:S(2)}, u32[]{:S(2)}) collective-permute-start(bf16[128,256]{1,0:T(8,128)(2,1)S(1)} %hidden.1.h_own), channel_id=1, source_target_pairs={{0,4},{1,5},{2,6},{3,7},{4,0},{5,1},{6,2},{7,3},{8,12},{9,13},{10,... | collective-permute-start | bytes 196616 | tf_op jit(solution)/shard_map/ppermute | solution.py:241
  42.8 20.2 %all-to-all-start.1 = ((f16[32,8,640]{2,1,0:T(8,128)(2,1)}), f16[32,8,640]{2,1,0:T(8,128)(2,1)S(1)}, u32[]{:S(2)}, u32[]{:S(2)}) async-start(f16[32,8,640]{2,1,0:T(8,128)(2,1)} %convert_bitcast_fusion), calls=%async_computation.1 | async-start | bytes 655360 | tf_op jit(solution)/shard_map/all_to_all | solution.py:333
  63.5 5.1 %collective-permute-start.11 = (f32[64,256]{1,0:T(8,128)S(1)}, f32[64,256]{1,0:T(8,128)S(1)}, u32[]{:S(2)}, u32[]{:S(2)}) collective-permute-start(f32[64,256]{1,0:T(8,128)S(1)} %get-tuple-element.28), channel_id=1, source_target_pairs={{0,1},{1,0},{2,3},{3,2},{4,5},{5,4},{6,7},{7,6},{8,9},{9,8},{10,11... | collective-permute-start | bytes 196616 | tf_op jit(solution)/shard_map/ppermute | solution.py:344

commit v4 on v3

--- a/solution.py
+++ b/solution.py
@@ -10,6 +10,7 @@
 
 GROUPS = 4
 CORES = 2
+DEPTH, SPAN = 8, 4
 EPSILON = 1e-05
 LANES = 128
 HEADROOM = 13.0
@@ -70,11 +71,15 @@
         giving[i] = ref[1 - core]
 
 
+def member(place):
+    return place % DEPTH * SPAN + place // DEPTH
+
+
 def slots_of(ids, core, experts, copies):
     top_count, rows = ids.shape
     ids = jnp.concatenate([ids] * copies, axis=1)
     shape = (experts, rows * copies)
-    expert = CORES * iota(shape, 0) + core
+    expert = CORES * member(iota(shape, 0)) + core
     hits = [ids[k : k + 1, :] == expert for k in range(top_count)]
     named = functools.reduce(jnp.logical_or, hits)
     ones = jnp.where(named, 1.0, 0.0).astype(jnp.bfloat16)
@@ -230,6 +235,7 @@
     rows = ep_size * slots
     share = features // chips
     units = expert_gate.shape[2]
+    order = [[member(i) for i in range(ep_size)]]
     swap = [(i, i ^ 1) for i in range(tp_size)]
     near = [(i, i ^ 2) for i in range(tp_size)]
     same = [(i, 6 - i // 2 * 2 + i % 2) for i in range(tp_size)]
@@ -265,7 +271,7 @@
     gate_both = ppermute(expert_gate.transpose(0, 2, 1), turns)
     up_both = ppermute(expert_up.transpose(0, 2, 1), turns)
     arrived = lax.all_to_all(
-        packed.reshape(ep_size, slots, features // 2), "ep", split_axis=0, concat_axis=0, tiled=True
+        packed.reshape(ep_size, slots, features // 2), "ep", split_axis=0, concat_axis=0, tiled=True, axis_index_groups=order
     ).reshape(rows, features // 2)
 
     pair = pltpu.VMEM((2, units, features), jnp.bfloat16)
@@ -330,7 +336,7 @@
         name="down",
     )(*on_chip(*hiddens), *downs, *on_chip(d_other))
     wire = result.astype(jnp.float16).reshape(ep_size, slots, share + LANES)
-    returned = lax.all_to_all(wire, "ep", split_axis=0, concat_axis=0, tiled=True)
+    returned = lax.all_to_all(wire, "ep", split_axis=0, concat_axis=0, tiled=True, axis_index_groups=order)
     returned = returned.astype(jnp.float32).reshape(rows, share + LANES)
     half = pltpu.VMEM((tok_rows, share // CORES), jnp.float32)
     kept, sent = pl.pallas_call(

time: 69.6 us -> 68.8 us (0.989)
  waiting for transfers between devices: 20.6 us -> 18.8 us
  starting transfers between devices: 37.8 us -> 38.8 us
    all_to_all x1, waiting for transfers between devices: 10.2 us -> 9.07 us  [per_device(): lax.all_to_all(wire, 'ep', split_axis=0, concat_axis=0, tiled=True, axis_...]
where the time goes in v4:
time: 68.8 us; the launch traced here: 68.4 us
  starting transfers between devices  38.8 us (56%)
  waiting for transfers between devices  18.8 us (27%)
  Pallas kernels  9.28 us (13%)
  other arithmetic  1.44 us (2%)
    ppermute x11, starting transfers between devices, ppermute(): return lax.ppermute(array, 'tp', pairs)  13.4 us
    all_to_all x1, starting transfers between devices, per_device(): lax.all_to_all(packed.reshape(ep_size, slots, features // 2), 'ep', split...  11 us
    all_to_all x1, starting transfers between devices, per_device(): lax.all_to_all(wire, 'ep', split_axis=0, concat_axis=0, tiled=True, axis_...  9.78 us
    all_to_all x1, waiting for transfers between devices, per_device(): lax.all_to_all(wire, 'ep', split_axis=0, concat_axis=0, tiled=True, axis_...  9.07 us
    ppermute x11, waiting for transfers between devices, ppermute(): return lax.ppermute(array, 'tp', pairs)  8.85 us
    ppermute x1, starting transfers between devices, per_device(): mixed_out = kept + lax.ppermute(sent, 'tp', swap)  4.55 us
    pallas_call x1, Pallas kernels, per_device(): pl.pallas_call(functools.partial(pack_kernel, slots=slots), out_shape=plt...  2.31 us
    pallas_call x1, Pallas kernels, per_device(): pl.pallas_call(functools.partial(down_kernel, slots=slots), out_shape=plt...  1.48 us
  transfers between devices with their start and end apart: 14, of which 6 were waited for; matrix products, arithmetic and copies ran while one was open for 0% of the time, Pallas kernels for 11%

profile of v4, /device:TPU:1, one launch (start us, length us, event | category | flops | bytes accessed | tf_op | source)
XLA Modules:
  0.0 68.4 jit_solution(4295852829776406173)
XLA Ops:
  0.0 2.1 %collective-permute-start.1 = (bf16[2,64,2048]{2,1,0:T(8,128)(2,1)}, bf16[2,64,2048]{2,1,0:T(8,128)(2,1)S(1)}, u32[]{:S(2)}, u32[]{:S(2)}) collective-permute-start(bf16[2,64,2048]{2,1,0:T(8,128)(2,1)} %bitcast.14), channel_id=1, source_target_pairs={{0,6},{1,3},{2,0},{3,5},{4,2},{5,7},{6,4},{7,1},{8,14},{9,11},{10,... | collective-permute-start | bytes 1572872 | tf_op jit(solution)/shard_map/ppermute | solution.py:247
  2.1 1.3 %collective-permute-start.2 = (bf16[2,64,2048]{2,1,0:T(8,128)(2,1)}, bf16[2,64,2048]{2,1,0:T(8,128)(2,1)S(1)}, u32[]{:S(2)}, u32[]{:S(2)}) collective-permute-start(bf16[2,64,2048]{2,1,0:T(8,128)(2,1)} %bitcast.16), channel_id=1, source_target_pairs={{0,6},{1,3},{2,0},{3,5},{4,2},{5,7},{6,4},{7,1},{8,14},{9,11},{10,... | collective-permute-start | bytes 1572872 | tf_op jit(solution)/shard_map/ppermute | solution.py:247
  3.4 2.3 %pack.1 = bf16[256,1024]{1,0:T(8,128)(2,1)} custom-call(bf16[64,2048]{1,0:T(8,128)(2,1)} %tokens.1, f32[1,2048]{1,0:T(1,128)} %bitcast.18, f32[1,2048]{1,0:T(1,128)} %bitcast.19, s32[4,64]{1,0:T(4,128)} %bitcast.20), custom_call_target="tpu_custom_call" | custom-call | tf_op jit(solution)/shard_map/pack/pallas_call | solution.py:250
  5.7 11.0 %all-to-all-start = ((bf16[32,8,1024]{2,1,0:T(8,128)(2,1)}), bf16[32,8,1024]{2,1,0:T(8,128)(2,1)S(1)}, u32[]{:S(2)}, u32[]{:S(2)}) async-start(bf16[32,8,1024]{2,1,0:T(8,128)(2,1)} %bitcast.4), calls=%async_computation | async-start | bytes 1048576 | tf_op jit(solution)/shard_map/all_to_all | solution.py:273
  16.8 1.2 %theirs.1 = (bf16[2,64,2048]{2,1,0:T(8,128)(2,1)S(1)}, bf16[2,64,2048]{2,1,0:T(8,128)(2,1)S(1)}) custom-call(bf16[2,64,2048]{2,1,0:T(8,128)(2,1)} %bitcast.15, bf16[2,64,2048]{2,1,0:T(8,128)(2,1)} %bitcast.17), custom_call_target="tpu_custom_call" | custom-call | tf_op jit(solution)/shard_map/theirs/pallas_call | solution.py:278
  18.0 2.2 %collective-permute-start = (bf16[2,64,2048]{2,1,0:T(8,128)(2,1)S(1)}, bf16[2,64,2048]{2,1,0:T(8,128)(2,1)S(1)}, u32[]{:S(2)}, u32[]{:S(2)}) collective-permute-start(bf16[2,64,2048]{2,1,0:T(8,128)(2,1)S(1)} %get-tuple-element.20), channel_id=1, source_target_pairs={{0,1},{1,0},{2,3},{3,2},{4,5},{5,4},{6,7},{7,6},{8,9},{9,8},{10,11... | collective-permute-start | bytes 1572872 | tf_op jit(solution)/shard_map/ppermute | solution.py:247
  20.2 0.0 collective-permute-done.1.gate
  20.2 0.0 collective-permute-done.2.up
  20.2 0.9 %pick.1 = (bf16[2,64,2048]{2,1,0:T(8,128)(2,1)S(1)}, bf16[2,64,2048]{2,1,0:T(8,128)(2,1)}) custom-call(bf16[2,64,2048]{2,1,0:T(8,128)(2,1)S(1)} %collective-permute-done.1.gate, bf16[2,64,2048]{2,1,0:T(8,128)(2,1)S(1)} %collective-permute-done.2.up), custom_call_target="tpu_custom_call" | custom-call | tf_op jit(solution)/shard_map/pick/pallas_call | solution.py:289
  21.1 0.0 collective-permute-start.3
  21.1 1.1 %pieces.1 = (bf16[2,64,512]{2,1,0:T(8,128)(2,1)S(1)}, bf16[2,64,512]{2,1,0:T(8,128)(2,1)S(1)}, bf16[2,64,512]{2,1,0:T(8,128)(2,1)S(1)}, bf16[2,64,512]{2,1,0:T(8,128)(2,1)S(1)}) custom-call(bf16[2,64,2048]{2,1,0:T(8,128)(2,1)} %down.2), custom_call_target="tpu_custom_call" | custom-call | tf_op jit(solution)/shard_map/pieces/pallas_call | solution.py:300
  22.3 1.1 %collective-permute-start.7 = (bf16[2,64,512]{2,1,0:T(8,128)(2,1)S(1)}, bf16[2,64,512]{2,1,0:T(8,128)(2,1)S(1)}, u32[]{:S(2)}, u32[]{:S(2)}) collective-permute-start(bf16[2,64,512]{2,1,0:T(8,128)(2,1)S(1)} %get-tuple-element.24), channel_id=1, source_target_pairs={{0,2},{1,3},{2,0},{3,1},{4,6},{5,7},{6,4},{7,5},{8,10},{9,11},{10,... | collective-permute-start | bytes 393224 | tf_op jit(solution)/shard_map/ppermute | solution.py:247
  23.3 0.0 collective-permute-start.8
  23.4 2.2 %collective-permute-start.9 = (bf16[2,64,512]{2,1,0:T(8,128)(2,1)S(1)}, bf16[2,64,512]{2,1,0:T(8,128)(2,1)S(1)}, u32[]{:S(2)}, u32[]{:S(2)}) collective-permute-start(bf16[2,64,512]{2,1,0:T(8,128)(2,1)S(1)} %get-tuple-element.26), channel_id=1, source_target_pairs={{0,4},{1,5},{2,6},{3,7},{4,0},{5,1},{6,2},{7,3},{8,12},{9,13},{10,... | collective-permute-start | bytes 393224 | tf_op jit(solution)/shard_map/ppermute | solution.py:247
  25.6 1.3 %collective-permute-done.7.first = bf16[2,64,512]{2,1,0:T(8,128)(2,1)S(1)} collective-permute-done((bf16[2,64,512]{2,1,0:T(8,128)(2,1)S(1)}, bf16[2,64,512]{2,1,0:T(8,128)(2,1)S(1)}, u32[]{:S(2)}, u32[]{:S(2)}) %collective-permute-start.7) | collective-permute-done | bytes 131104 | tf_op jit(solution)/shard_map/ppermute | solution.py:247
  26.9 5.4 %collective-permute-done.8.second = bf16[2,64,512]{2,1,0:T(8,128)(2,1)S(1)} collective-permute-done((bf16[2,64,512]{2,1,0:T(8,128)(2,1)S(1)}, bf16[2,64,512]{2,1,0:T(8,128)(2,1)S(1)}, u32[]{:S(2)}, u32[]{:S(2)}) %collective-permute-start.8) | collective-permute-done | bytes 131104 | tf_op jit(solution)/shard_map/ppermute | solution.py:247
  32.3 0.0 collective-permute-done.9.third
  32.3 1.1 %collective-permute-start.10 = (bf16[4,64,512]{2,1,0:T(8,128)(2,1)S(1)}, bf16[4,64,512]{2,1,0:T(8,128)(2,1)}, u32[]{:S(2)}, u32[]{:S(2)}) collective-permute-start(bf16[4,64,512]{2,1,0:T(8,128)(2,1)S(1)} %give.1), channel_id=1, source_target_pairs={{0,1},{1,0},{2,3},{3,2},{4,5},{5,4},{6,7},{7,6},{8,9},{9,8},{10,11... | collective-permute-start | bytes 786440 | tf_op jit(solution)/shard_map/ppermute | solution.py:247
  33.4 0.0 collective-permute-done.swapped
  33.4 0.0 all-to-all-done
  33.4 0.0 collective-permute-done.3.passed
  33.4 1.0 %hidden.1.h_own = bf16[128,256]{1,0:T(8,128)(2,1)S(1)} custom-call(bf16[256,1024]{1,0:T(8,128)(2,1)S(1)} %bitcast.13, bf16[2,64,2048]{2,1,0:T(8,128)(2,1)S(1)} %get-tuple-element.19.mine, bf16[2,64,2048]{2,1,0:T(8,128)(2,1)S(1)} %collective-permute-done.swapped, bf16[2,64,2048]{2,1,0:T(8,128)(2,1)S(1)} %get-tuple-element.21.kept_in, ...), custom_call_target="tpu_custom_call" | custom-call | tf_op jit(solution)/shard_map/hidden/pallas_call | solution.py:321
  34.4 0.1 collective-permute-start.4
  34.5 0.6 collective-permute-start.5
  35.1 2.7 %collective-permute-start.6 = (bf16[128,256]{1,0:T(8,128)(2,1)S(1)}, bf16[128,256]{1,0:T(8,128)(2,1)S(1)}, u32[]{:S(2)}, u32[]{:S(2)}) collective-permute-start(bf16[128,256]{1,0:T(8,128)(2,1)S(1)} %hidden.1.h_own), channel_id=1, source_target_pairs={{0,4},{1,5},{2,6},{3,7},{4,0},{5,1},{6,2},{7,3},{8,12},{9,13},{10,... | collective-permute-start | bytes 196616 | tf_op jit(solution)/shard_map/ppermute | solution.py:247
  37.8 0.0 collective-permute-done.10.other
  37.8 0.0 collective-permute-done.4.h_first
  37.8 1.2 %collective-permute-done.5.h_second = bf16[128,256]{1,0:T(8,128)(2,1)S(1)} collective-permute-done((bf16[128,256]{1,0:T(8,128)(2,1)S(1)}, bf16[128,256]{1,0:T(8,128)(2,1)S(1)}, u32[]{:S(2)}, u32[]{:S(2)}) %collective-permute-start.5) | collective-permute-done | bytes 65568 | tf_op jit(solution)/shard_map/ppermute | solution.py:247
  38.9 1.0 %collective-permute-done.6.h_third = bf16[128,256]{1,0:T(8,128)(2,1)S(1)} collective-permute-done((bf16[128,256]{1,0:T(8,128)(2,1)S(1)}, bf16[128,256]{1,0:T(8,128)(2,1)S(1)}, u32[]{:S(2)}, u32[]{:S(2)}) %collective-permute-start.6) | collective-permute-done | bytes 65568 | tf_op jit(solution)/shard_map/ppermute | solution.py:247
  39.9 1.5 %down.3 = f32[256,640]{1,0:T(8,128)S(1)} custom-call(bf16[128,256]{1,0:T(8,128)(2,1)S(1)} %hidden.1.h_own, bf16[128,256]{1,0:T(8,128)(2,1)S(1)} %collective-permute-done.4.h_first, bf16[128,256]{1,0:T(8,128)(2,1)S(1)} %collective-permute-done.5.h_second, bf16[128,256]{1,0:T(8,128)(2,1)S(1)} %collective-permute-done.6.h_third, ...), custom_call_target="tpu_custom_call" | custom-call | tf_op jit(solution)/shard_map/down/pallas_call | solution.py:330
  41.4 0.8 %convert_bitcast_fusion = f16[32,8,640]{2,1,0:T(8,128)(2,1)} fusion(f32[256,640]{1,0:T(8,128)S(1)} %down.3), kind=kLoop, calls=%fused_computation.1 | loop fusion | flops 163840 | bytes 983040 | tf_op jit(solution)/shard_map/reshape | solution.py:338
  42.2 9.8 %all-to-all-start.1 = ((f16[32,8,640]{2,1,0:T(8,128)(2,1)}), f16[32,8,640]{2,1,0:T(8,128)(2,1)S(1)}, u32[]{:S(2)}, u32[]{:S(2)}) async-start(f16[32,8,640]{2,1,0:T(8,128)(2,1)} %convert_bitcast_fusion), calls=%async_computation.1 | async-start | bytes 655360 | tf_op jit(solution)/shard_map/all_to_all | solution.py:339
  52.0 0.9 %factors.1 = (bf16[256,64]{1,0:T(8,128)(2,1)S(1)}, bf16[256,64]{1,0:T(8,128)(2,1)S(1)}) custom-call(s32[4,64]{1,0:T(4,128)} %bitcast.21, f32[4,64]{1,0:T(4,128)} %bitcast.22), custom_call_target="tpu_custom_call" | custom-call | tf_op jit(solution)/shard_map/factors/pallas_call | solution.py:263
  52.9 9.1 %all-to-all-done.1 = f16[32,8,640]{2,1,0:T(8,128)(2,1)S(1)} async-done(((f16[32,8,640]{2,1,0:T(8,128)(2,1)}), f16[32,8,640]{2,1,0:T(8,128)(2,1)S(1)}, u32[]{:S(2)}, u32[]{:S(2)}) %all-to-all-start.1) | async-done | bytes 327712 | tf_op jit(solution)/shard_map/all_to_all | solution.py:339
  62.0 0.3 combine.1
  62.3 4.6 %collective-permute-start.11 = (f32[64,256]{1,0:T(8,128)S(1)}, f32[64,256]{1,0:T(8,128)S(1)}, u32[]{:S(2)}, u32[]{:S(2)}) collective-permute-start(f32[64,256]{1,0:T(8,128)S(1)} %get-tuple-element.28), channel_id=1, source_target_pairs={{0,1},{1,0},{2,3},{3,2},{4,5},{5,4},{6,7},{7,6},{8,9},{9,8},{10,11... | collective-permute-start | bytes 196616 | tf_op jit(solution)/shard_map/ppermute | solution.py:350
  66.9 0.9 %collective-permute-done.11 = f32[64,256]{1,0:T(8,128)S(1)} collective-permute-done((f32[64,256]{1,0:T(8,128)S(1)}, f32[64,256]{1,0:T(8,128)S(1)}, u32[]{:S(2)}, u32[]{:S(2)}) %collective-permute-start.11) | collective-permute-done | bytes 65568 | tf_op jit(solution)/shard_map/ppermute | solution.py:350
  67.8 0.6 add_convert_fusion
  (2 shorter events, 0.1 us)
Async XLA Ops:
  0.0 20.2 %collective-permute-start.1 = (bf16[2,64,2048]{2,1,0:T(8,128)(2,1)}, bf16[2,64,2048]{2,1,0:T(8,128)(2,1)S(1)}, u32[]{:S(2)}, u32[]{:S(2)}) collective-permute-start(bf16[2,64,2048]{2,1,0:T(8,128)(2,1)} %bitcast.14), channel_id=1, source_target_pairs={{0,6},{1,3},{2,0},{3,5},{4,2},{5,7},{6,4},{7,1},{8,14},{9,11},{10,... | collective-permute-start | bytes 1572872 | tf_op jit(solution)/shard_map/ppermute | solution.py:247
  2.1 18.1 %collective-permute-start.2 = (bf16[2,64,2048]{2,1,0:T(8,128)(2,1)}, bf16[2,64,2048]{2,1,0:T(8,128)(2,1)S(1)}, u32[]{:S(2)}, u32[]{:S(2)}) collective-permute-start(bf16[2,64,2048]{2,1,0:T(8,128)(2,1)} %bitcast.16), channel_id=1, source_target_pairs={{0,6},{1,3},{2,0},{3,5},{4,2},{5,7},{6,4},{7,1},{8,14},{9,11},{10,... | collective-permute-start | bytes 1572872 | tf_op jit(solution)/shard_map/ppermute | solution.py:247
  5.7 27.7 %all-to-all-start = ((bf16[32,8,1024]{2,1,0:T(8,128)(2,1)}), bf16[32,8,1024]{2,1,0:T(8,128)(2,1)S(1)}, u32[]{:S(2)}, u32[]{:S(2)}) async-start(bf16[32,8,1024]{2,1,0:T(8,128)(2,1)} %bitcast.4), calls=%async_computation | async-start | bytes 1048576 | tf_op jit(solution)/shard_map/all_to_all | solution.py:273
  18.0 15.4 %collective-permute-start = (bf16[2,64,2048]{2,1,0:T(8,128)(2,1)S(1)}, bf16[2,64,2048]{2,1,0:T(8,128)(2,1)S(1)}, u32[]{:S(2)}, u32[]{:S(2)}) collective-permute-start(bf16[2,64,2048]{2,1,0:T(8,128)(2,1)S(1)} %get-tuple-element.20), channel_id=1, source_target_pairs={{0,1},{1,0},{2,3},{3,2},{4,5},{5,4},{6,7},{7,6},{8,9},{9,8},{10,11... | collective-permute-start | bytes 1572872 | tf_op jit(solution)/shard_map/ppermute | solution.py:247
  21.1 12.3 %collective-permute-start.3 = (bf16[2,64,2048]{2,1,0:T(8,128)(2,1)}, bf16[2,64,2048]{2,1,0:T(8,128)(2,1)S(1)}, u32[]{:S(2)}, u32[]{:S(2)}) collective-permute-start(bf16[2,64,2048]{2,1,0:T(8,128)(2,1)} %get-tuple-element.22), channel_id=1, source_target_pairs={{0,1},{1,0},{2,3},{3,2},{4,5},{5,4},{6,7},{7,6},{8,9},{9,8},{10,11... | collective-permute-start | bytes 1572872 | tf_op jit(solution)/shard_map/ppermute | solution.py:247
  22.3 4.7 %collective-permute-start.7 = (bf16[2,64,512]{2,1,0:T(8,128)(2,1)S(1)}, bf16[2,64,512]{2,1,0:T(8,128)(2,1)S(1)}, u32[]{:S(2)}, u32[]{:S(2)}) collective-permute-start(bf16[2,64,512]{2,1,0:T(8,128)(2,1)S(1)} %get-tuple-element.24), channel_id=1, source_target_pairs={{0,2},{1,3},{2,0},{3,1},{4,6},{5,7},{6,4},{7,5},{8,10},{9,11},{10,... | collective-permute-start | bytes 393224 | tf_op jit(solution)/shard_map/ppermute | solution.py:247
  23.3 8.9 %collective-permute-start.8 = (bf16[2,64,512]{2,1,0:T(8,128)(2,1)S(1)}, bf16[2,64,512]{2,1,0:T(8,128)(2,1)S(1)}, u32[]{:S(2)}, u32[]{:S(2)}) collective-permute-start(bf16[2,64,512]{2,1,0:T(8,128)(2,1)S(1)} %get-tuple-element.25), channel_id=1, source_target_pairs={{0,6},{1,7},{2,4},{3,5},{4,2},{5,3},{6,0},{7,1},{8,14},{9,15},{10,... | collective-permute-start | bytes 393224 | tf_op jit(solution)/shard_map/ppermute | solution.py:247
  23.4 8.9 %collective-permute-start.9 = (bf16[2,64,512]{2,1,0:T(8,128)(2,1)S(1)}, bf16[2,64,512]{2,1,0:T(8,128)(2,1)S(1)}, u32[]{:S(2)}, u32[]{:S(2)}) collective-permute-start(bf16[2,64,512]{2,1,0:T(8,128)(2,1)S(1)} %get-tuple-element.26), channel_id=1, source_target_pairs={{0,4},{1,5},{2,6},{3,7},{4,0},{5,1},{6,2},{7,3},{8,12},{9,13},{10,... | collective-permute-start | bytes 393224 | tf_op jit(solution)/shard_map/ppermute | solution.py:247
  32.3 5.5 %collective-permute-start.10 = (bf16[4,64,512]{2,1,0:T(8,128)(2,1)S(1)}, bf16[4,64,512]{2,1,0:T(8,128)(2,1)}, u32[]{:S(2)}, u32[]{:S(2)}) collective-permute-start(bf16[4,64,512]{2,1,0:T(8,128)(2,1)S(1)} %give.1), channel_id=1, source_target_pairs={{0,1},{1,0},{2,3},{3,2},{4,5},{5,4},{6,7},{7,6},{8,9},{9,8},{10,11... | collective-permute-start | bytes 786440 | tf_op jit(solution)/shard_map/ppermute | solution.py:247
  34.4 3.3 %collective-permute-start.4 = (bf16[128,256]{1,0:T(8,128)(2,1)S(1)}, bf16[128,256]{1,0:T(8,128)(2,1)S(1)}, u32[]{:S(2)}, u32[]{:S(2)}) collective-permute-start(bf16[128,256]{1,0:T(8,128)(2,1)S(1)} %hidden.1.h_own), channel_id=1, source_target_pairs={{0,2},{1,3},{2,0},{3,1},{4,6},{5,7},{6,4},{7,5},{8,10},{9,11},{10,... | collective-permute-start | bytes 196616 | tf_op jit(solution)/shard_map/ppermute | solution.py:247
  34.5 4.4 %collective-permute-start.5 = (bf16[128,256]{1,0:T(8,128)(2,1)S(1)}, bf16[128,256]{1,0:T(8,128)(2,1)S(1)}, u32[]{:S(2)}, u32[]{:S(2)}) collective-permute-start(bf16[128,256]{1,0:T(8,128)(2,1)S(1)} %hidden.1.h_own), channel_id=1, source_target_pairs={{0,6},{1,7},{2,4},{3,5},{4,2},{5,3},{6,0},{7,1},{8,14},{9,15},{10,... | collective-permute-start | bytes 196616 | tf_op jit(solution)/shard_map/ppermute | solution.py:247
  35.1 4.8 %collective-permute-start.6 = (bf16[128,256]{1,0:T(8,128)(2,1)S(1)}, bf16[128,256]{1,0:T(8,128)(2,1)S(1)}, u32[]{:S(2)}, u32[]{:S(2)}) collective-permute-start(bf16[128,256]{1,0:T(8,128)(2,1)S(1)} %hidden.1.h_own), channel_id=1, source_target_pairs={{0,4},{1,5},{2,6},{3,7},{4,0},{5,1},{6,2},{7,3},{8,12},{9,13},{10,... | collective-permute-start | bytes 196616 | tf_op jit(solution)/shard_map/ppermute | solution.py:247
  42.2 19.7 %all-to-all-start.1 = ((f16[32,8,640]{2,1,0:T(8,128)(2,1)}), f16[32,8,640]{2,1,0:T(8,128)(2,1)S(1)}, u32[]{:S(2)}, u32[]{:S(2)}) async-start(f16[32,8,640]{2,1,0:T(8,128)(2,1)} %convert_bitcast_fusion), calls=%async_computation.1 | async-start | bytes 655360 | tf_op jit(solution)/shard_map/all_to_all | solution.py:339
  62.3 5.5 %collective-permute-start.11 = (f32[64,256]{1,0:T(8,128)S(1)}, f32[64,256]{1,0:T(8,128)S(1)}, u32[]{:S(2)}, u32[]{:S(2)}) collective-permute-start(f32[64,256]{1,0:T(8,128)S(1)} %get-tuple-element.28), channel_id=1, source_target_pairs={{0,1},{1,0},{2,3},{3,2},{4,5},{5,4},{6,7},{7,6},{8,9},{9,8},{10,11... | collective-permute-start | bytes 196616 | tf_op jit(solution)/shard_map/ppermute | solution.py:350

commit v5 on v4

--- a/solution.py
+++ b/solution.py
@@ -72,7 +72,8 @@
 
 
 def member(place):
-    return place % DEPTH * SPAN + place // DEPTH
+    back = DEPTH - 1 - place % DEPTH
+    return back * SPAN + place // DEPTH
 
 
 def slots_of(ids, core, experts, copies):
@@ -326,7 +327,8 @@
         compiler_params=PARAMS,
         name="hidden",
     )(*on_chip(arrived, mine, swapped, kept, passed))
-    hiddens = [hidden] + [ppermute(hidden, pairs) for pairs in (near, same, across)]
+    h_across = ppermute(hidden, across)
+    hiddens = [hidden, ppermute(hidden, near), ppermute(hidden, same), h_across]
     result = pl.pallas_call(
         functools.partial(down_kernel, slots=slots),
         out_shape=pltpu.VMEM((rows, share + LANES), jnp.float32),

time: 68.8 us -> 66.2 us (0.962)
  waiting for transfers between devices: 18.8 us -> 17.5 us
  starting transfers between devices: 38.8 us -> 37.5 us
    ppermute x1, starting transfers between devices: 4.55 us -> 3.15 us  [per_device(): mixed_out = kept + lax.ppermute(sent, 'tp', swap)]
    all_to_all x1, waiting for transfers between devices: 9.07 us -> 7.92 us  [per_device(): lax.all_to_all(wire, 'ep', split_axis=0, concat_axis=0, tiled=True, axis_...]
  transfers between devices with their start and end apart: 14 -> 14, of which waited for: 6 -> 7; matrix products, arithmetic and copies ran while one was open for 0% -> 0% of each run, Pallas kernels for 11% -> 11%
where the time goes in v5:
time: 66.2 us; the launch traced here: 65.9 us
  starting transfers between devices  37.5 us (57%)
  waiting for transfers between devices  17.5 us (26%)
  Pallas kernels  9.28 us (14%)
  other arithmetic  1.44 us (2%)
    ppermute x11, starting transfers between devices, ppermute(): return lax.ppermute(array, 'tp', pairs)  13.7 us
    all_to_all x1, starting transfers between devices, per_device(): lax.all_to_all(packed.reshape(ep_size, slots, features // 2), 'ep', split...  11.1 us
    all_to_all x1, starting transfers between devices, per_device(): lax.all_to_all(wire, 'ep', split_axis=0, concat_axis=0, tiled=True, axis_...  9.61 us
    ppermute x11, waiting for transfers between devices, ppermute(): return lax.ppermute(array, 'tp', pairs)  8.71 us
    all_to_all x1, waiting for transfers between devices, per_device(): lax.all_to_all(wire, 'ep', split_axis=0, concat_axis=0, tiled=True, axis_...  7.92 us
    ppermute x1, starting transfers between devices, per_device(): mixed_out = kept + lax.ppermute(sent, 'tp', swap)  3.15 us
    pallas_call x1, Pallas kernels, per_device(): pl.pallas_call(functools.partial(pack_kernel, slots=slots), out_shape=plt...  2.31 us
    pallas_call x1, Pallas kernels, per_device(): pl.pallas_call(functools.partial(down_kernel, slots=slots), out_shape=plt...  1.48 us
  transfers between devices with their start and end apart: 14, of which 7 were waited for; matrix products, arithmetic and copies ran while one was open for 0% of the time, Pallas kernels for 11%

profile of v5, /device:TPU:1, one launch (start us, length us, event | category | flops | bytes accessed | tf_op | source)
XLA Modules:
  0.0 65.9 jit_solution(14340357879397185944)
XLA Ops:
  0.0 2.1 %collective-permute-start.1 = (bf16[2,64,2048]{2,1,0:T(8,128)(2,1)}, bf16[2,64,2048]{2,1,0:T(8,128)(2,1)S(1)}, u32[]{:S(2)}, u32[]{:S(2)}) collective-permute-start(bf16[2,64,2048]{2,1,0:T(8,128)(2,1)} %bitcast.14), channel_id=1, source_target_pairs={{0,6},{1,3},{2,0},{3,5},{4,2},{5,7},{6,4},{7,1},{8,14},{9,11},{10,... | collective-permute-start | bytes 1572872 | tf_op jit(solution)/shard_map/ppermute | solution.py:248
  2.1 1.3 %collective-permute-start.2 = (bf16[2,64,2048]{2,1,0:T(8,128)(2,1)}, bf16[2,64,2048]{2,1,0:T(8,128)(2,1)S(1)}, u32[]{:S(2)}, u32[]{:S(2)}) collective-permute-start(bf16[2,64,2048]{2,1,0:T(8,128)(2,1)} %bitcast.16), channel_id=1, source_target_pairs={{0,6},{1,3},{2,0},{3,5},{4,2},{5,7},{6,4},{7,1},{8,14},{9,11},{10,... | collective-permute-start | bytes 1572872 | tf_op jit(solution)/shard_map/ppermute | solution.py:248
  3.4 2.3 %pack.1 = bf16[256,1024]{1,0:T(8,128)(2,1)} custom-call(bf16[64,2048]{1,0:T(8,128)(2,1)} %tokens.1, f32[1,2048]{1,0:T(1,128)} %bitcast.18, f32[1,2048]{1,0:T(1,128)} %bitcast.19, s32[4,64]{1,0:T(4,128)} %bitcast.20), custom_call_target="tpu_custom_call" | custom-call | tf_op jit(solution)/shard_map/pack/pallas_call | solution.py:251
  5.7 11.1 %all-to-all-start = ((bf16[32,8,1024]{2,1,0:T(8,128)(2,1)}), bf16[32,8,1024]{2,1,0:T(8,128)(2,1)S(1)}, u32[]{:S(2)}, u32[]{:S(2)}) async-start(bf16[32,8,1024]{2,1,0:T(8,128)(2,1)} %bitcast.4), calls=%async_computation | async-start | bytes 1048576 | tf_op jit(solution)/shard_map/all_to_all | solution.py:274
  16.8 1.2 %theirs.1 = (bf16[2,64,2048]{2,1,0:T(8,128)(2,1)S(1)}, bf16[2,64,2048]{2,1,0:T(8,128)(2,1)S(1)}) custom-call(bf16[2,64,2048]{2,1,0:T(8,128)(2,1)} %bitcast.15, bf16[2,64,2048]{2,1,0:T(8,128)(2,1)} %bitcast.17), custom_call_target="tpu_custom_call" | custom-call | tf_op jit(solution)/shard_map/theirs/pallas_call | solution.py:279
  18.1 2.5 %collective-permute-start = (bf16[2,64,2048]{2,1,0:T(8,128)(2,1)S(1)}, bf16[2,64,2048]{2,1,0:T(8,128)(2,1)S(1)}, u32[]{:S(2)}, u32[]{:S(2)}) collective-permute-start(bf16[2,64,2048]{2,1,0:T(8,128)(2,1)S(1)} %get-tuple-element.20), channel_id=1, source_target_pairs={{0,1},{1,0},{2,3},{3,2},{4,5},{5,4},{6,7},{7,6},{8,9},{9,8},{10,11... | collective-permute-start | bytes 1572872 | tf_op jit(solution)/shard_map/ppermute | solution.py:248
  20.5 0.0 collective-permute-done.1.gate
  20.5 0.0 collective-permute-done.2.up
  20.5 0.9 %pick.1 = (bf16[2,64,2048]{2,1,0:T(8,128)(2,1)S(1)}, bf16[2,64,2048]{2,1,0:T(8,128)(2,1)}) custom-call(bf16[2,64,2048]{2,1,0:T(8,128)(2,1)S(1)} %collective-permute-done.1.gate, bf16[2,64,2048]{2,1,0:T(8,128)(2,1)S(1)} %collective-permute-done.2.up), custom_call_target="tpu_custom_call" | custom-call | tf_op jit(solution)/shard_map/pick/pallas_call | solution.py:290
  21.4 0.0 collective-permute-start.3
  21.4 1.1 %pieces.1 = (bf16[2,64,512]{2,1,0:T(8,128)(2,1)S(1)}, bf16[2,64,512]{2,1,0:T(8,128)(2,1)S(1)}, bf16[2,64,512]{2,1,0:T(8,128)(2,1)S(1)}, bf16[2,64,512]{2,1,0:T(8,128)(2,1)S(1)}) custom-call(bf16[2,64,2048]{2,1,0:T(8,128)(2,1)} %down.2), custom_call_target="tpu_custom_call" | custom-call | tf_op jit(solution)/shard_map/pieces/pallas_call | solution.py:301
  22.6 1.1 %collective-permute-start.7 = (bf16[2,64,512]{2,1,0:T(8,128)(2,1)S(1)}, bf16[2,64,512]{2,1,0:T(8,128)(2,1)S(1)}, u32[]{:S(2)}, u32[]{:S(2)}) collective-permute-start(bf16[2,64,512]{2,1,0:T(8,128)(2,1)S(1)} %get-tuple-element.24), channel_id=1, source_target_pairs={{0,2},{1,3},{2,0},{3,1},{4,6},{5,7},{6,4},{7,5},{8,10},{9,11},{10,... | collective-permute-start | bytes 393224 | tf_op jit(solution)/shard_map/ppermute | solution.py:248
  23.7 0.0 collective-permute-start.8
  23.7 2.2 %collective-permute-start.9 = (bf16[2,64,512]{2,1,0:T(8,128)(2,1)S(1)}, bf16[2,64,512]{2,1,0:T(8,128)(2,1)S(1)}, u32[]{:S(2)}, u32[]{:S(2)}) collective-permute-start(bf16[2,64,512]{2,1,0:T(8,128)(2,1)S(1)} %get-tuple-element.26), channel_id=1, source_target_pairs={{0,4},{1,5},{2,6},{3,7},{4,0},{5,1},{6,2},{7,3},{8,12},{9,13},{10,... | collective-permute-start | bytes 393224 | tf_op jit(solution)/shard_map/ppermute | solution.py:248
  25.9 1.3 %collective-permute-done.7.first = bf16[2,64,512]{2,1,0:T(8,128)(2,1)S(1)} collective-permute-done((bf16[2,64,512]{2,1,0:T(8,128)(2,1)S(1)}, bf16[2,64,512]{2,1,0:T(8,128)(2,1)S(1)}, u32[]{:S(2)}, u32[]{:S(2)}) %collective-permute-start.7) | collective-permute-done | bytes 131104 | tf_op jit(solution)/shard_map/ppermute | solution.py:248
  27.3 5.4 %collective-permute-done.8.second = bf16[2,64,512]{2,1,0:T(8,128)(2,1)S(1)} collective-permute-done((bf16[2,64,512]{2,1,0:T(8,128)(2,1)S(1)}, bf16[2,64,512]{2,1,0:T(8,128)(2,1)S(1)}, u32[]{:S(2)}, u32[]{:S(2)}) %collective-permute-start.8) | collective-permute-done | bytes 131104 | tf_op jit(solution)/shard_map/ppermute | solution.py:248
  32.6 0.0 collective-permute-done.9.third
  32.7 1.1 %collective-permute-start.10 = (bf16[4,64,512]{2,1,0:T(8,128)(2,1)S(1)}, bf16[4,64,512]{2,1,0:T(8,128)(2,1)}, u32[]{:S(2)}, u32[]{:S(2)}) collective-permute-start(bf16[4,64,512]{2,1,0:T(8,128)(2,1)S(1)} %give.1), channel_id=1, source_target_pairs={{0,1},{1,0},{2,3},{3,2},{4,5},{5,4},{6,7},{7,6},{8,9},{9,8},{10,11... | collective-permute-start | bytes 786440 | tf_op jit(solution)/shard_map/ppermute | solution.py:248
  33.7 0.0 collective-permute-done.swapped
  33.7 0.0 all-to-all-done
  33.7 0.0 collective-permute-done.3.passed
  33.7 1.0 %hidden.1.h_own = bf16[128,256]{1,0:T(8,128)(2,1)S(1)} custom-call(bf16[256,1024]{1,0:T(8,128)(2,1)S(1)} %bitcast.13, bf16[2,64,2048]{2,1,0:T(8,128)(2,1)S(1)} %get-tuple-element.19.mine, bf16[2,64,2048]{2,1,0:T(8,128)(2,1)S(1)} %collective-permute-done.swapped, bf16[2,64,2048]{2,1,0:T(8,128)(2,1)S(1)} %get-tuple-element.21.kept_in, ...), custom_call_target="tpu_custom_call" | custom-call | tf_op jit(solution)/shard_map/hidden/pallas_call | solution.py:322
  34.8 0.1 collective-permute-start.4
  34.9 0.6 collective-permute-start.5
  35.4 2.7 %collective-permute-start.6 = (bf16[128,256]{1,0:T(8,128)(2,1)S(1)}, bf16[128,256]{1,0:T(8,128)(2,1)S(1)}, u32[]{:S(2)}, u32[]{:S(2)}) collective-permute-start(bf16[128,256]{1,0:T(8,128)(2,1)S(1)} %hidden.1.h_own), channel_id=1, source_target_pairs={{0,4},{1,5},{2,6},{3,7},{4,0},{5,1},{6,2},{7,3},{8,12},{9,13},{10,... | collective-permute-start | bytes 196616 | tf_op jit(solution)/shard_map/ppermute | solution.py:248
  38.1 0.0 collective-permute-done.10.other
  38.1 0.4 collective-permute-done.4.h_first
  38.5 0.8 %collective-permute-done.5.h_second = bf16[128,256]{1,0:T(8,128)(2,1)S(1)} collective-permute-done((bf16[128,256]{1,0:T(8,128)(2,1)S(1)}, bf16[128,256]{1,0:T(8,128)(2,1)S(1)}, u32[]{:S(2)}, u32[]{:S(2)}) %collective-permute-start.5) | collective-permute-done | bytes 65568 | tf_op jit(solution)/shard_map/ppermute | solution.py:248
  39.3 0.8 %collective-permute-done.6.h_third = bf16[128,256]{1,0:T(8,128)(2,1)S(1)} collective-permute-done((bf16[128,256]{1,0:T(8,128)(2,1)S(1)}, bf16[128,256]{1,0:T(8,128)(2,1)S(1)}, u32[]{:S(2)}, u32[]{:S(2)}) %collective-permute-start.6) | collective-permute-done | bytes 65568 | tf_op jit(solution)/shard_map/ppermute | solution.py:248
  40.1 1.5 %down.3 = f32[256,640]{1,0:T(8,128)S(1)} custom-call(bf16[128,256]{1,0:T(8,128)(2,1)S(1)} %hidden.1.h_own, bf16[128,256]{1,0:T(8,128)(2,1)S(1)} %collective-permute-done.4.h_first, bf16[128,256]{1,0:T(8,128)(2,1)S(1)} %collective-permute-done.5.h_second, bf16[128,256]{1,0:T(8,128)(2,1)S(1)} %collective-permute-done.6.h_third, ...), custom_call_target="tpu_custom_call" | custom-call | tf_op jit(solution)/shard_map/down/pallas_call | solution.py:332
  41.6 0.8 %convert_bitcast_fusion = f16[32,8,640]{2,1,0:T(8,128)(2,1)} fusion(f32[256,640]{1,0:T(8,128)S(1)} %down.3), kind=kLoop, calls=%fused_computation.1 | loop fusion | flops 163840 | bytes 983040 | tf_op jit(solution)/shard_map/reshape | solution.py:340
  42.4 9.6 %all-to-all-start.1 = ((f16[32,8,640]{2,1,0:T(8,128)(2,1)}), f16[32,8,640]{2,1,0:T(8,128)(2,1)S(1)}, u32[]{:S(2)}, u32[]{:S(2)}) async-start(f16[32,8,640]{2,1,0:T(8,128)(2,1)} %convert_bitcast_fusion), calls=%async_computation.1 | async-start | bytes 655360 | tf_op jit(solution)/shard_map/all_to_all | solution.py:341
  52.0 0.9 %factors.1 = (bf16[256,64]{1,0:T(8,128)(2,1)S(1)}, bf16[256,64]{1,0:T(8,128)(2,1)S(1)}) custom-call(s32[4,64]{1,0:T(4,128)} %bitcast.21, f32[4,64]{1,0:T(4,128)} %bitcast.22), custom_call_target="tpu_custom_call" | custom-call | tf_op jit(solution)/shard_map/factors/pallas_call | solution.py:264
  52.8 7.9 %all-to-all-done.1 = f16[32,8,640]{2,1,0:T(8,128)(2,1)S(1)} async-done(((f16[32,8,640]{2,1,0:T(8,128)(2,1)}), f16[32,8,640]{2,1,0:T(8,128)(2,1)S(1)}, u32[]{:S(2)}, u32[]{:S(2)}) %all-to-all-start.1) | async-done | bytes 327712 | tf_op jit(solution)/shard_map/all_to_all | solution.py:341
  60.8 0.3 combine.1
  61.2 3.2 %collective-permute-start.11 = (f32[64,256]{1,0:T(8,128)S(1)}, f32[64,256]{1,0:T(8,128)S(1)}, u32[]{:S(2)}, u32[]{:S(2)}) collective-permute-start(f32[64,256]{1,0:T(8,128)S(1)} %get-tuple-element.28), channel_id=1, source_target_pairs={{0,1},{1,0},{2,3},{3,2},{4,5},{5,4},{6,7},{7,6},{8,9},{9,8},{10,11... | collective-permute-start | bytes 196616 | tf_op jit(solution)/shard_map/ppermute | solution.py:352
  64.3 0.9 %collective-permute-done.11 = f32[64,256]{1,0:T(8,128)S(1)} collective-permute-done((f32[64,256]{1,0:T(8,128)S(1)}, f32[64,256]{1,0:T(8,128)S(1)}, u32[]{:S(2)}, u32[]{:S(2)}) %collective-permute-start.11) | collective-permute-done | bytes 65568 | tf_op jit(solution)/shard_map/ppermute | solution.py:352
  65.2 0.6 add_convert_fusion
  (2 shorter events, 0.1 us)
Async XLA Ops:
  0.0 20.5 %collective-permute-start.1 = (bf16[2,64,2048]{2,1,0:T(8,128)(2,1)}, bf16[2,64,2048]{2,1,0:T(8,128)(2,1)S(1)}, u32[]{:S(2)}, u32[]{:S(2)}) collective-permute-start(bf16[2,64,2048]{2,1,0:T(8,128)(2,1)} %bitcast.14), channel_id=1, source_target_pairs={{0,6},{1,3},{2,0},{3,5},{4,2},{5,7},{6,4},{7,1},{8,14},{9,11},{10,... | collective-permute-start | bytes 1572872 | tf_op jit(solution)/shard_map/ppermute | solution.py:248
  2.1 18.4 %collective-permute-start.2 = (bf16[2,64,2048]{2,1,0:T(8,128)(2,1)}, bf16[2,64,2048]{2,1,0:T(8,128)(2,1)S(1)}, u32[]{:S(2)}, u32[]{:S(2)}) collective-permute-start(bf16[2,64,2048]{2,1,0:T(8,128)(2,1)} %bitcast.16), channel_id=1, source_target_pairs={{0,6},{1,3},{2,0},{3,5},{4,2},{5,7},{6,4},{7,1},{8,14},{9,11},{10,... | collective-permute-start | bytes 1572872 | tf_op jit(solution)/shard_map/ppermute | solution.py:248
  5.7 28.0 %all-to-all-start = ((bf16[32,8,1024]{2,1,0:T(8,128)(2,1)}), bf16[32,8,1024]{2,1,0:T(8,128)(2,1)S(1)}, u32[]{:S(2)}, u32[]{:S(2)}) async-start(bf16[32,8,1024]{2,1,0:T(8,128)(2,1)} %bitcast.4), calls=%async_computation | async-start | bytes 1048576 | tf_op jit(solution)/shard_map/all_to_all | solution.py:274
  18.1 15.7 %collective-permute-start = (bf16[2,64,2048]{2,1,0:T(8,128)(2,1)S(1)}, bf16[2,64,2048]{2,1,0:T(8,128)(2,1)S(1)}, u32[]{:S(2)}, u32[]{:S(2)}) collective-permute-start(bf16[2,64,2048]{2,1,0:T(8,128)(2,1)S(1)} %get-tuple-element.20), channel_id=1, source_target_pairs={{0,1},{1,0},{2,3},{3,2},{4,5},{5,4},{6,7},{7,6},{8,9},{9,8},{10,11... | collective-permute-start | bytes 1572872 | tf_op jit(solution)/shard_map/ppermute | solution.py:248
  21.4 12.3 %collective-permute-start.3 = (bf16[2,64,2048]{2,1,0:T(8,128)(2,1)}, bf16[2,64,2048]{2,1,0:T(8,128)(2,1)S(1)}, u32[]{:S(2)}, u32[]{:S(2)}) collective-permute-start(bf16[2,64,2048]{2,1,0:T(8,128)(2,1)} %get-tuple-element.22), channel_id=1, source_target_pairs={{0,1},{1,0},{2,3},{3,2},{4,5},{5,4},{6,7},{7,6},{8,9},{9,8},{10,11... | collective-permute-start | bytes 1572872 | tf_op jit(solution)/shard_map/ppermute | solution.py:248
  22.6 4.7 %collective-permute-start.7 = (bf16[2,64,512]{2,1,0:T(8,128)(2,1)S(1)}, bf16[2,64,512]{2,1,0:T(8,128)(2,1)S(1)}, u32[]{:S(2)}, u32[]{:S(2)}) collective-permute-start(bf16[2,64,512]{2,1,0:T(8,128)(2,1)S(1)} %get-tuple-element.24), channel_id=1, source_target_pairs={{0,2},{1,3},{2,0},{3,1},{4,6},{5,7},{6,4},{7,5},{8,10},{9,11},{10,... | collective-permute-start | bytes 393224 | tf_op jit(solution)/shard_map/ppermute | solution.py:248
  23.7 9.0 %collective-permute-start.8 = (bf16[2,64,512]{2,1,0:T(8,128)(2,1)S(1)}, bf16[2,64,512]{2,1,0:T(8,128)(2,1)S(1)}, u32[]{:S(2)}, u32[]{:S(2)}) collective-permute-start(bf16[2,64,512]{2,1,0:T(8,128)(2,1)S(1)} %get-tuple-element.25), channel_id=1, source_target_pairs={{0,6},{1,7},{2,4},{3,5},{4,2},{5,3},{6,0},{7,1},{8,14},{9,15},{10,... | collective-permute-start | bytes 393224 | tf_op jit(solution)/shard_map/ppermute | solution.py:248
  23.7 9.0 %collective-permute-start.9 = (bf16[2,64,512]{2,1,0:T(8,128)(2,1)S(1)}, bf16[2,64,512]{2,1,0:T(8,128)(2,1)S(1)}, u32[]{:S(2)}, u32[]{:S(2)}) collective-permute-start(bf16[2,64,512]{2,1,0:T(8,128)(2,1)S(1)} %get-tuple-element.26), channel_id=1, source_target_pairs={{0,4},{1,5},{2,6},{3,7},{4,0},{5,1},{6,2},{7,3},{8,12},{9,13},{10,... | collective-permute-start | bytes 393224 | tf_op jit(solution)/shard_map/ppermute | solution.py:248
  32.7 5.4 %collective-permute-start.10 = (bf16[4,64,512]{2,1,0:T(8,128)(2,1)S(1)}, bf16[4,64,512]{2,1,0:T(8,128)(2,1)}, u32[]{:S(2)}, u32[]{:S(2)}) collective-permute-start(bf16[4,64,512]{2,1,0:T(8,128)(2,1)S(1)} %give.1), channel_id=1, source_target_pairs={{0,1},{1,0},{2,3},{3,2},{4,5},{5,4},{6,7},{7,6},{8,9},{9,8},{10,11... | collective-permute-start | bytes 786440 | tf_op jit(solution)/shard_map/ppermute | solution.py:248
  34.8 3.7 %collective-permute-start.4 = (bf16[128,256]{1,0:T(8,128)(2,1)S(1)}, bf16[128,256]{1,0:T(8,128)(2,1)S(1)}, u32[]{:S(2)}, u32[]{:S(2)}) collective-permute-start(bf16[128,256]{1,0:T(8,128)(2,1)S(1)} %hidden.1.h_own), channel_id=1, source_target_pairs={{0,2},{1,3},{2,0},{3,1},{4,6},{5,7},{6,4},{7,5},{8,10},{9,11},{10,... | collective-permute-start | bytes 196616 | tf_op jit(solution)/shard_map/ppermute | solution.py:248
  34.9 4.4 %collective-permute-start.5 = (bf16[128,256]{1,0:T(8,128)(2,1)S(1)}, bf16[128,256]{1,0:T(8,128)(2,1)S(1)}, u32[]{:S(2)}, u32[]{:S(2)}) collective-permute-start(bf16[128,256]{1,0:T(8,128)(2,1)S(1)} %hidden.1.h_own), channel_id=1, source_target_pairs={{0,6},{1,7},{2,4},{3,5},{4,2},{5,3},{6,0},{7,1},{8,14},{9,15},{10,... | collective-permute-start | bytes 196616 | tf_op jit(solution)/shard_map/ppermute | solution.py:248
  35.4 4.7 %collective-permute-start.6 = (bf16[128,256]{1,0:T(8,128)(2,1)S(1)}, bf16[128,256]{1,0:T(8,128)(2,1)S(1)}, u32[]{:S(2)}, u32[]{:S(2)}) collective-permute-start(bf16[128,256]{1,0:T(8,128)(2,1)S(1)} %hidden.1.h_own), channel_id=1, source_target_pairs={{0,4},{1,5},{2,6},{3,7},{4,0},{5,1},{6,2},{7,3},{8,12},{9,13},{10,... | collective-permute-start | bytes 196616 | tf_op jit(solution)/shard_map/ppermute | solution.py:248
  42.4 18.4 %all-to-all-start.1 = ((f16[32,8,640]{2,1,0:T(8,128)(2,1)}), f16[32,8,640]{2,1,0:T(8,128)(2,1)S(1)}, u32[]{:S(2)}, u32[]{:S(2)}) async-start(f16[32,8,640]{2,1,0:T(8,128)(2,1)} %convert_bitcast_fusion), calls=%async_computation.1 | async-start | bytes 655360 | tf_op jit(solution)/shard_map/all_to_all | solution.py:341
  61.2 4.1 %collective-permute-start.11 = (f32[64,256]{1,0:T(8,128)S(1)}, f32[64,256]{1,0:T(8,128)S(1)}, u32[]{:S(2)}, u32[]{:S(2)}) collective-permute-start(f32[64,256]{1,0:T(8,128)S(1)} %get-tuple-element.28), channel_id=1, source_target_pairs={{0,1},{1,0},{2,3},{3,2},{4,5},{5,4},{6,7},{7,6},{8,9},{9,8},{10,11... | collective-permute-start | bytes 196616 | tf_op jit(solution)/shard_map/ppermute | solution.py:352

commit v6 on v5

--- a/solution.py
+++ b/solution.py
@@ -10,7 +10,7 @@
 
 GROUPS = 4
 CORES = 2
-DEPTH, SPAN = 8, 4
+MEMBERS, SPAN = 32, 4
 EPSILON = 1e-05
 LANES = 128
 HEADROOM = 13.0
@@ -72,8 +72,7 @@
 
 
 def member(place):
-    back = DEPTH - 1 - place % DEPTH
-    return back * SPAN + place // DEPTH
+    return (MEMBERS - 1 - SPAN - place) % MEMBERS
 
 
 def slots_of(ids, core, experts, copies):

time: 66.2 us -> 65.7 us (level)
  waiting for transfers between devices: 17.5 us -> 16 us
  starting transfers between devices: 37.5 us -> 38.6 us
    all_to_all x1, waiting for transfers between devices: 7.92 us -> 5.98 us  [per_device(): lax.all_to_all(wire, 'ep', split_axis=0, concat_axis=0, tiled=True, axis_...]
    all_to_all x1, starting transfers between devices: 11.1 us -> 11.9 us  [per_device(): lax.all_to_all(packed.reshape(ep_size, slots, features // 2), 'ep', split...]
    ppermute x1, starting transfers between devices: 3.15 us -> 3.83 us  [per_device(): mixed_out = kept + lax.ppermute(sent, 'tp', swap)]
  transfers between devices with their start and end apart: 14 -> 14, of which waited for: 7 -> 6; matrix products, arithmetic and copies ran while one was open for 0% -> 0% of each run, Pallas kernels for 11% -> 11%
where the time goes in v6:
time: 65.7 us; the launch traced here: 65.4 us
  starting transfers between devices  38.6 us (59%)
  waiting for transfers between devices  16 us (24%)
  Pallas kernels  9.28 us (14%)
  other arithmetic  1.44 us (2%)
    ppermute x11, starting transfers between devices, ppermute(): return lax.ppermute(array, 'tp', pairs)  13.5 us
    all_to_all x1, starting transfers between devices, per_device(): lax.all_to_all(packed.reshape(ep_size, slots, features // 2), 'ep', split...  11.9 us
    all_to_all x1, starting transfers between devices, per_device(): lax.all_to_all(wire, 'ep', split_axis=0, concat_axis=0, tiled=True, axis_...  9.38 us
    ppermute x11, waiting for transfers between devices, ppermute(): return lax.ppermute(array, 'tp', pairs)  9.1 us
    all_to_all x1, waiting for transfers between devices, per_device(): lax.all_to_all(wire, 'ep', split_axis=0, concat_axis=0, tiled=True, axis_...  5.98 us
    ppermute x1, starting transfers between devices, per_device(): mixed_out = kept + lax.ppermute(sent, 'tp', swap)  3.83 us
    pallas_call x1, Pallas kernels, per_device(): pl.pallas_call(functools.partial(pack_kernel, slots=slots), out_shape=plt...  2.31 us
    pallas_call x1, Pallas kernels, per_device(): pl.pallas_call(functools.partial(down_kernel, slots=slots), out_shape=plt...  1.48 us
  transfers between devices with their start and end apart: 14, of which 6 were waited for; matrix products, arithmetic and copies ran while one was open for 0% of the time, Pallas kernels for 11%

profile of v6, /device:TPU:1, one launch (start us, length us, event | category | flops | bytes accessed | tf_op | source)
XLA Modules:
  0.0 65.4 jit_solution(5365964397500984628)
XLA Ops:
  0.0 2.1 %collective-permute-start.1 = (bf16[2,64,2048]{2,1,0:T(8,128)(2,1)}, bf16[2,64,2048]{2,1,0:T(8,128)(2,1)S(1)}, u32[]{:S(2)}, u32[]{:S(2)}) collective-permute-start(bf16[2,64,2048]{2,1,0:T(8,128)(2,1)} %bitcast.14), channel_id=1, source_target_pairs={{0,6},{1,3},{2,0},{3,5},{4,2},{5,7},{6,4},{7,1},{8,14},{9,11},{10,... | collective-permute-start | bytes 1572872 | tf_op jit(solution)/shard_map/ppermute | solution.py:247
  2.1 1.3 %collective-permute-start.2 = (bf16[2,64,2048]{2,1,0:T(8,128)(2,1)}, bf16[2,64,2048]{2,1,0:T(8,128)(2,1)S(1)}, u32[]{:S(2)}, u32[]{:S(2)}) collective-permute-start(bf16[2,64,2048]{2,1,0:T(8,128)(2,1)} %bitcast.16), channel_id=1, source_target_pairs={{0,6},{1,3},{2,0},{3,5},{4,2},{5,7},{6,4},{7,1},{8,14},{9,11},{10,... | collective-permute-start | bytes 1572872 | tf_op jit(solution)/shard_map/ppermute | solution.py:247
  3.4 2.3 %pack.1 = bf16[256,1024]{1,0:T(8,128)(2,1)} custom-call(bf16[64,2048]{1,0:T(8,128)(2,1)} %tokens.1, f32[1,2048]{1,0:T(1,128)} %bitcast.18, f32[1,2048]{1,0:T(1,128)} %bitcast.19, s32[4,64]{1,0:T(4,128)} %bitcast.20), custom_call_target="tpu_custom_call" | custom-call | tf_op jit(solution)/shard_map/pack/pallas_call | solution.py:250
  5.7 11.9 %all-to-all-start = ((bf16[32,8,1024]{2,1,0:T(8,128)(2,1)}), bf16[32,8,1024]{2,1,0:T(8,128)(2,1)S(1)}, u32[]{:S(2)}, u32[]{:S(2)}) async-start(bf16[32,8,1024]{2,1,0:T(8,128)(2,1)} %bitcast.4), calls=%async_computation | async-start | bytes 1048576 | tf_op jit(solution)/shard_map/all_to_all | solution.py:273
  17.7 1.2 %theirs.1 = (bf16[2,64,2048]{2,1,0:T(8,128)(2,1)S(1)}, bf16[2,64,2048]{2,1,0:T(8,128)(2,1)S(1)}) custom-call(bf16[2,64,2048]{2,1,0:T(8,128)(2,1)} %bitcast.15, bf16[2,64,2048]{2,1,0:T(8,128)(2,1)} %bitcast.17), custom_call_target="tpu_custom_call" | custom-call | tf_op jit(solution)/shard_map/theirs/pallas_call | solution.py:278
  18.9 2.3 %collective-permute-start = (bf16[2,64,2048]{2,1,0:T(8,128)(2,1)S(1)}, bf16[2,64,2048]{2,1,0:T(8,128)(2,1)S(1)}, u32[]{:S(2)}, u32[]{:S(2)}) collective-permute-start(bf16[2,64,2048]{2,1,0:T(8,128)(2,1)S(1)} %get-tuple-element.20), channel_id=1, source_target_pairs={{0,1},{1,0},{2,3},{3,2},{4,5},{5,4},{6,7},{7,6},{8,9},{9,8},{10,11... | collective-permute-start | bytes 1572872 | tf_op jit(solution)/shard_map/ppermute | solution.py:247
  21.2 0.0 collective-permute-done.1.gate
  21.2 0.0 collective-permute-done.2.up
  21.2 0.9 %pick.1 = (bf16[2,64,2048]{2,1,0:T(8,128)(2,1)S(1)}, bf16[2,64,2048]{2,1,0:T(8,128)(2,1)}) custom-call(bf16[2,64,2048]{2,1,0:T(8,128)(2,1)S(1)} %collective-permute-done.1.gate, bf16[2,64,2048]{2,1,0:T(8,128)(2,1)S(1)} %collective-permute-done.2.up), custom_call_target="tpu_custom_call" | custom-call | tf_op jit(solution)/shard_map/pick/pallas_call | solution.py:289
  22.1 0.0 collective-permute-start.3
  22.1 1.1 %pieces.1 = (bf16[2,64,512]{2,1,0:T(8,128)(2,1)S(1)}, bf16[2,64,512]{2,1,0:T(8,128)(2,1)S(1)}, bf16[2,64,512]{2,1,0:T(8,128)(2,1)S(1)}, bf16[2,64,512]{2,1,0:T(8,128)(2,1)S(1)}) custom-call(bf16[2,64,2048]{2,1,0:T(8,128)(2,1)} %down.2), custom_call_target="tpu_custom_call" | custom-call | tf_op jit(solution)/shard_map/pieces/pallas_call | solution.py:300
  23.2 1.1 %collective-permute-start.7 = (bf16[2,64,512]{2,1,0:T(8,128)(2,1)S(1)}, bf16[2,64,512]{2,1,0:T(8,128)(2,1)S(1)}, u32[]{:S(2)}, u32[]{:S(2)}) collective-permute-start(bf16[2,64,512]{2,1,0:T(8,128)(2,1)S(1)} %get-tuple-element.24), channel_id=1, source_target_pairs={{0,2},{1,3},{2,0},{3,1},{4,6},{5,7},{6,4},{7,5},{8,10},{9,11},{10,... | collective-permute-start | bytes 393224 | tf_op jit(solution)/shard_map/ppermute | solution.py:247
  24.3 0.0 collective-permute-start.8
  24.3 2.2 %collective-permute-start.9 = (bf16[2,64,512]{2,1,0:T(8,128)(2,1)S(1)}, bf16[2,64,512]{2,1,0:T(8,128)(2,1)S(1)}, u32[]{:S(2)}, u32[]{:S(2)}) collective-permute-start(bf16[2,64,512]{2,1,0:T(8,128)(2,1)S(1)} %get-tuple-element.26), channel_id=1, source_target_pairs={{0,4},{1,5},{2,6},{3,7},{4,0},{5,1},{6,2},{7,3},{8,12},{9,13},{10,... | collective-permute-start | bytes 393224 | tf_op jit(solution)/shard_map/ppermute | solution.py:247
  26.6 1.3 %collective-permute-done.7.first = bf16[2,64,512]{2,1,0:T(8,128)(2,1)S(1)} collective-permute-done((bf16[2,64,512]{2,1,0:T(8,128)(2,1)S(1)}, bf16[2,64,512]{2,1,0:T(8,128)(2,1)S(1)}, u32[]{:S(2)}, u32[]{:S(2)}) %collective-permute-start.7) | collective-permute-done | bytes 131104 | tf_op jit(solution)/shard_map/ppermute | solution.py:247
  27.9 5.4 %collective-permute-done.8.second = bf16[2,64,512]{2,1,0:T(8,128)(2,1)S(1)} collective-permute-done((bf16[2,64,512]{2,1,0:T(8,128)(2,1)S(1)}, bf16[2,64,512]{2,1,0:T(8,128)(2,1)S(1)}, u32[]{:S(2)}, u32[]{:S(2)}) %collective-permute-start.8) | collective-permute-done | bytes 131104 | tf_op jit(solution)/shard_map/ppermute | solution.py:247
  33.3 0.0 collective-permute-done.9.third
  33.3 1.1 %collective-permute-start.10 = (bf16[4,64,512]{2,1,0:T(8,128)(2,1)S(1)}, bf16[4,64,512]{2,1,0:T(8,128)(2,1)}, u32[]{:S(2)}, u32[]{:S(2)}) collective-permute-start(bf16[4,64,512]{2,1,0:T(8,128)(2,1)S(1)} %give.1), channel_id=1, source_target_pairs={{0,1},{1,0},{2,3},{3,2},{4,5},{5,4},{6,7},{7,6},{8,9},{9,8},{10,11... | collective-permute-start | bytes 786440 | tf_op jit(solution)/shard_map/ppermute | solution.py:247
  34.4 0.0 collective-permute-done.swapped
  34.4 0.0 all-to-all-done
  34.4 0.0 collective-permute-done.3.passed
  34.4 1.0 %hidden.1.h_own = bf16[128,256]{1,0:T(8,128)(2,1)S(1)} custom-call(bf16[256,1024]{1,0:T(8,128)(2,1)S(1)} %bitcast.13, bf16[2,64,2048]{2,1,0:T(8,128)(2,1)S(1)} %get-tuple-element.19.mine, bf16[2,64,2048]{2,1,0:T(8,128)(2,1)S(1)} %collective-permute-done.swapped, bf16[2,64,2048]{2,1,0:T(8,128)(2,1)S(1)} %get-tuple-element.21.kept_in, ...), custom_call_target="tpu_custom_call" | custom-call | tf_op jit(solution)/shard_map/hidden/pallas_call | solution.py:321
  35.4 0.1 collective-permute-start.4
  35.5 0.6 collective-permute-start.5
  36.1 2.7 %collective-permute-start.6 = (bf16[128,256]{1,0:T(8,128)(2,1)S(1)}, bf16[128,256]{1,0:T(8,128)(2,1)S(1)}, u32[]{:S(2)}, u32[]{:S(2)}) collective-permute-start(bf16[128,256]{1,0:T(8,128)(2,1)S(1)} %hidden.1.h_own), channel_id=1, source_target_pairs={{0,4},{1,5},{2,6},{3,7},{4,0},{5,1},{6,2},{7,3},{8,12},{9,13},{10,... | collective-permute-start | bytes 196616 | tf_op jit(solution)/shard_map/ppermute | solution.py:247
  38.7 0.0 collective-permute-done.10.other
  38.7 0.4 collective-permute-done.4.h_first
  39.1 2.0 %collective-permute-done.5.h_second = bf16[128,256]{1,0:T(8,128)(2,1)S(1)} collective-permute-done((bf16[128,256]{1,0:T(8,128)(2,1)S(1)}, bf16[128,256]{1,0:T(8,128)(2,1)S(1)}, u32[]{:S(2)}, u32[]{:S(2)}) %collective-permute-start.5) | collective-permute-done | bytes 65568 | tf_op jit(solution)/shard_map/ppermute | solution.py:247
  41.1 0.0 collective-permute-done.6.h_third
  41.1 1.5 %down.3 = f32[256,640]{1,0:T(8,128)S(1)} custom-call(bf16[128,256]{1,0:T(8,128)(2,1)S(1)} %hidden.1.h_own, bf16[128,256]{1,0:T(8,128)(2,1)S(1)} %collective-permute-done.4.h_first, bf16[128,256]{1,0:T(8,128)(2,1)S(1)} %collective-permute-done.5.h_second, bf16[128,256]{1,0:T(8,128)(2,1)S(1)} %collective-permute-done.6.h_third, ...), custom_call_target="tpu_custom_call" | custom-call | tf_op jit(solution)/shard_map/down/pallas_call | solution.py:331
  42.6 0.8 %convert_bitcast_fusion = f16[32,8,640]{2,1,0:T(8,128)(2,1)} fusion(f32[256,640]{1,0:T(8,128)S(1)} %down.3), kind=kLoop, calls=%fused_computation.1 | loop fusion | flops 163840 | bytes 983040 | tf_op jit(solution)/shard_map/reshape | solution.py:339
  43.4 9.4 %all-to-all-start.1 = ((f16[32,8,640]{2,1,0:T(8,128)(2,1)}), f16[32,8,640]{2,1,0:T(8,128)(2,1)S(1)}, u32[]{:S(2)}, u32[]{:S(2)}) async-start(f16[32,8,640]{2,1,0:T(8,128)(2,1)} %convert_bitcast_fusion), calls=%async_computation.1 | async-start | bytes 655360 | tf_op jit(solution)/shard_map/all_to_all | solution.py:340
  52.8 0.9 %factors.1 = (bf16[256,64]{1,0:T(8,128)(2,1)S(1)}, bf16[256,64]{1,0:T(8,128)(2,1)S(1)}) custom-call(s32[4,64]{1,0:T(4,128)} %bitcast.21, f32[4,64]{1,0:T(4,128)} %bitcast.22), custom_call_target="tpu_custom_call" | custom-call | tf_op jit(solution)/shard_map/factors/pallas_call | solution.py:263
  53.7 6.0 %all-to-all-done.1 = f16[32,8,640]{2,1,0:T(8,128)(2,1)S(1)} async-done(((f16[32,8,640]{2,1,0:T(8,128)(2,1)}), f16[32,8,640]{2,1,0:T(8,128)(2,1)S(1)}, u32[]{:S(2)}, u32[]{:S(2)}) %all-to-all-start.1) | async-done | bytes 327712 | tf_op jit(solution)/shard_map/all_to_all | solution.py:340
  59.7 0.3 combine.1
  60.0 3.8 %collective-permute-start.11 = (f32[64,256]{1,0:T(8,128)S(1)}, f32[64,256]{1,0:T(8,128)S(1)}, u32[]{:S(2)}, u32[]{:S(2)}) collective-permute-start(f32[64,256]{1,0:T(8,128)S(1)} %get-tuple-element.28), channel_id=1, source_target_pairs={{0,1},{1,0},{2,3},{3,2},{4,5},{5,4},{6,7},{7,6},{8,9},{9,8},{10,11... | collective-permute-start | bytes 196616 | tf_op jit(solution)/shard_map/ppermute | solution.py:351
  63.9 0.9 %collective-permute-done.11 = f32[64,256]{1,0:T(8,128)S(1)} collective-permute-done((f32[64,256]{1,0:T(8,128)S(1)}, f32[64,256]{1,0:T(8,128)S(1)}, u32[]{:S(2)}, u32[]{:S(2)}) %collective-permute-start.11) | collective-permute-done | bytes 65568 | tf_op jit(solution)/shard_map/ppermute | solution.py:351
  64.8 0.6 add_convert_fusion
  (2 shorter events, 0.1 us)
Async XLA Ops:
  0.0 21.2 %collective-permute-start.1 = (bf16[2,64,2048]{2,1,0:T(8,128)(2,1)}, bf16[2,64,2048]{2,1,0:T(8,128)(2,1)S(1)}, u32[]{:S(2)}, u32[]{:S(2)}) collective-permute-start(bf16[2,64,2048]{2,1,0:T(8,128)(2,1)} %bitcast.14), channel_id=1, source_target_pairs={{0,6},{1,3},{2,0},{3,5},{4,2},{5,7},{6,4},{7,1},{8,14},{9,11},{10,... | collective-permute-start | bytes 1572872 | tf_op jit(solution)/shard_map/ppermute | solution.py:247
  2.1 19.1 %collective-permute-start.2 = (bf16[2,64,2048]{2,1,0:T(8,128)(2,1)}, bf16[2,64,2048]{2,1,0:T(8,128)(2,1)S(1)}, u32[]{:S(2)}, u32[]{:S(2)}) collective-permute-start(bf16[2,64,2048]{2,1,0:T(8,128)(2,1)} %bitcast.16), channel_id=1, source_target_pairs={{0,6},{1,3},{2,0},{3,5},{4,2},{5,7},{6,4},{7,1},{8,14},{9,11},{10,... | collective-permute-start | bytes 1572872 | tf_op jit(solution)/shard_map/ppermute | solution.py:247
  5.7 28.6 %all-to-all-start = ((bf16[32,8,1024]{2,1,0:T(8,128)(2,1)}), bf16[32,8,1024]{2,1,0:T(8,128)(2,1)S(1)}, u32[]{:S(2)}, u32[]{:S(2)}) async-start(bf16[32,8,1024]{2,1,0:T(8,128)(2,1)} %bitcast.4), calls=%async_computation | async-start | bytes 1048576 | tf_op jit(solution)/shard_map/all_to_all | solution.py:273
  18.9 15.5 %collective-permute-start = (bf16[2,64,2048]{2,1,0:T(8,128)(2,1)S(1)}, bf16[2,64,2048]{2,1,0:T(8,128)(2,1)S(1)}, u32[]{:S(2)}, u32[]{:S(2)}) collective-permute-start(bf16[2,64,2048]{2,1,0:T(8,128)(2,1)S(1)} %get-tuple-element.20), channel_id=1, source_target_pairs={{0,1},{1,0},{2,3},{3,2},{4,5},{5,4},{6,7},{7,6},{8,9},{9,8},{10,11... | collective-permute-start | bytes 1572872 | tf_op jit(solution)/shard_map/ppermute | solution.py:247
  22.1 12.3 %collective-permute-start.3 = (bf16[2,64,2048]{2,1,0:T(8,128)(2,1)}, bf16[2,64,2048]{2,1,0:T(8,128)(2,1)S(1)}, u32[]{:S(2)}, u32[]{:S(2)}) collective-permute-start(bf16[2,64,2048]{2,1,0:T(8,128)(2,1)} %get-tuple-element.22), channel_id=1, source_target_pairs={{0,1},{1,0},{2,3},{3,2},{4,5},{5,4},{6,7},{7,6},{8,9},{9,8},{10,11... | collective-permute-start | bytes 1572872 | tf_op jit(solution)/shard_map/ppermute | solution.py:247
  23.2 4.7 %collective-permute-start.7 = (bf16[2,64,512]{2,1,0:T(8,128)(2,1)S(1)}, bf16[2,64,512]{2,1,0:T(8,128)(2,1)S(1)}, u32[]{:S(2)}, u32[]{:S(2)}) collective-permute-start(bf16[2,64,512]{2,1,0:T(8,128)(2,1)S(1)} %get-tuple-element.24), channel_id=1, source_target_pairs={{0,2},{1,3},{2,0},{3,1},{4,6},{5,7},{6,4},{7,5},{8,10},{9,11},{10,... | collective-permute-start | bytes 393224 | tf_op jit(solution)/shard_map/ppermute | solution.py:247
  24.3 9.0 %collective-permute-start.8 = (bf16[2,64,512]{2,1,0:T(8,128)(2,1)S(1)}, bf16[2,64,512]{2,1,0:T(8,128)(2,1)S(1)}, u32[]{:S(2)}, u32[]{:S(2)}) collective-permute-start(bf16[2,64,512]{2,1,0:T(8,128)(2,1)S(1)} %get-tuple-element.25), channel_id=1, source_target_pairs={{0,6},{1,7},{2,4},{3,5},{4,2},{5,3},{6,0},{7,1},{8,14},{9,15},{10,... | collective-permute-start | bytes 393224 | tf_op jit(solution)/shard_map/ppermute | solution.py:247
  24.3 9.0 %collective-permute-start.9 = (bf16[2,64,512]{2,1,0:T(8,128)(2,1)S(1)}, bf16[2,64,512]{2,1,0:T(8,128)(2,1)S(1)}, u32[]{:S(2)}, u32[]{:S(2)}) collective-permute-start(bf16[2,64,512]{2,1,0:T(8,128)(2,1)S(1)} %get-tuple-element.26), channel_id=1, source_target_pairs={{0,4},{1,5},{2,6},{3,7},{4,0},{5,1},{6,2},{7,3},{8,12},{9,13},{10,... | collective-permute-start | bytes 393224 | tf_op jit(solution)/shard_map/ppermute | solution.py:247
  33.3 5.4 %collective-permute-start.10 = (bf16[4,64,512]{2,1,0:T(8,128)(2,1)S(1)}, bf16[4,64,512]{2,1,0:T(8,128)(2,1)}, u32[]{:S(2)}, u32[]{:S(2)}) collective-permute-start(bf16[4,64,512]{2,1,0:T(8,128)(2,1)S(1)} %give.1), channel_id=1, source_target_pairs={{0,1},{1,0},{2,3},{3,2},{4,5},{5,4},{6,7},{7,6},{8,9},{9,8},{10,11... | collective-permute-start | bytes 786440 | tf_op jit(solution)/shard_map/ppermute | solution.py:247
  35.4 3.7 %collective-permute-start.4 = (bf16[128,256]{1,0:T(8,128)(2,1)S(1)}, bf16[128,256]{1,0:T(8,128)(2,1)S(1)}, u32[]{:S(2)}, u32[]{:S(2)}) collective-permute-start(bf16[128,256]{1,0:T(8,128)(2,1)S(1)} %hidden.1.h_own), channel_id=1, source_target_pairs={{0,2},{1,3},{2,0},{3,1},{4,6},{5,7},{6,4},{7,5},{8,10},{9,11},{10,... | collective-permute-start | bytes 196616 | tf_op jit(solution)/shard_map/ppermute | solution.py:247
  35.5 5.6 %collective-permute-start.5 = (bf16[128,256]{1,0:T(8,128)(2,1)S(1)}, bf16[128,256]{1,0:T(8,128)(2,1)S(1)}, u32[]{:S(2)}, u32[]{:S(2)}) collective-permute-start(bf16[128,256]{1,0:T(8,128)(2,1)S(1)} %hidden.1.h_own), channel_id=1, source_target_pairs={{0,6},{1,7},{2,4},{3,5},{4,2},{5,3},{6,0},{7,1},{8,14},{9,15},{10,... | collective-permute-start | bytes 196616 | tf_op jit(solution)/shard_map/ppermute | solution.py:247
  36.1 5.1 %collective-permute-start.6 = (bf16[128,256]{1,0:T(8,128)(2,1)S(1)}, bf16[128,256]{1,0:T(8,128)(2,1)S(1)}, u32[]{:S(2)}, u32[]{:S(2)}) collective-permute-start(bf16[128,256]{1,0:T(8,128)(2,1)S(1)} %hidden.1.h_own), channel_id=1, source_target_pairs={{0,4},{1,5},{2,6},{3,7},{4,0},{5,1},{6,2},{7,3},{8,12},{9,13},{10,... | collective-permute-start | bytes 196616 | tf_op jit(solution)/shard_map/ppermute | solution.py:247
  43.4 16.3 %all-to-all-start.1 = ((f16[32,8,640]{2,1,0:T(8,128)(2,1)}), f16[32,8,640]{2,1,0:T(8,128)(2,1)S(1)}, u32[]{:S(2)}, u32[]{:S(2)}) async-start(f16[32,8,640]{2,1,0:T(8,128)(2,1)} %convert_bitcast_fusion), calls=%async_computation.1 | async-start | bytes 655360 | tf_op jit(solution)/shard_map/all_to_all | solution.py:340
  60.0 4.7 %collective-permute-start.11 = (f32[64,256]{1,0:T(8,128)S(1)}, f32[64,256]{1,0:T(8,128)S(1)}, u32[]{:S(2)}, u32[]{:S(2)}) collective-permute-start(f32[64,256]{1,0:T(8,128)S(1)} %get-tuple-element.28), channel_id=1, source_target_pairs={{0,1},{1,0},{2,3},{3,2},{4,5},{5,4},{6,7},{7,6},{8,9},{9,8},{10,11... | collective-permute-start | bytes 196616 | tf_op jit(solution)/shard_map/ppermute | solution.py:351

commit v7 on v6

--- a/solution.py
+++ b/solution.py
@@ -72,7 +72,7 @@
 
 
 def member(place):
-    return (MEMBERS - 1 - SPAN - place) % MEMBERS
+    return (MEMBERS - 1 - 2 * SPAN - place) % MEMBERS
 
 
 def slots_of(ids, core, experts, copies):
@@ -327,7 +327,9 @@
         name="hidden",
     )(*on_chip(arrived, mine, swapped, kept, passed))
     h_across = ppermute(hidden, across)
-    hiddens = [hidden, ppermute(hidden, near), ppermute(hidden, same), h_across]
+    h_near = ppermute(hidden, near)
+    h_same = ppermute(hidden, same)
+    hiddens = [hidden, h_near, h_same, h_across]
     result = pl.pallas_call(
         functools.partial(down_kernel, slots=slots),
         out_shape=pltpu.VMEM((rows, share + LANES), jnp.float32),

time: 65.7 us -> 65.2 us (level)
  starting transfers between devices: 38.6 us -> 37.5 us
    ppermute x1, starting transfers between devices: 3.83 us -> 2.33 us  [per_device(): mixed_out = kept + lax.ppermute(sent, 'tp', swap)]
where the time goes in v7:
time: 65.2 us; the launch traced here: 64.9 us
  starting transfers between devices  37.5 us (58%)
  waiting for transfers between devices  16.5 us (25%)
  Pallas kernels  9.28 us (14%)
  other arithmetic  1.44 us (2%)
    ppermute x11, starting transfers between devices, ppermute(): return lax.ppermute(array, 'tp', pairs)  13.5 us
    all_to_all x1, starting transfers between devices, per_device(): lax.all_to_all(packed.reshape(ep_size, slots, features // 2), 'ep', split...  12.3 us
    all_to_all x1, starting transfers between devices, per_device(): lax.all_to_all(wire, 'ep', split_axis=0, concat_axis=0, tiled=True, axis_...  9.36 us
    ppermute x11, waiting for transfers between devices, ppermute(): return lax.ppermute(array, 'tp', pairs)  9.1 us
    all_to_all x1, waiting for transfers between devices, per_device(): lax.all_to_all(wire, 'ep', split_axis=0, concat_axis=0, tiled=True, axis_...  6.55 us
    ppermute x1, starting transfers between devices, per_device(): mixed_out = kept + lax.ppermute(sent, 'tp', swap)  2.33 us
    pallas_call x1, Pallas kernels, per_device(): pl.pallas_call(functools.partial(pack_kernel, slots=slots), out_shape=plt...  2.31 us
    pallas_call x1, Pallas kernels, per_device(): pl.pallas_call(functools.partial(down_kernel, slots=slots), out_shape=plt...  1.48 us
  transfers between devices with their start and end apart: 14, of which 6 were waited for; matrix products, arithmetic and copies ran while one was open for 0% of the time, Pallas kernels for 11%

profile of v7, /device:TPU:1, one launch (start us, length us, event | category | flops | bytes accessed | tf_op | source)
XLA Modules:
  0.0 64.9 jit_solution(11830839128163606174)
XLA Ops:
  0.0 2.1 %collective-permute-start.1 = (bf16[2,64,2048]{2,1,0:T(8,128)(2,1)}, bf16[2,64,2048]{2,1,0:T(8,128)(2,1)S(1)}, u32[]{:S(2)}, u32[]{:S(2)}) collective-permute-start(bf16[2,64,2048]{2,1,0:T(8,128)(2,1)} %bitcast.14), channel_id=1, source_target_pairs={{0,6},{1,3},{2,0},{3,5},{4,2},{5,7},{6,4},{7,1},{8,14},{9,11},{10,... | collective-permute-start | bytes 1572872 | tf_op jit(solution)/shard_map/ppermute | solution.py:247
  2.1 1.3 %collective-permute-start.2 = (bf16[2,64,2048]{2,1,0:T(8,128)(2,1)}, bf16[2,64,2048]{2,1,0:T(8,128)(2,1)S(1)}, u32[]{:S(2)}, u32[]{:S(2)}) collective-permute-start(bf16[2,64,2048]{2,1,0:T(8,128)(2,1)} %bitcast.16), channel_id=1, source_target_pairs={{0,6},{1,3},{2,0},{3,5},{4,2},{5,7},{6,4},{7,1},{8,14},{9,11},{10,... | collective-permute-start | bytes 1572872 | tf_op jit(solution)/shard_map/ppermute | solution.py:247
  3.4 2.3 %pack.1 = bf16[256,1024]{1,0:T(8,128)(2,1)} custom-call(bf16[64,2048]{1,0:T(8,128)(2,1)} %tokens.1, f32[1,2048]{1,0:T(1,128)} %bitcast.18, f32[1,2048]{1,0:T(1,128)} %bitcast.19, s32[4,64]{1,0:T(4,128)} %bitcast.20), custom_call_target="tpu_custom_call" | custom-call | tf_op jit(solution)/shard_map/pack/pallas_call | solution.py:250
  5.7 12.3 %all-to-all-start = ((bf16[32,8,1024]{2,1,0:T(8,128)(2,1)}), bf16[32,8,1024]{2,1,0:T(8,128)(2,1)S(1)}, u32[]{:S(2)}, u32[]{:S(2)}) async-start(bf16[32,8,1024]{2,1,0:T(8,128)(2,1)} %bitcast.4), calls=%async_computation | async-start | bytes 1048576 | tf_op jit(solution)/shard_map/all_to_all | solution.py:273
  18.1 1.2 %theirs.1 = (bf16[2,64,2048]{2,1,0:T(8,128)(2,1)S(1)}, bf16[2,64,2048]{2,1,0:T(8,128)(2,1)S(1)}) custom-call(bf16[2,64,2048]{2,1,0:T(8,128)(2,1)} %bitcast.15, bf16[2,64,2048]{2,1,0:T(8,128)(2,1)} %bitcast.17), custom_call_target="tpu_custom_call" | custom-call | tf_op jit(solution)/shard_map/theirs/pallas_call | solution.py:278
  19.3 2.3 %collective-permute-start = (bf16[2,64,2048]{2,1,0:T(8,128)(2,1)S(1)}, bf16[2,64,2048]{2,1,0:T(8,128)(2,1)S(1)}, u32[]{:S(2)}, u32[]{:S(2)}) collective-permute-start(bf16[2,64,2048]{2,1,0:T(8,128)(2,1)S(1)} %get-tuple-element.20), channel_id=1, source_target_pairs={{0,1},{1,0},{2,3},{3,2},{4,5},{5,4},{6,7},{7,6},{8,9},{9,8},{10,11... | collective-permute-start | bytes 1572872 | tf_op jit(solution)/shard_map/ppermute | solution.py:247
  21.6 0.0 collective-permute-done.1.gate
  21.6 0.0 collective-permute-done.2.up
  21.6 0.9 %pick.1 = (bf16[2,64,2048]{2,1,0:T(8,128)(2,1)S(1)}, bf16[2,64,2048]{2,1,0:T(8,128)(2,1)}) custom-call(bf16[2,64,2048]{2,1,0:T(8,128)(2,1)S(1)} %collective-permute-done.1.gate, bf16[2,64,2048]{2,1,0:T(8,128)(2,1)S(1)} %collective-permute-done.2.up), custom_call_target="tpu_custom_call" | custom-call | tf_op jit(solution)/shard_map/pick/pallas_call | solution.py:289
  22.5 0.0 collective-permute-start.3
  22.5 1.1 %pieces.1 = (bf16[2,64,512]{2,1,0:T(8,128)(2,1)S(1)}, bf16[2,64,512]{2,1,0:T(8,128)(2,1)S(1)}, bf16[2,64,512]{2,1,0:T(8,128)(2,1)S(1)}, bf16[2,64,512]{2,1,0:T(8,128)(2,1)S(1)}) custom-call(bf16[2,64,2048]{2,1,0:T(8,128)(2,1)} %down.2), custom_call_target="tpu_custom_call" | custom-call | tf_op jit(solution)/shard_map/pieces/pallas_call | solution.py:300
  23.7 1.1 %collective-permute-start.7 = (bf16[2,64,512]{2,1,0:T(8,128)(2,1)S(1)}, bf16[2,64,512]{2,1,0:T(8,128)(2,1)S(1)}, u32[]{:S(2)}, u32[]{:S(2)}) collective-permute-start(bf16[2,64,512]{2,1,0:T(8,128)(2,1)S(1)} %get-tuple-element.24), channel_id=1, source_target_pairs={{0,2},{1,3},{2,0},{3,1},{4,6},{5,7},{6,4},{7,5},{8,10},{9,11},{10,... | collective-permute-start | bytes 393224 | tf_op jit(solution)/shard_map/ppermute | solution.py:247
  24.8 0.0 collective-permute-start.8
  24.8 2.2 %collective-permute-start.9 = (bf16[2,64,512]{2,1,0:T(8,128)(2,1)S(1)}, bf16[2,64,512]{2,1,0:T(8,128)(2,1)S(1)}, u32[]{:S(2)}, u32[]{:S(2)}) collective-permute-start(bf16[2,64,512]{2,1,0:T(8,128)(2,1)S(1)} %get-tuple-element.26), channel_id=1, source_target_pairs={{0,4},{1,5},{2,6},{3,7},{4,0},{5,1},{6,2},{7,3},{8,12},{9,13},{10,... | collective-permute-start | bytes 393224 | tf_op jit(solution)/shard_map/ppermute | solution.py:247
  27.0 1.3 %collective-permute-done.7.first = bf16[2,64,512]{2,1,0:T(8,128)(2,1)S(1)} collective-permute-done((bf16[2,64,512]{2,1,0:T(8,128)(2,1)S(1)}, bf16[2,64,512]{2,1,0:T(8,128)(2,1)S(1)}, u32[]{:S(2)}, u32[]{:S(2)}) %collective-permute-start.7) | collective-permute-done | bytes 131104 | tf_op jit(solution)/shard_map/ppermute | solution.py:247
  28.3 5.4 %collective-permute-done.8.second = bf16[2,64,512]{2,1,0:T(8,128)(2,1)S(1)} collective-permute-done((bf16[2,64,512]{2,1,0:T(8,128)(2,1)S(1)}, bf16[2,64,512]{2,1,0:T(8,128)(2,1)S(1)}, u32[]{:S(2)}, u32[]{:S(2)}) %collective-permute-start.8) | collective-permute-done | bytes 131104 | tf_op jit(solution)/shard_map/ppermute | solution.py:247
  33.7 0.0 collective-permute-done.9.third
  33.7 1.1 %collective-permute-start.10 = (bf16[4,64,512]{2,1,0:T(8,128)(2,1)S(1)}, bf16[4,64,512]{2,1,0:T(8,128)(2,1)}, u32[]{:S(2)}, u32[]{:S(2)}) collective-permute-start(bf16[4,64,512]{2,1,0:T(8,128)(2,1)S(1)} %give.1), channel_id=1, source_target_pairs={{0,1},{1,0},{2,3},{3,2},{4,5},{5,4},{6,7},{7,6},{8,9},{9,8},{10,11... | collective-permute-start | bytes 786440 | tf_op jit(solution)/shard_map/ppermute | solution.py:247
  34.8 0.0 collective-permute-done.swapped
  34.8 0.0 all-to-all-done
  34.8 0.0 collective-permute-done.3.passed
  34.8 1.0 %hidden.1.h_own = bf16[128,256]{1,0:T(8,128)(2,1)S(1)} custom-call(bf16[256,1024]{1,0:T(8,128)(2,1)S(1)} %bitcast.13, bf16[2,64,2048]{2,1,0:T(8,128)(2,1)S(1)} %get-tuple-element.19.mine, bf16[2,64,2048]{2,1,0:T(8,128)(2,1)S(1)} %collective-permute-done.swapped, bf16[2,64,2048]{2,1,0:T(8,128)(2,1)S(1)} %get-tuple-element.21.kept_in, ...), custom_call_target="tpu_custom_call" | custom-call | tf_op jit(solution)/shard_map/hidden/pallas_call | solution.py:321
  35.8 0.1 collective-permute-start.4
  35.9 0.6 collective-permute-start.5
  36.5 2.7 %collective-permute-start.6 = (bf16[128,256]{1,0:T(8,128)(2,1)S(1)}, bf16[128,256]{1,0:T(8,128)(2,1)S(1)}, u32[]{:S(2)}, u32[]{:S(2)}) collective-permute-start(bf16[128,256]{1,0:T(8,128)(2,1)S(1)} %hidden.1.h_own), channel_id=1, source_target_pairs={{0,4},{1,5},{2,6},{3,7},{4,0},{5,1},{6,2},{7,3},{8,12},{9,13},{10,... | collective-permute-start | bytes 196616 | tf_op jit(solution)/shard_map/ppermute | solution.py:247
  39.2 0.0 collective-permute-done.10.other
  39.2 0.4 collective-permute-done.4.h_first
  39.5 2.0 %collective-permute-done.5.h_second = bf16[128,256]{1,0:T(8,128)(2,1)S(1)} collective-permute-done((bf16[128,256]{1,0:T(8,128)(2,1)S(1)}, bf16[128,256]{1,0:T(8,128)(2,1)S(1)}, u32[]{:S(2)}, u32[]{:S(2)}) %collective-permute-start.5) | collective-permute-done | bytes 65568 | tf_op jit(solution)/shard_map/ppermute | solution.py:247
  41.6 0.0 collective-permute-done.6.h_third
  41.6 1.5 %down.3 = f32[256,640]{1,0:T(8,128)S(1)} custom-call(bf16[128,256]{1,0:T(8,128)(2,1)S(1)} %hidden.1.h_own, bf16[128,256]{1,0:T(8,128)(2,1)S(1)} %collective-permute-done.4.h_first, bf16[128,256]{1,0:T(8,128)(2,1)S(1)} %collective-permute-done.5.h_second, bf16[128,256]{1,0:T(8,128)(2,1)S(1)} %collective-permute-done.6.h_third, ...), custom_call_target="tpu_custom_call" | custom-call | tf_op jit(solution)/shard_map/down/pallas_call | solution.py:333
  43.0 0.8 %convert_bitcast_fusion = f16[32,8,640]{2,1,0:T(8,128)(2,1)} fusion(f32[256,640]{1,0:T(8,128)S(1)} %down.3), kind=kLoop, calls=%fused_computation.1 | loop fusion | flops 163840 | bytes 983040 | tf_op jit(solution)/shard_map/reshape | solution.py:341
  43.8 9.4 %all-to-all-start.1 = ((f16[32,8,640]{2,1,0:T(8,128)(2,1)}), f16[32,8,640]{2,1,0:T(8,128)(2,1)S(1)}, u32[]{:S(2)}, u32[]{:S(2)}) async-start(f16[32,8,640]{2,1,0:T(8,128)(2,1)} %convert_bitcast_fusion), calls=%async_computation.1 | async-start | bytes 655360 | tf_op jit(solution)/shard_map/all_to_all | solution.py:342
  53.2 0.9 %factors.1 = (bf16[256,64]{1,0:T(8,128)(2,1)S(1)}, bf16[256,64]{1,0:T(8,128)(2,1)S(1)}) custom-call(s32[4,64]{1,0:T(4,128)} %bitcast.21, f32[4,64]{1,0:T(4,128)} %bitcast.22), custom_call_target="tpu_custom_call" | custom-call | tf_op jit(solution)/shard_map/factors/pallas_call | solution.py:263
  54.1 6.5 %all-to-all-done.1 = f16[32,8,640]{2,1,0:T(8,128)(2,1)S(1)} async-done(((f16[32,8,640]{2,1,0:T(8,128)(2,1)}), f16[32,8,640]{2,1,0:T(8,128)(2,1)S(1)}, u32[]{:S(2)}, u32[]{:S(2)}) %all-to-all-start.1) | async-done | bytes 327712 | tf_op jit(solution)/shard_map/all_to_all | solution.py:342
  60.7 0.3 combine.1
  61.0 2.3 %collective-permute-start.11 = (f32[64,256]{1,0:T(8,128)S(1)}, f32[64,256]{1,0:T(8,128)S(1)}, u32[]{:S(2)}, u32[]{:S(2)}) collective-permute-start(f32[64,256]{1,0:T(8,128)S(1)} %get-tuple-element.28), channel_id=1, source_target_pairs={{0,1},{1,0},{2,3},{3,2},{4,5},{5,4},{6,7},{7,6},{8,9},{9,8},{10,11... | collective-permute-start | bytes 196616 | tf_op jit(solution)/shard_map/ppermute | solution.py:353
  63.3 0.9 %collective-permute-done.11 = f32[64,256]{1,0:T(8,128)S(1)} collective-permute-done((f32[64,256]{1,0:T(8,128)S(1)}, f32[64,256]{1,0:T(8,128)S(1)}, u32[]{:S(2)}, u32[]{:S(2)}) %collective-permute-start.11) | collective-permute-done | bytes 65568 | tf_op jit(solution)/shard_map/ppermute | solution.py:353
  64.2 0.6 add_convert_fusion
  (2 shorter events, 0.1 us)
Async XLA Ops:
  0.0 21.6 %collective-permute-start.1 = (bf16[2,64,2048]{2,1,0:T(8,128)(2,1)}, bf16[2,64,2048]{2,1,0:T(8,128)(2,1)S(1)}, u32[]{:S(2)}, u32[]{:S(2)}) collective-permute-start(bf16[2,64,2048]{2,1,0:T(8,128)(2,1)} %bitcast.14), channel_id=1, source_target_pairs={{0,6},{1,3},{2,0},{3,5},{4,2},{5,7},{6,4},{7,1},{8,14},{9,11},{10,... | collective-permute-start | bytes 1572872 | tf_op jit(solution)/shard_map/ppermute | solution.py:247
  2.1 19.5 %collective-permute-start.2 = (bf16[2,64,2048]{2,1,0:T(8,128)(2,1)}, bf16[2,64,2048]{2,1,0:T(8,128)(2,1)S(1)}, u32[]{:S(2)}, u32[]{:S(2)}) collective-permute-start(bf16[2,64,2048]{2,1,0:T(8,128)(2,1)} %bitcast.16), channel_id=1, source_target_pairs={{0,6},{1,3},{2,0},{3,5},{4,2},{5,7},{6,4},{7,1},{8,14},{9,11},{10,... | collective-permute-start | bytes 1572872 | tf_op jit(solution)/shard_map/ppermute | solution.py:247
  5.7 29.1 %all-to-all-start = ((bf16[32,8,1024]{2,1,0:T(8,128)(2,1)}), bf16[32,8,1024]{2,1,0:T(8,128)(2,1)S(1)}, u32[]{:S(2)}, u32[]{:S(2)}) async-start(bf16[32,8,1024]{2,1,0:T(8,128)(2,1)} %bitcast.4), calls=%async_computation | async-start | bytes 1048576 | tf_op jit(solution)/shard_map/all_to_all | solution.py:273
  19.3 15.5 %collective-permute-start = (bf16[2,64,2048]{2,1,0:T(8,128)(2,1)S(1)}, bf16[2,64,2048]{2,1,0:T(8,128)(2,1)S(1)}, u32[]{:S(2)}, u32[]{:S(2)}) collective-permute-start(bf16[2,64,2048]{2,1,0:T(8,128)(2,1)S(1)} %get-tuple-element.20), channel_id=1, source_target_pairs={{0,1},{1,0},{2,3},{3,2},{4,5},{5,4},{6,7},{7,6},{8,9},{9,8},{10,11... | collective-permute-start | bytes 1572872 | tf_op jit(solution)/shard_map/ppermute | solution.py:247
  22.5 12.3 %collective-permute-start.3 = (bf16[2,64,2048]{2,1,0:T(8,128)(2,1)}, bf16[2,64,2048]{2,1,0:T(8,128)(2,1)S(1)}, u32[]{:S(2)}, u32[]{:S(2)}) collective-permute-start(bf16[2,64,2048]{2,1,0:T(8,128)(2,1)} %get-tuple-element.22), channel_id=1, source_target_pairs={{0,1},{1,0},{2,3},{3,2},{4,5},{5,4},{6,7},{7,6},{8,9},{9,8},{10,11... | collective-permute-start | bytes 1572872 | tf_op jit(solution)/shard_map/ppermute | solution.py:247
  23.7 4.7 %collective-permute-start.7 = (bf16[2,64,512]{2,1,0:T(8,128)(2,1)S(1)}, bf16[2,64,512]{2,1,0:T(8,128)(2,1)S(1)}, u32[]{:S(2)}, u32[]{:S(2)}) collective-permute-start(bf16[2,64,512]{2,1,0:T(8,128)(2,1)S(1)} %get-tuple-element.24), channel_id=1, source_target_pairs={{0,2},{1,3},{2,0},{3,1},{4,6},{5,7},{6,4},{7,5},{8,10},{9,11},{10,... | collective-permute-start | bytes 393224 | tf_op jit(solution)/shard_map/ppermute | solution.py:247
  24.8 9.0 %collective-permute-start.8 = (bf16[2,64,512]{2,1,0:T(8,128)(2,1)S(1)}, bf16[2,64,512]{2,1,0:T(8,128)(2,1)S(1)}, u32[]{:S(2)}, u32[]{:S(2)}) collective-permute-start(bf16[2,64,512]{2,1,0:T(8,128)(2,1)S(1)} %get-tuple-element.25), channel_id=1, source_target_pairs={{0,6},{1,7},{2,4},{3,5},{4,2},{5,3},{6,0},{7,1},{8,14},{9,15},{10,... | collective-permute-start | bytes 393224 | tf_op jit(solution)/shard_map/ppermute | solution.py:247
  24.8 9.0 %collective-permute-start.9 = (bf16[2,64,512]{2,1,0:T(8,128)(2,1)S(1)}, bf16[2,64,512]{2,1,0:T(8,128)(2,1)S(1)}, u32[]{:S(2)}, u32[]{:S(2)}) collective-permute-start(bf16[2,64,512]{2,1,0:T(8,128)(2,1)S(1)} %get-tuple-element.26), channel_id=1, source_target_pairs={{0,4},{1,5},{2,6},{3,7},{4,0},{5,1},{6,2},{7,3},{8,12},{9,13},{10,... | collective-permute-start | bytes 393224 | tf_op jit(solution)/shard_map/ppermute | solution.py:247
  33.7 5.4 %collective-permute-start.10 = (bf16[4,64,512]{2,1,0:T(8,128)(2,1)S(1)}, bf16[4,64,512]{2,1,0:T(8,128)(2,1)}, u32[]{:S(2)}, u32[]{:S(2)}) collective-permute-start(bf16[4,64,512]{2,1,0:T(8,128)(2,1)S(1)} %give.1), channel_id=1, source_target_pairs={{0,1},{1,0},{2,3},{3,2},{4,5},{5,4},{6,7},{7,6},{8,9},{9,8},{10,11... | collective-permute-start | bytes 786440 | tf_op jit(solution)/shard_map/ppermute | solution.py:247
  35.8 3.7 %collective-permute-start.4 = (bf16[128,256]{1,0:T(8,128)(2,1)S(1)}, bf16[128,256]{1,0:T(8,128)(2,1)S(1)}, u32[]{:S(2)}, u32[]{:S(2)}) collective-permute-start(bf16[128,256]{1,0:T(8,128)(2,1)S(1)} %hidden.1.h_own), channel_id=1, source_target_pairs={{0,2},{1,3},{2,0},{3,1},{4,6},{5,7},{6,4},{7,5},{8,10},{9,11},{10,... | collective-permute-start | bytes 196616 | tf_op jit(solution)/shard_map/ppermute | solution.py:247
  35.9 5.6 %collective-permute-start.5 = (bf16[128,256]{1,0:T(8,128)(2,1)S(1)}, bf16[128,256]{1,0:T(8,128)(2,1)S(1)}, u32[]{:S(2)}, u32[]{:S(2)}) collective-permute-start(bf16[128,256]{1,0:T(8,128)(2,1)S(1)} %hidden.1.h_own), channel_id=1, source_target_pairs={{0,6},{1,7},{2,4},{3,5},{4,2},{5,3},{6,0},{7,1},{8,14},{9,15},{10,... | collective-permute-start | bytes 196616 | tf_op jit(solution)/shard_map/ppermute | solution.py:247
  36.5 5.1 %collective-permute-start.6 = (bf16[128,256]{1,0:T(8,128)(2,1)S(1)}, bf16[128,256]{1,0:T(8,128)(2,1)S(1)}, u32[]{:S(2)}, u32[]{:S(2)}) collective-permute-start(bf16[128,256]{1,0:T(8,128)(2,1)S(1)} %hidden.1.h_own), channel_id=1, source_target_pairs={{0,4},{1,5},{2,6},{3,7},{4,0},{5,1},{6,2},{7,3},{8,12},{9,13},{10,... | collective-permute-start | bytes 196616 | tf_op jit(solution)/shard_map/ppermute | solution.py:247
  43.8 16.8 %all-to-all-start.1 = ((f16[32,8,640]{2,1,0:T(8,128)(2,1)}), f16[32,8,640]{2,1,0:T(8,128)(2,1)S(1)}, u32[]{:S(2)}, u32[]{:S(2)}) async-start(f16[32,8,640]{2,1,0:T(8,128)(2,1)} %convert_bitcast_fusion), calls=%async_computation.1 | async-start | bytes 655360 | tf_op jit(solution)/shard_map/all_to_all | solution.py:342
  61.0 3.2 %collective-permute-start.11 = (f32[64,256]{1,0:T(8,128)S(1)}, f32[64,256]{1,0:T(8,128)S(1)}, u32[]{:S(2)}, u32[]{:S(2)}) collective-permute-start(f32[64,256]{1,0:T(8,128)S(1)} %get-tuple-element.28), channel_id=1, source_target_pairs={{0,1},{1,0},{2,3},{3,2},{4,5},{5,4},{6,7},{7,6},{8,9},{9,8},{10,11... | collective-permute-start | bytes 196616 | tf_op jit(solution)/shard_map/ppermute | solution.py:353

commit v8 on v6

--- a/solution.py
+++ b/solution.py
@@ -72,7 +72,7 @@
 
 
 def member(place):
-    return (MEMBERS - 1 - SPAN - place) % MEMBERS
+    return (MEMBERS - 1 - 2 * SPAN - place) % MEMBERS
 
 
 def slots_of(ids, core, experts, copies):
@@ -306,7 +306,8 @@
         compiler_params=PARAMS,
         name="pieces",
     )(*off_chip(expert_down))
-    downs = [ppermute(p, pairs) for p, pairs in zip(pieces[1:], (near, same, across))]
+    d_across = ppermute(pieces[3], across)
+    downs = [ppermute(pieces[1], near), ppermute(pieces[2], same), d_across]
     downs = on_chip(pieces[0], *downs)
     d_giving = pl.pallas_call(
         give_kernel,

time: 65.7 us -> 65.2 us (level)
  starting transfers between devices: 38.6 us -> 37.5 us
    ppermute x1, starting transfers between devices: 3.83 us -> 2.33 us  [per_device(): mixed_out = kept + lax.ppermute(sent, 'tp', swap)]
where the time goes in v8:
time: 65.2 us; the launch traced here: 64.9 us
  starting transfers between devices  37.5 us (58%)
  waiting for transfers between devices  16.5 us (25%)
  Pallas kernels  9.28 us (14%)
  other arithmetic  1.44 us (2%)
    ppermute x11, starting transfers between devices, ppermute(): return lax.ppermute(array, 'tp', pairs)  13.5 us
    all_to_all x1, starting transfers between devices, per_device(): lax.all_to_all(packed.reshape(ep_size, slots, features // 2), 'ep', split...  12.3 us
    all_to_all x1, starting transfers between devices, per_device(): lax.all_to_all(wire, 'ep', split_axis=0, concat_axis=0, tiled=True, axis_...  9.36 us
    ppermute x11, waiting for transfers between devices, ppermute(): return lax.ppermute(array, 'tp', pairs)  9.1 us
    all_to_all x1, waiting for transfers between devices, per_device(): lax.all_to_all(wire, 'ep', split_axis=0, concat_axis=0, tiled=True, axis_...  6.55 us
    ppermute x1, starting transfers between devices, per_device(): mixed_out = kept + lax.ppermute(sent, 'tp', swap)  2.33 us
    pallas_call x1, Pallas kernels, per_device(): pl.pallas_call(functools.partial(pack_kernel, slots=slots), out_shape=plt...  2.31 us
    pallas_call x1, Pallas kernels, per_device(): pl.pallas_call(functools.partial(down_kernel, slots=slots), out_shape=plt...  1.48 us
  transfers between devices with their start and end apart: 14, of which 6 were waited for; matrix products, arithmetic and copies ran while one was open for 0% of the time, Pallas kernels for 11%

profile of v8, /device:TPU:1, one launch (start us, length us, event | category | flops | bytes accessed | tf_op | source)
XLA Modules:
  0.0 64.9 jit_solution(11830839128163606174)
XLA Ops:
  0.0 2.1 %collective-permute-start.1 = (bf16[2,64,2048]{2,1,0:T(8,128)(2,1)}, bf16[2,64,2048]{2,1,0:T(8,128)(2,1)S(1)}, u32[]{:S(2)}, u32[]{:S(2)}) collective-permute-start(bf16[2,64,2048]{2,1,0:T(8,128)(2,1)} %bitcast.14), channel_id=1, source_target_pairs={{0,6},{1,3},{2,0},{3,5},{4,2},{5,7},{6,4},{7,1},{8,14},{9,11},{10,... | collective-permute-start | bytes 1572872 | tf_op jit(solution)/shard_map/ppermute | solution.py:247
  2.1 1.3 %collective-permute-start.2 = (bf16[2,64,2048]{2,1,0:T(8,128)(2,1)}, bf16[2,64,2048]{2,1,0:T(8,128)(2,1)S(1)}, u32[]{:S(2)}, u32[]{:S(2)}) collective-permute-start(bf16[2,64,2048]{2,1,0:T(8,128)(2,1)} %bitcast.16), channel_id=1, source_target_pairs={{0,6},{1,3},{2,0},{3,5},{4,2},{5,7},{6,4},{7,1},{8,14},{9,11},{10,... | collective-permute-start | bytes 1572872 | tf_op jit(solution)/shard_map/ppermute | solution.py:247
  3.4 2.3 %pack.1 = bf16[256,1024]{1,0:T(8,128)(2,1)} custom-call(bf16[64,2048]{1,0:T(8,128)(2,1)} %tokens.1, f32[1,2048]{1,0:T(1,128)} %bitcast.18, f32[1,2048]{1,0:T(1,128)} %bitcast.19, s32[4,64]{1,0:T(4,128)} %bitcast.20), custom_call_target="tpu_custom_call" | custom-call | tf_op jit(solution)/shard_map/pack/pallas_call | solution.py:250
  5.7 12.3 %all-to-all-start = ((bf16[32,8,1024]{2,1,0:T(8,128)(2,1)}), bf16[32,8,1024]{2,1,0:T(8,128)(2,1)S(1)}, u32[]{:S(2)}, u32[]{:S(2)}) async-start(bf16[32,8,1024]{2,1,0:T(8,128)(2,1)} %bitcast.4), calls=%async_computation | async-start | bytes 1048576 | tf_op jit(solution)/shard_map/all_to_all | solution.py:273
  18.1 1.2 %theirs.1 = (bf16[2,64,2048]{2,1,0:T(8,128)(2,1)S(1)}, bf16[2,64,2048]{2,1,0:T(8,128)(2,1)S(1)}) custom-call(bf16[2,64,2048]{2,1,0:T(8,128)(2,1)} %bitcast.15, bf16[2,64,2048]{2,1,0:T(8,128)(2,1)} %bitcast.17), custom_call_target="tpu_custom_call" | custom-call | tf_op jit(solution)/shard_map/theirs/pallas_call | solution.py:278
  19.3 2.3 %collective-permute-start = (bf16[2,64,2048]{2,1,0:T(8,128)(2,1)S(1)}, bf16[2,64,2048]{2,1,0:T(8,128)(2,1)S(1)}, u32[]{:S(2)}, u32[]{:S(2)}) collective-permute-start(bf16[2,64,2048]{2,1,0:T(8,128)(2,1)S(1)} %get-tuple-element.20), channel_id=1, source_target_pairs={{0,1},{1,0},{2,3},{3,2},{4,5},{5,4},{6,7},{7,6},{8,9},{9,8},{10,11... | collective-permute-start | bytes 1572872 | tf_op jit(solution)/shard_map/ppermute | solution.py:247
  21.6 0.0 collective-permute-done.1.gate
  21.6 0.0 collective-permute-done.2.up
  21.6 0.9 %pick.1 = (bf16[2,64,2048]{2,1,0:T(8,128)(2,1)S(1)}, bf16[2,64,2048]{2,1,0:T(8,128)(2,1)}) custom-call(bf16[2,64,2048]{2,1,0:T(8,128)(2,1)S(1)} %collective-permute-done.1.gate, bf16[2,64,2048]{2,1,0:T(8,128)(2,1)S(1)} %collective-permute-done.2.up), custom_call_target="tpu_custom_call" | custom-call | tf_op jit(solution)/shard_map/pick/pallas_call | solution.py:289
  22.5 0.0 collective-permute-start.3
  22.5 1.1 %pieces.1 = (bf16[2,64,512]{2,1,0:T(8,128)(2,1)S(1)}, bf16[2,64,512]{2,1,0:T(8,128)(2,1)S(1)}, bf16[2,64,512]{2,1,0:T(8,128)(2,1)S(1)}, bf16[2,64,512]{2,1,0:T(8,128)(2,1)S(1)}) custom-call(bf16[2,64,2048]{2,1,0:T(8,128)(2,1)} %down.2), custom_call_target="tpu_custom_call" | custom-call | tf_op jit(solution)/shard_map/pieces/pallas_call | solution.py:300
  23.7 1.1 %collective-permute-start.7 = (bf16[2,64,512]{2,1,0:T(8,128)(2,1)S(1)}, bf16[2,64,512]{2,1,0:T(8,128)(2,1)S(1)}, u32[]{:S(2)}, u32[]{:S(2)}) collective-permute-start(bf16[2,64,512]{2,1,0:T(8,128)(2,1)S(1)} %get-tuple-element.24), channel_id=1, source_target_pairs={{0,2},{1,3},{2,0},{3,1},{4,6},{5,7},{6,4},{7,5},{8,10},{9,11},{10,... | collective-permute-start | bytes 393224 | tf_op jit(solution)/shard_map/ppermute | solution.py:247
  24.8 0.0 collective-permute-start.8
  24.8 2.2 %collective-permute-start.9 = (bf16[2,64,512]{2,1,0:T(8,128)(2,1)S(1)}, bf16[2,64,512]{2,1,0:T(8,128)(2,1)S(1)}, u32[]{:S(2)}, u32[]{:S(2)}) collective-permute-start(bf16[2,64,512]{2,1,0:T(8,128)(2,1)S(1)} %get-tuple-element.26), channel_id=1, source_target_pairs={{0,4},{1,5},{2,6},{3,7},{4,0},{5,1},{6,2},{7,3},{8,12},{9,13},{10,... | collective-permute-start | bytes 393224 | tf_op jit(solution)/shard_map/ppermute | solution.py:247
  27.0 1.3 %collective-permute-done.7.first = bf16[2,64,512]{2,1,0:T(8,128)(2,1)S(1)} collective-permute-done((bf16[2,64,512]{2,1,0:T(8,128)(2,1)S(1)}, bf16[2,64,512]{2,1,0:T(8,128)(2,1)S(1)}, u32[]{:S(2)}, u32[]{:S(2)}) %collective-permute-start.7) | collective-permute-done | bytes 131104 | tf_op jit(solution)/shard_map/ppermute | solution.py:247
  28.3 5.4 %collective-permute-done.8.second = bf16[2,64,512]{2,1,0:T(8,128)(2,1)S(1)} collective-permute-done((bf16[2,64,512]{2,1,0:T(8,128)(2,1)S(1)}, bf16[2,64,512]{2,1,0:T(8,128)(2,1)S(1)}, u32[]{:S(2)}, u32[]{:S(2)}) %collective-permute-start.8) | collective-permute-done | bytes 131104 | tf_op jit(solution)/shard_map/ppermute | solution.py:247
  33.7 0.0 collective-permute-done.9.third
  33.7 1.1 %collective-permute-start.10 = (bf16[4,64,512]{2,1,0:T(8,128)(2,1)S(1)}, bf16[4,64,512]{2,1,0:T(8,128)(2,1)}, u32[]{:S(2)}, u32[]{:S(2)}) collective-permute-start(bf16[4,64,512]{2,1,0:T(8,128)(2,1)S(1)} %give.1), channel_id=1, source_target_pairs={{0,1},{1,0},{2,3},{3,2},{4,5},{5,4},{6,7},{7,6},{8,9},{9,8},{10,11... | collective-permute-start | bytes 786440 | tf_op jit(solution)/shard_map/ppermute | solution.py:247
  34.8 0.0 collective-permute-done.swapped
  34.8 0.0 all-to-all-done
  34.8 0.0 collective-permute-done.3.passed
  34.8 1.0 %hidden.1.h_own = bf16[128,256]{1,0:T(8,128)(2,1)S(1)} custom-call(bf16[256,1024]{1,0:T(8,128)(2,1)S(1)} %bitcast.13, bf16[2,64,2048]{2,1,0:T(8,128)(2,1)S(1)} %get-tuple-element.19.mine, bf16[2,64,2048]{2,1,0:T(8,128)(2,1)S(1)} %collective-permute-done.swapped, bf16[2,64,2048]{2,1,0:T(8,128)(2,1)S(1)} %get-tuple-element.21.kept_in, ...), custom_call_target="tpu_custom_call" | custom-call | tf_op jit(solution)/shard_map/hidden/pallas_call | solution.py:322
  35.8 0.1 collective-permute-start.4
  35.9 0.6 collective-permute-start.5
  36.5 2.7 %collective-permute-start.6 = (bf16[128,256]{1,0:T(8,128)(2,1)S(1)}, bf16[128,256]{1,0:T(8,128)(2,1)S(1)}, u32[]{:S(2)}, u32[]{:S(2)}) collective-permute-start(bf16[128,256]{1,0:T(8,128)(2,1)S(1)} %hidden.1.h_own), channel_id=1, source_target_pairs={{0,4},{1,5},{2,6},{3,7},{4,0},{5,1},{6,2},{7,3},{8,12},{9,13},{10,... | collective-permute-start | bytes 196616 | tf_op jit(solution)/shard_map/ppermute | solution.py:247
  39.2 0.0 collective-permute-done.10.other
  39.2 0.4 collective-permute-done.4.h_first
  39.5 2.0 %collective-permute-done.5.h_second = bf16[128,256]{1,0:T(8,128)(2,1)S(1)} collective-permute-done((bf16[128,256]{1,0:T(8,128)(2,1)S(1)}, bf16[128,256]{1,0:T(8,128)(2,1)S(1)}, u32[]{:S(2)}, u32[]{:S(2)}) %collective-permute-start.5) | collective-permute-done | bytes 65568 | tf_op jit(solution)/shard_map/ppermute | solution.py:247
  41.6 0.0 collective-permute-done.6.h_third
  41.6 1.5 %down.3 = f32[256,640]{1,0:T(8,128)S(1)} custom-call(bf16[128,256]{1,0:T(8,128)(2,1)S(1)} %hidden.1.h_own, bf16[128,256]{1,0:T(8,128)(2,1)S(1)} %collective-permute-done.4.h_first, bf16[128,256]{1,0:T(8,128)(2,1)S(1)} %collective-permute-done.5.h_second, bf16[128,256]{1,0:T(8,128)(2,1)S(1)} %collective-permute-done.6.h_third, ...), custom_call_target="tpu_custom_call" | custom-call | tf_op jit(solution)/shard_map/down/pallas_call | solution.py:332
  43.0 0.8 %convert_bitcast_fusion = f16[32,8,640]{2,1,0:T(8,128)(2,1)} fusion(f32[256,640]{1,0:T(8,128)S(1)} %down.3), kind=kLoop, calls=%fused_computation.1 | loop fusion | flops 163840 | bytes 983040 | tf_op jit(solution)/shard_map/reshape | solution.py:340
  43.8 9.4 %all-to-all-start.1 = ((f16[32,8,640]{2,1,0:T(8,128)(2,1)}), f16[32,8,640]{2,1,0:T(8,128)(2,1)S(1)}, u32[]{:S(2)}, u32[]{:S(2)}) async-start(f16[32,8,640]{2,1,0:T(8,128)(2,1)} %convert_bitcast_fusion), calls=%async_computation.1 | async-start | bytes 655360 | tf_op jit(solution)/shard_map/all_to_all | solution.py:341
  53.2 0.9 %factors.1 = (bf16[256,64]{1,0:T(8,128)(2,1)S(1)}, bf16[256,64]{1,0:T(8,128)(2,1)S(1)}) custom-call(s32[4,64]{1,0:T(4,128)} %bitcast.21, f32[4,64]{1,0:T(4,128)} %bitcast.22), custom_call_target="tpu_custom_call" | custom-call | tf_op jit(solution)/shard_map/factors/pallas_call | solution.py:263
  54.1 6.5 %all-to-all-done.1 = f16[32,8,640]{2,1,0:T(8,128)(2,1)S(1)} async-done(((f16[32,8,640]{2,1,0:T(8,128)(2,1)}), f16[32,8,640]{2,1,0:T(8,128)(2,1)S(1)}, u32[]{:S(2)}, u32[]{:S(2)}) %all-to-all-start.1) | async-done | bytes 327712 | tf_op jit(solution)/shard_map/all_to_all | solution.py:341
  60.7 0.3 combine.1
  61.0 2.3 %collective-permute-start.11 = (f32[64,256]{1,0:T(8,128)S(1)}, f32[64,256]{1,0:T(8,128)S(1)}, u32[]{:S(2)}, u32[]{:S(2)}) collective-permute-start(f32[64,256]{1,0:T(8,128)S(1)} %get-tuple-element.28), channel_id=1, source_target_pairs={{0,1},{1,0},{2,3},{3,2},{4,5},{5,4},{6,7},{7,6},{8,9},{9,8},{10,11... | collective-permute-start | bytes 196616 | tf_op jit(solution)/shard_map/ppermute | solution.py:352
  63.3 0.9 %collective-permute-done.11 = f32[64,256]{1,0:T(8,128)S(1)} collective-permute-done((f32[64,256]{1,0:T(8,128)S(1)}, f32[64,256]{1,0:T(8,128)S(1)}, u32[]{:S(2)}, u32[]{:S(2)}) %collective-permute-start.11) | collective-permute-done | bytes 65568 | tf_op jit(solution)/shard_map/ppermute | solution.py:352
  64.2 0.6 add_convert_fusion
  (2 shorter events, 0.1 us)
Async XLA Ops:
  0.0 21.6 %collective-permute-start.1 = (bf16[2,64,2048]{2,1,0:T(8,128)(2,1)}, bf16[2,64,2048]{2,1,0:T(8,128)(2,1)S(1)}, u32[]{:S(2)}, u32[]{:S(2)}) collective-permute-start(bf16[2,64,2048]{2,1,0:T(8,128)(2,1)} %bitcast.14), channel_id=1, source_target_pairs={{0,6},{1,3},{2,0},{3,5},{4,2},{5,7},{6,4},{7,1},{8,14},{9,11},{10,... | collective-permute-start | bytes 1572872 | tf_op jit(solution)/shard_map/ppermute | solution.py:247
  2.1 19.5 %collective-permute-start.2 = (bf16[2,64,2048]{2,1,0:T(8,128)(2,1)}, bf16[2,64,2048]{2,1,0:T(8,128)(2,1)S(1)}, u32[]{:S(2)}, u32[]{:S(2)}) collective-permute-start(bf16[2,64,2048]{2,1,0:T(8,128)(2,1)} %bitcast.16), channel_id=1, source_target_pairs={{0,6},{1,3},{2,0},{3,5},{4,2},{5,7},{6,4},{7,1},{8,14},{9,11},{10,... | collective-permute-start | bytes 1572872 | tf_op jit(solution)/shard_map/ppermute | solution.py:247
  5.7 29.1 %all-to-all-start = ((bf16[32,8,1024]{2,1,0:T(8,128)(2,1)}), bf16[32,8,1024]{2,1,0:T(8,128)(2,1)S(1)}, u32[]{:S(2)}, u32[]{:S(2)}) async-start(bf16[32,8,1024]{2,1,0:T(8,128)(2,1)} %bitcast.4), calls=%async_computation | async-start | bytes 1048576 | tf_op jit(solution)/shard_map/all_to_all | solution.py:273
  19.3 15.5 %collective-permute-start = (bf16[2,64,2048]{2,1,0:T(8,128)(2,1)S(1)}, bf16[2,64,2048]{2,1,0:T(8,128)(2,1)S(1)}, u32[]{:S(2)}, u32[]{:S(2)}) collective-permute-start(bf16[2,64,2048]{2,1,0:T(8,128)(2,1)S(1)} %get-tuple-element.20), channel_id=1, source_target_pairs={{0,1},{1,0},{2,3},{3,2},{4,5},{5,4},{6,7},{7,6},{8,9},{9,8},{10,11... | collective-permute-start | bytes 1572872 | tf_op jit(solution)/shard_map/ppermute | solution.py:247
  22.5 12.3 %collective-permute-start.3 = (bf16[2,64,2048]{2,1,0:T(8,128)(2,1)}, bf16[2,64,2048]{2,1,0:T(8,128)(2,1)S(1)}, u32[]{:S(2)}, u32[]{:S(2)}) collective-permute-start(bf16[2,64,2048]{2,1,0:T(8,128)(2,1)} %get-tuple-element.22), channel_id=1, source_target_pairs={{0,1},{1,0},{2,3},{3,2},{4,5},{5,4},{6,7},{7,6},{8,9},{9,8},{10,11... | collective-permute-start | bytes 1572872 | tf_op jit(solution)/shard_map/ppermute | solution.py:247
  23.7 4.7 %collective-permute-start.7 = (bf16[2,64,512]{2,1,0:T(8,128)(2,1)S(1)}, bf16[2,64,512]{2,1,0:T(8,128)(2,1)S(1)}, u32[]{:S(2)}, u32[]{:S(2)}) collective-permute-start(bf16[2,64,512]{2,1,0:T(8,128)(2,1)S(1)} %get-tuple-element.24), channel_id=1, source_target_pairs={{0,2},{1,3},{2,0},{3,1},{4,6},{5,7},{6,4},{7,5},{8,10},{9,11},{10,... | collective-permute-start | bytes 393224 | tf_op jit(solution)/shard_map/ppermute | solution.py:247
  24.8 9.0 %collective-permute-start.8 = (bf16[2,64,512]{2,1,0:T(8,128)(2,1)S(1)}, bf16[2,64,512]{2,1,0:T(8,128)(2,1)S(1)}, u32[]{:S(2)}, u32[]{:S(2)}) collective-permute-start(bf16[2,64,512]{2,1,0:T(8,128)(2,1)S(1)} %get-tuple-element.25), channel_id=1, source_target_pairs={{0,6},{1,7},{2,4},{3,5},{4,2},{5,3},{6,0},{7,1},{8,14},{9,15},{10,... | collective-permute-start | bytes 393224 | tf_op jit(solution)/shard_map/ppermute | solution.py:247
  24.8 9.0 %collective-permute-start.9 = (bf16[2,64,512]{2,1,0:T(8,128)(2,1)S(1)}, bf16[2,64,512]{2,1,0:T(8,128)(2,1)S(1)}, u32[]{:S(2)}, u32[]{:S(2)}) collective-permute-start(bf16[2,64,512]{2,1,0:T(8,128)(2,1)S(1)} %get-tuple-element.26), channel_id=1, source_target_pairs={{0,4},{1,5},{2,6},{3,7},{4,0},{5,1},{6,2},{7,3},{8,12},{9,13},{10,... | collective-permute-start | bytes 393224 | tf_op jit(solution)/shard_map/ppermute | solution.py:247
  33.7 5.4 %collective-permute-start.10 = (bf16[4,64,512]{2,1,0:T(8,128)(2,1)S(1)}, bf16[4,64,512]{2,1,0:T(8,128)(2,1)}, u32[]{:S(2)}, u32[]{:S(2)}) collective-permute-start(bf16[4,64,512]{2,1,0:T(8,128)(2,1)S(1)} %give.1), channel_id=1, source_target_pairs={{0,1},{1,0},{2,3},{3,2},{4,5},{5,4},{6,7},{7,6},{8,9},{9,8},{10,11... | collective-permute-start | bytes 786440 | tf_op jit(solution)/shard_map/ppermute | solution.py:247
  35.8 3.7 %collective-permute-start.4 = (bf16[128,256]{1,0:T(8,128)(2,1)S(1)}, bf16[128,256]{1,0:T(8,128)(2,1)S(1)}, u32[]{:S(2)}, u32[]{:S(2)}) collective-permute-start(bf16[128,256]{1,0:T(8,128)(2,1)S(1)} %hidden.1.h_own), channel_id=1, source_target_pairs={{0,2},{1,3},{2,0},{3,1},{4,6},{5,7},{6,4},{7,5},{8,10},{9,11},{10,... | collective-permute-start | bytes 196616 | tf_op jit(solution)/shard_map/ppermute | solution.py:247
  35.9 5.6 %collective-permute-start.5 = (bf16[128,256]{1,0:T(8,128)(2,1)S(1)}, bf16[128,256]{1,0:T(8,128)(2,1)S(1)}, u32[]{:S(2)}, u32[]{:S(2)}) collective-permute-start(bf16[128,256]{1,0:T(8,128)(2,1)S(1)} %hidden.1.h_own), channel_id=1, source_target_pairs={{0,6},{1,7},{2,4},{3,5},{4,2},{5,3},{6,0},{7,1},{8,14},{9,15},{10,... | collective-permute-start | bytes 196616 | tf_op jit(solution)/shard_map/ppermute | solution.py:247
  36.5 5.1 %collective-permute-start.6 = (bf16[128,256]{1,0:T(8,128)(2,1)S(1)}, bf16[128,256]{1,0:T(8,128)(2,1)S(1)}, u32[]{:S(2)}, u32[]{:S(2)}) collective-permute-start(bf16[128,256]{1,0:T(8,128)(2,1)S(1)} %hidden.1.h_own), channel_id=1, source_target_pairs={{0,4},{1,5},{2,6},{3,7},{4,0},{5,1},{6,2},{7,3},{8,12},{9,13},{10,... | collective-permute-start | bytes 196616 | tf_op jit(solution)/shard_map/ppermute | solution.py:247
  43.8 16.8 %all-to-all-start.1 = ((f16[32,8,640]{2,1,0:T(8,128)(2,1)}), f16[32,8,640]{2,1,0:T(8,128)(2,1)S(1)}, u32[]{:S(2)}, u32[]{:S(2)}) async-start(f16[32,8,640]{2,1,0:T(8,128)(2,1)} %convert_bitcast_fusion), calls=%async_computation.1 | async-start | bytes 655360 | tf_op jit(solution)/shard_map/all_to_all | solution.py:341
  61.0 3.2 %collective-permute-start.11 = (f32[64,256]{1,0:T(8,128)S(1)}, f32[64,256]{1,0:T(8,128)S(1)}, u32[]{:S(2)}, u32[]{:S(2)}) collective-permute-start(f32[64,256]{1,0:T(8,128)S(1)} %get-tuple-element.28), channel_id=1, source_target_pairs={{0,1},{1,0},{2,3},{3,2},{4,5},{5,4},{6,7},{7,6},{8,9},{9,8},{10,11... | collective-permute-start | bytes 196616 | tf_op jit(solution)/shard_map/ppermute | solution.py:352
